TPU v7x, 512 devices: a 8x2x16 block of a 8x16x16 slice. The times are simulated.
512 devices in a mesh: grp: 2 (over y), tp: 16 (over z), dp: 16 (over x, core).
Axes of the slice: x: 8, y: 2, z: 16, core: 2. Of those that a mesh axis runs over, the one named last changes fastest.
The devices are a block of a 8x16x16 slice.
Arguments:
- stream: bfloat16 [1024, 4096], P(('grp', 'tp'), 'dp'), parts along dimension 0, may hold values from -6 to 6
- lengths: int32 [64], P(('grp', 'dp')), parts along dimension 0, may hold values from 1 to 16, as said below
- input_norm_gain: float32 [2, 4096], P(None, 'dp'), may hold values from 0.1 to 1.9
- query_projection: bfloat16 [2, 4096, 2048], P(None, 'dp', 'tp'), may hold values from -0.09375 to 0.09375
- key_projection: bfloat16 [2, 4096, 2048], P(None, 'dp', 'tp'), may hold values from -0.09375 to 0.09375
- forget_gate_weight: bfloat16 [2, 4096, 2048], P(None, 'dp', 'tp'), may hold values from -0.09375 to 0.09375
- value_projection: bfloat16 [2, 4096, 4096], P(None, 'dp', 'tp'), may hold values from -0.09375 to 0.09375
- output_gate_weight: bfloat16 [2, 4096, 4096], P(None, 'dp', 'tp'), may hold values from -0.09375 to 0.09375
- forget_gate_bias: float32 [2, 2048], P(None, 'tp'), may hold values from -3 to 3
- extra_frame_decay: float32 [2, 1024, 2048], P(None, ('grp', 'dp'), 'tp'), parts along dimension 1, may hold values from -0.7 to 0, as said below
- head_norm_gain: float32 [2, 512], replicated, may hold values from 0.1 to 1.9
- output_projection: bfloat16 [2, 4096, 4096], P(None, 'tp', 'dp'), may hold values from -0.09375 to 0.09375
- memory: float32 [2, 64, 2048, 512], P(None, ('grp', 'dp'), 'tp'), parts along dimension 1, may hold values from -6 to 6
Outputs:
- stream_out: bfloat16 [1024, 4096], P(('grp', 'tp'), 'dp'), parts along dimension 0
- memory_out: float32 [2, 64, 2048, 512], P(None, ('grp', 'dp'), 'tp'), parts along dimension 1
There are 2 independent parts, one for each index of `grp`. A program takes and returns all parts, laid end to end along the dimension named above; an argument that names none is the same for every part. Nothing has to cross between parts.
Inputs may be any that keep to these rules, and one draw needn't show every extreme that they name: `lengths`: live frames of each sequence; at least one sequence has all 16. `extra_frame_decay`: zero at most frames; at the others, for every key channel, a value from -0.7 to -0.22.
All inputs are finite; a program needn't handle non-finite values.
Results may differ from a plain program's by a relative error of at most 0.03.
Values may be sent and summed in bfloat16 or wider, within the bound.
No kernel may reach another device: no remote copies, remote signals or barrier semaphores. Data moves between devices by JAX's collectives and lax.ppermute only.
A program may use at most 64 MiB of HBM per device.

v0:
```python
import jax
import jax.numpy as jnp
from jax import lax
from jax.sharding import PartitionSpec as P

D = 4096
KEY_DIM = 256
VALUE_DIM = 512
BLOCK_LEN = 16


EPS = 1e-06
TIME_CONSTANT = 16.0


def joined_along(parts, dim):
    parts = jnp.moveaxis(parts, 0, dim)
    dims = parts.shape
    return parts.reshape(*dims[:dim], dims[dim] * dims[dim + 1], *dims[dim + 2 :])


def from_everyone(array, axis):
    length = lax.axis_size(axis)
    return lax.all_to_all(
        jnp.broadcast_to(array[None], (length, *array.shape)), axis, 0, 0, tiled=True
    )


def collect(array, axis, dim):
    return joined_along(from_everyone(array, axis), dim)


def in_blocks(array, dim, length):
    before, after = (array.shape[:dim], array.shape[dim + 1 :])
    return jnp.moveaxis(array.reshape(*before, length, -1, *after), dim, 0)


def sum_at_owner(array, axis, dim):
    length = lax.axis_size(axis)
    parts = lax.all_to_all(in_blocks(array, dim, length), axis, 0, 0, tiled=True)
    return jnp.sum(parts, axis=0)


def sent_and_summed(array, axis, dim):
    parts = in_blocks(array, dim, lax.axis_size(axis))
    arrived = lax.all_to_all(parts, axis, split_axis=0, concat_axis=0, tiled=True)
    return arrived.astype(jnp.float32).sum(axis=0)


def swapped(value, axis, distance):
    mask = 2**distance
    pairs = [(source, source ^ mask) for source in range(lax.axis_size(axis))]
    return lax.ppermute(value, axis, pairs)


def recurrence(queries, keys_in, values_in, decay_logarithm, state_in):
    frames = queries.shape[1]
    totals = jnp.cumsum(decay_logarithm, axis=1)
    causal = (jnp.arange(frames)[:, None] >= jnp.arange(frames)[None, :])[None, :, :, None, None]
    spread = totals[:, :, None] - totals[:, None, :]
    decays = jnp.where(causal, jnp.exp(jnp.where(causal, spread, 0.0)), 0.0)
    scores = jnp.einsum("sihk,sijhk,sjhk->shij", queries, decays, keys_in)
    inner_part = jnp.einsum("shij,sjhv->sihv", scores, values_in)
    carried = jnp.einsum("sihk,shkv->sihv", queries * jnp.exp(totals), state_in)
    last_total = totals[:, -1]
    weighted = keys_in * jnp.exp(last_total[:, None] - totals)
    fresh_mem = jnp.exp(last_total)[..., None] * state_in + jnp.einsum(
        "sjhk,sjhv->shkv", weighted, values_in
    )
    return (inner_part + carried, fresh_mem)


def local(
    stream,
    lengths,
    input_norm_gain,
    query_projection,
    key_projection,
    forget_gate_weight,
    value_projection,
    output_gate_weight,
    forget_gate_bias,
    extra_frame_decay,
    head_norm_gain,
    output_projection,
    memory,
):
    key_local = query_projection.shape[2]
    value_local = value_projection.shape[2]
    local_heads = max(1, key_local // KEY_DIM)
    key_width = key_local // local_heads
    seq_local = lengths.shape[0]
    own_tokens = seq_local * BLOCK_LEN
    tp_spot = lax.axis_index("tp")
    position = jnp.arange(BLOCK_LEN, dtype=jnp.int32)
    alive_mask = (position[None, :] < lengths[:, None]).astype(jnp.float32).reshape(own_tokens, 1)
    current = stream
    outputs = []
    for block_layer in range(2):
        residual = current.astype(jnp.float32)
        gathered = collect(current, "tp", 0)
        wide_res = gathered.astype(jnp.float32)
        scaled = (wide_res * input_norm_gain[block_layer]).astype(jnp.bfloat16)
        own_power = sum_at_owner(jnp.sum(wide_res * wide_res, axis=1), "dp", 0)
        row_scale = lax.rsqrt(own_power / D + EPS)[:, None]
        joined = jnp.concatenate(
            [
                query_projection[block_layer],
                key_projection[block_layer],
                forget_gate_weight[block_layer],
                value_projection[block_layer],
                output_gate_weight[block_layer],
            ],
            axis=1,
        )
        summed = (
            sent_and_summed(
                jnp.dot(scaled, joined, preferred_element_type=jnp.float32).astype(jnp.bfloat16),
                "dp",
                0,
            )
            * row_scale
        )
        second_cut = 2 * key_local
        third_cut = 3 * key_local
        fourth_cut = 3 * key_local + value_local
        queries = summed[:, :key_local] * KEY_DIM ** (-0.5)
        keys_in = summed[:, key_local:second_cut] * alive_mask
        forget_preactivation = summed[:, second_cut:third_cut] + forget_gate_bias[block_layer]
        values_in = summed[:, third_cut:fourth_cut]
        gate_pre = summed[:, fourth_cut:]
        decay_logarithm = (
            jax.nn.log_sigmoid(forget_preactivation) / TIME_CONSTANT
            + extra_frame_decay[block_layer]
        ) * alive_mask
        is_upper = tp_spot % 2 == 1
        partner = swapped(values_in.astype(jnp.bfloat16), "tp", 0).astype(values_in.dtype)
        values_full = jnp.where(
            is_upper,
            jnp.concatenate([partner, values_in], 1),
            jnp.concatenate([values_in, partner], 1),
        )
        read_out, fresh_mem = recurrence(
            queries.reshape(seq_local, BLOCK_LEN, local_heads, key_width),
            keys_in.reshape(seq_local, BLOCK_LEN, local_heads, key_width),
            values_full.reshape(seq_local, BLOCK_LEN, local_heads, VALUE_DIM),
            decay_logarithm.reshape(seq_local, BLOCK_LEN, local_heads, key_width),
            memory[block_layer].reshape(seq_local, local_heads, key_width, VALUE_DIM),
        )
        read_out = read_out + swapped(read_out.astype(jnp.bfloat16), "tp", 0).astype(read_out.dtype)
        normed = (
            read_out
            * lax.rsqrt(jnp.mean(read_out * read_out, axis=3, keepdims=True) + EPS)
            * head_norm_gain[block_layer]
        )
        flat = normed.reshape(own_tokens, local_heads * VALUE_DIM)
        flat = lax.dynamic_slice_in_dim(flat, tp_spot % 2 * value_local, value_local, 1)
        gated = (flat * jax.nn.silu(gate_pre) * alive_mask).astype(jnp.bfloat16)
        partials = jnp.dot(
            collect(gated, "dp", 0),
            output_projection[block_layer],
            preferred_element_type=jnp.float32,
        )
        mixer_out = sent_and_summed(partials.astype(jnp.bfloat16), "tp", 0).astype(jnp.bfloat16)
        current = (residual + mixer_out.astype(jnp.float32)).astype(jnp.bfloat16)
        outputs.append(fresh_mem.reshape(seq_local, key_local, VALUE_DIM))
    return (current, jnp.stack(outputs))


def solution(mesh):
    placed = (
        P(("grp", "tp"), "dp"),
        P(("grp", "dp")),
        P(None, "dp"),
        P(None, "dp", "tp"),
        P(None, "dp", "tp"),
        P(None, "dp", "tp"),
        P(None, "dp", "tp"),
        P(None, "dp", "tp"),
        P(None, "tp"),
        P(None, ("grp", "dp"), "tp"),
        P(),
        P(None, "tp", "dp"),
        P(None, ("grp", "dp"), "tp", None),
    )
    return jax.shard_map(
        local,
        mesh=mesh,
        in_specs=placed,
        out_specs=(P(("grp", "tp"), "dp"), P(None, ("grp", "dp"), "tp", None)),
        check_vma=False,
    )
```

profile of v0, /device:TPU:80, one launch (start us, length us, event | category | flops | bytes accessed | tf_op | source)
XLA Modules:
  0.0 278.6 jit_solution(15113498230399927122)
XLA Ops:
  0.7 1.5 broadcast_in_dim.38
  2.2 43.7 %all-to-all-start = ((bf16[16,32,256]{2,1,0:T(8,128)(2,1)}), bf16[16,32,256]{2,1,0:T(8,128)(2,1)S(1)}, u32[]{:S(2)}, u32[]{:S(2)}) async-start(bf16[16,32,256]{2,1,0:T(8,128)(2,1)} %broadcast_in_dim.38), calls=%async_computation | async-start | bytes 524288 | tf_op jit(solution)/shard_map/all_to_all | solution.py:24
  45.9 0.9 bitcast_dynamic-update-slice_fusion.6
  47.0 17.0 %all-to-all-done = bf16[16,32,256]{2,1,0:T(8,128)(2,1)S(1)} async-done(((bf16[16,32,256]{2,1,0:T(8,128)(2,1)}), bf16[16,32,256]{2,1,0:T(8,128)(2,1)S(1)}, u32[]{:S(2)}, u32[]{:S(2)}) %all-to-all-start) | async-done | bytes 262176 | tf_op jit(solution)/shard_map/all_to_all | solution.py:24
  64.0 0.7 multiply_reduce_fusion.1
  64.8 7.6 %all-to-all-start.2 = ((f32[16,1,32]{2,1,0:T(1,128)}), f32[16,1,32]{2,1,0:T(1,128)S(1)}, u32[]{:S(2)}, u32[]{:S(2)}) async-start(f32[16,1,32]{2,1,0:T(1,128)} %bitcast.9), calls=%async_computation.2 | async-start | bytes 16384 | tf_op jit(solution)/shard_map/all_to_all | solution.py:40
  72.4 1.4 convolution_convert_fusion.1
  73.8 5.9 %all-to-all-done.2 = f32[16,1,32]{2,1,0:T(1,128)S(1)} async-done(((f32[16,1,32]{2,1,0:T(1,128)}), f32[16,1,32]{2,1,0:T(1,128)S(1)}, u32[]{:S(2)}, u32[]{:S(2)}) %all-to-all-start.2) | async-done | bytes 2080 | tf_op jit(solution)/shard_map/all_to_all | solution.py:40
  79.7 4.1 %all-to-all-start.1 = ((bf16[16,32,896]{2,1,0:T(8,128)(2,1)}), bf16[16,32,896]{2,1,0:T(8,128)(2,1)S(1)}, u32[]{:S(2)}, u32[]{:S(2)}) async-start(bf16[16,32,896]{2,1,0:T(8,128)(2,1)} %bitcast.7), calls=%async_computation.1 | async-start | bytes 1835008 | tf_op jit(solution)/shard_map/all_to_all | solution.py:46
  84.1 23.0 %all-to-all-done.1 = bf16[16,32,896]{2,1,0:T(8,128)(2,1)S(1)} async-done(((bf16[16,32,896]{2,1,0:T(8,128)(2,1)}), bf16[16,32,896]{2,1,0:T(8,128)(2,1)S(1)}, u32[]{:S(2)}, u32[]{:S(2)}) %all-to-all-start.1) | async-done | bytes 917536 | tf_op jit(solution)/shard_map/all_to_all | solution.py:46
  107.3 3.6 %collective-permute-start = (bf16[32,256]{1,0:T(8,128)(2,1)S(1)}, bf16[32,256]{1,0:T(8,128)(2,1)S(1)}, u32[]{:S(2)}, u32[]{:S(2)}) collective-permute-start(bf16[32,256]{1,0:T(8,128)(2,1)S(1)} %slice.209), channel_id=1, source_target_pairs={{0,16},{16,0},{32,48},{48,32},{64,80},{80,64},{96,112},{112,96},{1... | collective-permute-start | bytes 49160 | tf_op jit(solution)/shard_map/ppermute | solution.py:53
  111.4 1.5 collective-permute-done
  113.0 3.6 %collective-permute-start.1 = (bf16[2,16,1,512]{3,1,0,2:T(8,128)(2,1)S(1)}, bf16[2,16,1,512]{3,1,0,2:T(8,128)(2,1)S(1)}, u32[]{:S(2)}, u32[]{:S(2)}) collective-permute-start(bf16[2,16,1,512]{3,1,0,2:T(8,128)(2,1)S(1)} %get-tuple-element.28), channel_id=1, source_target_pairs={{0,16},{16,0},{32,48},{48,32},{64,80},{80,64},{96,112},{112,96},{1... | collective-permute-start | bytes 98312 | tf_op jit(solution)/shard_map/ppermute | solution.py:53
  116.7 2.6 collective-permute-done.1
  119.5 15.6 %all_to_all.58 = bf16[16,32,256]{2,1,0:T(8,128)(2,1)S(1)} all-to-all(bf16[16,32,256]{2,1,0:T(8,128)(2,1)S(1)} %broadcast_in_dim.41), channel_id=1, replica_groups=mesh['grp'=2,'tp'=16,'dp'=16] {'dp'}, dimensions={0} | all-to-all | bytes 524288 | tf_op jit(solution)/shard_map/all_to_all | solution.py:24
  135.4 25.0 %all_to_all.59 = bf16[16,32,256]{2,1,0:T(8,128)(2,1)S(1)} all-to-all(bf16[16,32,256]{2,1,0:T(8,128)(2,1)S(1)} %bitcast.139), channel_id=1, replica_groups=mesh['grp'=2,'tp'=16,'dp'=16] {'tp'}, dimensions={0} | all-to-all | bytes 524288 | tf_op jit(solution)/shard_map/all_to_all | solution.py:46
  160.5 24.1 %all_to_all.60 = bf16[16,32,256]{2,1,0:T(8,128)(2,1)S(1)} all-to-all(bf16[16,32,256]{2,1,0:T(8,128)(2,1)S(1)} %broadcast_in_dim.76), channel_id=1, replica_groups=mesh['grp'=2,'tp'=16,'dp'=16] {'tp'}, dimensions={0} | all-to-all | bytes 524288 | tf_op jit(solution)/shard_map/all_to_all | solution.py:24
  184.6 0.7 multiply_reduce_fusion
  185.3 3.9 %all-to-all-start.7 = ((f32[16,1,32]{2,1,0:T(1,128)}), f32[16,1,32]{2,1,0:T(1,128)S(1)}, u32[]{:S(2)}, u32[]{:S(2)}) async-start(f32[16,1,32]{2,1,0:T(1,128)} %bitcast.44), calls=%async_computation.7 | async-start | bytes 16384 | tf_op jit(solution)/shard_map/all_to_all | solution.py:40
  189.3 1.4 convolution_convert_fusion
  190.7 5.7 %all-to-all-done.7 = f32[16,1,32]{2,1,0:T(1,128)S(1)} async-done(((f32[16,1,32]{2,1,0:T(1,128)}), f32[16,1,32]{2,1,0:T(1,128)S(1)}, u32[]{:S(2)}, u32[]{:S(2)}) %all-to-all-start.7) | async-done | bytes 2080 | tf_op jit(solution)/shard_map/all_to_all | solution.py:40
  196.4 4.1 %all-to-all-start.6 = ((bf16[16,32,896]{2,1,0:T(8,128)(2,1)}), bf16[16,32,896]{2,1,0:T(8,128)(2,1)S(1)}, u32[]{:S(2)}, u32[]{:S(2)}) async-start(bf16[16,32,896]{2,1,0:T(8,128)(2,1)} %bitcast.42), calls=%async_computation.6 | async-start | bytes 1835008 | tf_op jit(solution)/shard_map/all_to_all | solution.py:46
  200.5 23.2 %all-to-all-done.6 = bf16[16,32,896]{2,1,0:T(8,128)(2,1)S(1)} async-done(((bf16[16,32,896]{2,1,0:T(8,128)(2,1)}), bf16[16,32,896]{2,1,0:T(8,128)(2,1)S(1)}, u32[]{:S(2)}, u32[]{:S(2)}) %all-to-all-start.6) | async-done | bytes 917536 | tf_op jit(solution)/shard_map/all_to_all | solution.py:46
  223.9 3.8 %collective-permute-start.2 = (bf16[32,256]{1,0:T(8,128)(2,1)S(1)}, bf16[32,256]{1,0:T(8,128)(2,1)S(1)}, u32[]{:S(2)}, u32[]{:S(2)}) collective-permute-start(bf16[32,256]{1,0:T(8,128)(2,1)S(1)} %slice.208), channel_id=1, source_target_pairs={{0,16},{16,0},{32,48},{48,32},{64,80},{80,64},{96,112},{112,96},{1... | collective-permute-start | bytes 49160 | tf_op jit(solution)/shard_map/ppermute | solution.py:53
  228.2 1.4 collective-permute-done.2
  229.7 3.8 %collective-permute-start.3 = (bf16[2,16,1,512]{3,1,0,2:T(8,128)(2,1)S(1)}, bf16[2,16,1,512]{3,1,0,2:T(8,128)(2,1)S(1)}, u32[]{:S(2)}, u32[]{:S(2)}) collective-permute-start(bf16[2,16,1,512]{3,1,0,2:T(8,128)(2,1)S(1)} %get-tuple-element.30), channel_id=1, source_target_pairs={{0,16},{16,0},{32,48},{48,32},{64,80},{80,64},{96,112},{112,96},{1... | collective-permute-start | bytes 98312 | tf_op jit(solution)/shard_map/ppermute | solution.py:53
  233.5 2.3 collective-permute-done.3
  236.1 15.7 %all_to_all.61 = bf16[16,32,256]{2,1,0:T(8,128)(2,1)S(1)} all-to-all(bf16[16,32,256]{2,1,0:T(8,128)(2,1)S(1)} %broadcast_in_dim.77), channel_id=1, replica_groups=mesh['grp'=2,'tp'=16,'dp'=16] {'dp'}, dimensions={0} | all-to-all | bytes 524288 | tf_op jit(solution)/shard_map/all_to_all | solution.py:24
  251.8 0.9 convolution_convert_fusion.2
  252.7 6.2 %all-to-all-start.9 = ((bf16[16,32,256]{2,1,0:T(8,128)(2,1)}), bf16[16,32,256]{2,1,0:T(8,128)(2,1)S(1)}, u32[]{:S(2)}, u32[]{:S(2)}) async-start(bf16[16,32,256]{2,1,0:T(8,128)(2,1)} %bitcast.69), calls=%async_computation.9 | async-start | bytes 524288 | tf_op jit(solution)/shard_map/all_to_all | solution.py:46
  259.5 1.0 pad_maximum_fusion
  260.5 17.4 %all-to-all-done.9 = bf16[16,32,256]{2,1,0:T(8,128)(2,1)S(1)} async-done(((bf16[16,32,256]{2,1,0:T(8,128)(2,1)}), bf16[16,32,256]{2,1,0:T(8,128)(2,1)S(1)}, u32[]{:S(2)}, u32[]{:S(2)}) %all-to-all-start.9) | async-done | bytes 262176 | tf_op jit(solution)/shard_map/all_to_all | solution.py:46
  (78 shorter events, 4.3 us)
Async XLA Ops:
  0.6 46.2 %copy-start.9 = (f32[2,256]{1,0:T(2,128)S(1)}, f32[2,256]{1,0:T(2,128)}, u32[]{:S(2)}) copy-start(f32[2,256]{1,0:T(2,128)} %param.15) | copy-start | bytes 6148
  0.6 46.2 %copy-start.4 = (bf16[2,256,128]{2,1,0:T(8,128)(2,1)S(1)}, bf16[2,256,128]{2,1,0:T(8,128)(2,1)}, u32[]{:S(2)}) copy-start(bf16[2,256,128]{2,1,0:T(8,128)(2,1)} %param.17) | copy-start | bytes 393220
  0.7 46.2 %copy-start.5 = (bf16[2,256,128]{2,1,0:T(8,128)(2,1)S(1)}, bf16[2,256,128]{2,1,0:T(8,128)(2,1)}, u32[]{:S(2)}) copy-start(bf16[2,256,128]{2,1,0:T(8,128)(2,1)} %param.18) | copy-start | bytes 393220
  0.7 46.3 %copy-start.2 = (bf16[2,256,256]{2,1,0:T(8,128)(2,1)S(1)}, bf16[2,256,256]{2,1,0:T(8,128)(2,1)}, u32[]{:S(2)}) copy-start(bf16[2,256,256]{2,1,0:T(8,128)(2,1)} %param.19) | copy-start | bytes 786436
  0.7 46.3 %copy-start.3 = (bf16[2,256,256]{2,1,0:T(8,128)(2,1)S(1)}, bf16[2,256,256]{2,1,0:T(8,128)(2,1)}, u32[]{:S(2)}) copy-start(bf16[2,256,256]{2,1,0:T(8,128)(2,1)} %param.20) | copy-start | bytes 786436
  2.2 61.8 %all-to-all-start = ((bf16[16,32,256]{2,1,0:T(8,128)(2,1)}), bf16[16,32,256]{2,1,0:T(8,128)(2,1)S(1)}, u32[]{:S(2)}, u32[]{:S(2)}) async-start(bf16[16,32,256]{2,1,0:T(8,128)(2,1)} %broadcast_in_dim.38), calls=%async_computation | async-start | bytes 524288 | tf_op jit(solution)/shard_map/all_to_all | solution.py:24
  64.8 15.0 %all-to-all-start.2 = ((f32[16,1,32]{2,1,0:T(1,128)}), f32[16,1,32]{2,1,0:T(1,128)S(1)}, u32[]{:S(2)}, u32[]{:S(2)}) async-start(f32[16,1,32]{2,1,0:T(1,128)} %bitcast.9), calls=%async_computation.2 | async-start | bytes 16384 | tf_op jit(solution)/shard_map/all_to_all | solution.py:40
  73.8 10.0 %copy-start.11 = (s32[2]{0:T(128)S(1)}, s32[2]{0:T(128)}, u32[]{:S(2)}) copy-start(s32[2]{0:T(128)} %param.14) | copy-start | bytes 28
  73.8 10.2 %copy-start.10 = (f32[2,128]{1,0:T(2,128)S(1)}, f32[2,128]{1,0:T(2,128)}, u32[]{:S(2)}) copy-start(f32[2,128]{1,0:T(2,128)} %param.21) | copy-start | bytes 3076
  79.7 27.3 %all-to-all-start.1 = ((bf16[16,32,896]{2,1,0:T(8,128)(2,1)}), bf16[16,32,896]{2,1,0:T(8,128)(2,1)S(1)}, u32[]{:S(2)}, u32[]{:S(2)}) async-start(bf16[16,32,896]{2,1,0:T(8,128)(2,1)} %bitcast.7), calls=%async_computation.1 | async-start | bytes 1835008 | tf_op jit(solution)/shard_map/all_to_all | solution.py:46
  83.8 27.0 %copy-start.7 = (f32[2,32,128]{2,1,0:T(8,128)S(1)}, f32[2,32,128]{2,1,0:T(8,128)}, u32[]{:S(2)}) copy-start(f32[2,32,128]{2,1,0:T(8,128)} %param.22) | copy-start | bytes 98308
  83.8 27.1 %copy-start = (f32[2,2,128,512]{3,2,1,0:T(8,128)S(1)}, f32[2,2,128,512]{3,2,1,0:T(8,128)}, u32[]{:S(2)}) copy-start(f32[2,2,128,512]{3,2,1,0:T(8,128)} %param.25) | copy-start | bytes 3145732
  107.2 9.5 %copy-start.8 = (f32[2,512]{1,0:T(2,128)S(1)}, f32[2,512]{1,0:T(2,128)}, u32[]{:S(2)}) copy-start(f32[2,512]{1,0:T(2,128)} %param.23) | copy-start | bytes 12292
  107.3 5.7 %collective-permute-start = (bf16[32,256]{1,0:T(8,128)(2,1)S(1)}, bf16[32,256]{1,0:T(8,128)(2,1)S(1)}, u32[]{:S(2)}, u32[]{:S(2)}) collective-permute-start(bf16[32,256]{1,0:T(8,128)(2,1)S(1)} %slice.209), channel_id=1, source_target_pairs={{0,16},{16,0},{32,48},{48,32},{64,80},{80,64},{96,112},{112,96},{1... | collective-permute-start | bytes 49160 | tf_op jit(solution)/shard_map/ppermute | solution.py:53
  111.1 24.0 %copy-start.1 = (bf16[2,256,256]{2,1,0:T(8,128)(2,1)S(1)}, bf16[2,256,256]{2,1,0:T(8,128)(2,1)}, u32[]{:S(2)}) copy-start(bf16[2,256,256]{2,1,0:T(8,128)(2,1)} %param.24) | copy-start | bytes 786436
  113.0 6.2 %collective-permute-start.1 = (bf16[2,16,1,512]{3,1,0,2:T(8,128)(2,1)S(1)}, bf16[2,16,1,512]{3,1,0,2:T(8,128)(2,1)S(1)}, u32[]{:S(2)}, u32[]{:S(2)}) collective-permute-start(bf16[2,16,1,512]{3,1,0,2:T(8,128)(2,1)S(1)} %get-tuple-element.28), channel_id=1, source_target_pairs={{0,16},{16,0},{32,48},{48,32},{64,80},{80,64},{96,112},{112,96},{1... | collective-permute-start | bytes 98312 | tf_op jit(solution)/shard_map/ppermute | solution.py:53
  119.5 40.9 %copy-start.6 = (bf16[32,256]{1,0:T(8,128)(2,1)S(1)}, bf16[32,256]{1,0:T(8,128)(2,1)}, u32[]{:S(2)}) copy-start(bf16[32,256]{1,0:T(8,128)(2,1)} %param.13) | copy-start | bytes 49156
  185.3 11.0 %all-to-all-start.7 = ((f32[16,1,32]{2,1,0:T(1,128)}), f32[16,1,32]{2,1,0:T(1,128)S(1)}, u32[]{:S(2)}, u32[]{:S(2)}) async-start(f32[16,1,32]{2,1,0:T(1,128)} %bitcast.44), calls=%async_computation.7 | async-start | bytes 16384 | tf_op jit(solution)/shard_map/all_to_all | solution.py:40
  196.4 27.3 %all-to-all-start.6 = ((bf16[16,32,896]{2,1,0:T(8,128)(2,1)}), bf16[16,32,896]{2,1,0:T(8,128)(2,1)S(1)}, u32[]{:S(2)}, u32[]{:S(2)}) async-start(bf16[16,32,896]{2,1,0:T(8,128)(2,1)} %bitcast.42), calls=%async_computation.6 | async-start | bytes 1835008 | tf_op jit(solution)/shard_map/all_to_all | solution.py:46
  223.9 5.7 %collective-permute-start.2 = (bf16[32,256]{1,0:T(8,128)(2,1)S(1)}, bf16[32,256]{1,0:T(8,128)(2,1)S(1)}, u32[]{:S(2)}, u32[]{:S(2)}) collective-permute-start(bf16[32,256]{1,0:T(8,128)(2,1)S(1)} %slice.208), channel_id=1, source_target_pairs={{0,16},{16,0},{32,48},{48,32},{64,80},{80,64},{96,112},{112,96},{1... | collective-permute-start | bytes 49160 | tf_op jit(solution)/shard_map/ppermute | solution.py:53
  229.7 6.1 %collective-permute-start.3 = (bf16[2,16,1,512]{3,1,0,2:T(8,128)(2,1)S(1)}, bf16[2,16,1,512]{3,1,0,2:T(8,128)(2,1)S(1)}, u32[]{:S(2)}, u32[]{:S(2)}) collective-permute-start(bf16[2,16,1,512]{3,1,0,2:T(8,128)(2,1)S(1)} %get-tuple-element.30), channel_id=1, source_target_pairs={{0,16},{16,0},{32,48},{48,32},{64,80},{80,64},{96,112},{112,96},{1... | collective-permute-start | bytes 98312 | tf_op jit(solution)/shard_map/ppermute | solution.py:53
  252.7 25.3 %all-to-all-start.9 = ((bf16[16,32,256]{2,1,0:T(8,128)(2,1)}), bf16[16,32,256]{2,1,0:T(8,128)(2,1)S(1)}, u32[]{:S(2)}, u32[]{:S(2)}) async-start(bf16[16,32,256]{2,1,0:T(8,128)(2,1)} %bitcast.69), calls=%async_computation.9 | async-start | bytes 524288 | tf_op jit(solution)/shard_map/all_to_all | solution.py:46
where the time goes:
time: 280 us; the launch traced here: 279 us
  waiting for transfers between devices  100 us (36%)
  starting transfers between devices  84.2 us (30%)
  blocking collectives  80.4 us (29%)
  matrix products  5.52 us (2%)
  other arithmetic  4.62 us (2%)
    all_to_all x3, waiting for transfers between devices, sent_and_summed(): lax.all_to_all(parts, axis, split_axis=0, concat_axis=0, tiled=True)  63.6 us
    all_to_all x3, blocking collectives, from_everyone(): lax.all_to_all(jnp.broadcast_to(array[None], (length, *array.shape)), axi...  55.4 us
    all_to_all x1, starting transfers between devices, from_everyone(): lax.all_to_all(jnp.broadcast_to(array[None], (length, *array.shape)), axi...  43.7 us
    all_to_all x1, blocking collectives, sent_and_summed(): lax.all_to_all(parts, axis, split_axis=0, concat_axis=0, tiled=True)  25 us
    all_to_all x1, waiting for transfers between devices, from_everyone(): lax.all_to_all(jnp.broadcast_to(array[None], (length, *array.shape)), axi...  17 us
    ppermute x4, starting transfers between devices, swapped(): return lax.ppermute(value, axis, pairs)  14.7 us
    all_to_all x3, starting transfers between devices, sent_and_summed(): lax.all_to_all(parts, axis, split_axis=0, concat_axis=0, tiled=True)  14.3 us
    all_to_all x2, waiting for transfers between devices, sum_at_owner(): lax.all_to_all(in_blocks(array, dim, length), axis, 0, 0, tiled=True)  11.6 us
  transfers between devices with their start and end apart: 10, of which 10 were waited for; matrix products, arithmetic and copies ran while one was open for 2% of the time, Pallas kernels for 0%

commit v1 on v0

v1 whole, which is shorter than its diff:
```python
import jax
import jax.numpy as jnp
from jax import lax
from jax.sharding import Mesh
from jax.sharding import PartitionSpec as P

D = 4096
KEY_DIM = 256
VALUE_DIM = 512
BLOCK_LEN = 16

EPS = 1e-06
TIME_CONSTANT = 16.0

ALONG_TP = ("a", "b")
ALONG_X = ("b", "c")


def exchange(array, axes):
    return lax.all_to_all(array, axes, 0, 0, tiled=True)


def to_all(array, axes):
    length = lax.axis_size(axes)
    return exchange(jnp.broadcast_to(array[None], (length, *array.shape)), axes)


def other(array, axis):
    return lax.ppermute(array, axis, [(0, 1), (1, 0)])


def pick(array, index, dim):
    return lax.dynamic_index_in_dim(array, index, dim, keepdims=False)


def ordered(own, theirs, spot, dim):
    return jnp.where(
        spot == 0, jnp.concatenate([own, theirs], dim), jnp.concatenate([theirs, own], dim)
    )


def three_terms(value):
    high = lax.reduce_precision(value, 8, 7)
    rest = value - high
    middle = lax.reduce_precision(rest, 8, 7)
    return [part.astype(jnp.bfloat16) for part in (high, middle, rest - middle)]


def local(
    stream,
    lengths,
    input_norm_gain,
    query_projection,
    key_projection,
    forget_gate_weight,
    value_projection,
    output_gate_weight,
    forget_gate_bias,
    extra_frame_decay,
    head_norm_gain,
    output_projection,
    memory,
):
    f32, bf16 = jnp.float32, jnp.bfloat16
    tall, wide = lax.axis_size("a"), lax.axis_size("c")
    a, b, k = lax.axis_index("a"), lax.axis_index("b"), lax.axis_index("k")
    frames, features = stream.shape
    keys = query_projection.shape[2]
    values = value_projection.shape[2]
    layers = memory.shape[0]

    gathered = to_all(stream, ALONG_TP).reshape(tall, 2, frames, features)
    x_own = pick(gathered, k, 1)
    x_other = other(pick(gathered, 1 - k, 1), "k")
    x = jnp.where(k == 0, jnp.stack([x_own, x_other], 1), jnp.stack([x_other, x_own], 1))

    gains = input_norm_gain[:, None]
    gains = ordered(gains, other(gains, "k"), k, 1)
    weights = [
        jnp.concatenate(
            [
                query_projection[n],
                key_projection[n],
                forget_gate_weight[n],
                value_projection[n],
                output_gate_weight[n],
            ],
            1,
        )
        for n in range(layers)
    ]
    weights = [ordered(w, other(w, "k"), k, 0) for w in weights]
    out_weights = ordered(output_projection[0], other(output_projection[0], "k"), k, 1)

    decay = extra_frame_decay.reshape(layers, 2, BLOCK_LEN, keys)
    decay_own = pick(decay, b, 1)
    decay = ordered(decay_own, other(pick(decay, 1 - b, 1), "b"), b, 2)
    bias = ordered(forget_gate_bias, other(forget_gate_bias, "b"), b, 1)
    state_own = pick(memory, b, 1)
    state_next = pick(memory, 1 - b, 1)
    state_other = other(state_next.astype(bf16), "b")
    position = jnp.arange(BLOCK_LEN, dtype=jnp.int32)
    alive = (position < pick(lengths, b, 0)).astype(f32)[:, None]
    causal = position[:, None] >= position[None, :]

    outputs = []
    for n in range(layers):
        wide_x = x.astype(f32)
        scaled = (wide_x * gains[n][None, :, None, :]).astype(bf16)
        scaled = jnp.swapaxes(scaled, 1, 2).reshape(tall * frames, 2 * features)
        power = jnp.sum(wide_x * wide_x, axis=(1, 3)).reshape(tall * frames, 1)
        partial = jnp.dot(scaled, weights[n], preferred_element_type=f32).astype(bf16)
        extra = three_terms(power)
        pad = jnp.zeros((tall * frames, 128 - len(extra)), bf16)
        sent = jnp.concatenate([partial, *extra, pad], 1)
        columns = sent.shape[1]
        sent = sent.reshape(tall, 2, BLOCK_LEN, columns).swapaxes(0, 1)
        got = exchange(sent.reshape(2 * tall, BLOCK_LEN, columns), ALONG_X)
        got = got.reshape(2, wide, BLOCK_LEN, columns).astype(f32).sum(axis=1)
        base = 3 * keys + 2 * values
        power = got[0, :, base : base + 1] + got[0, :, base + 1 : base + 2] + got[0, :, base + 2 : base + 3]
        got = got[:, :, :base] * lax.rsqrt(power / D + EPS)
        both = lambda low, high: jnp.concatenate([got[0, :, low:high], got[1, :, low:high]], 1)
        queries = both(0, keys) * KEY_DIM ** (-0.5)
        keys_in = both(keys, 2 * keys) * alive
        forget = both(2 * keys, 3 * keys) + bias[n]
        values_in = both(3 * keys, 3 * keys + values)
        gate = both(3 * keys + values, base)
        log_decay = (jax.nn.log_sigmoid(forget) / TIME_CONSTANT + decay[n]) * alive

        totals = jnp.cumsum(log_decay, axis=0)
        spread = totals[:, None] - totals[None, :]
        decays = jnp.where(causal[..., None], jnp.exp(jnp.where(causal[..., None], spread, 0.0)), 0.0)
        scores = jnp.einsum("ik,ijk,jk->ij", queries, decays, keys_in)
        carried = (queries * jnp.exp(totals)).reshape(BLOCK_LEN, 2, keys)
        read = (
            jnp.dot(scores, values_in)
            + jnp.dot(pick(carried, b, 1), state_own[n])
            + jnp.dot(pick(carried, 1 - b, 1).astype(bf16), state_other[n], preferred_element_type=f32)
        )
        normed = read * lax.rsqrt(jnp.mean(read * read, axis=1, keepdims=True) + EPS) * head_norm_gain[n]
        gated = (normed * jax.nn.silu(gate) * alive).astype(bf16)
        halves = gated.reshape(BLOCK_LEN, 2, values).swapaxes(0, 1)
        sent = jnp.broadcast_to(halves[:, None], (2, wide, BLOCK_LEN, values))
        got = exchange(sent.reshape(2 * wide, BLOCK_LEN, values), ALONG_X)

        last = totals[-1:]
        weighted = (keys_in * jnp.exp(last - totals)).reshape(BLOCK_LEN, 2, keys)
        kept = jnp.exp(last).reshape(2, keys)
        fresh_own = pick(kept, b, 0)[:, None] * state_own[n] + jnp.einsum(
            "jk,jv->kv", pick(weighted, b, 1), values_in
        )
        note = jnp.concatenate(
            [
                pick(weighted, 1 - b, 1),
                values_in,
                jnp.broadcast_to(pick(kept, 1 - b, 0)[None], (BLOCK_LEN, keys)),
            ],
            1,
        )
        note = other(note, "b")
        fresh_next = note[0, keys + 2 * values :][:, None] * state_next[n] + jnp.einsum(
            "jk,jv->kv", note[:, :keys], note[:, keys : keys + 2 * values]
        )
        outputs.append(
            jnp.where(b == 0, jnp.stack([fresh_own, fresh_next]), jnp.stack([fresh_next, fresh_own]))
        )

        if n + 1 < layers:
            partial = jnp.dot(
                got.reshape(2 * wide * BLOCK_LEN, values), out_weights, preferred_element_type=f32
            ).astype(bf16)
            partial = partial.reshape(2, wide, BLOCK_LEN, 2, features).transpose(1, 3, 0, 2, 4)
            residual = pick(pick(x, a, 0), b, 0)
        else:
            got = ordered(got[None], other(got, "k")[None], k, 0)
            partial = jnp.dot(
                got.reshape(4 * wide * BLOCK_LEN, values),
                output_projection[n],
                preferred_element_type=f32,
            ).astype(bf16)
            partial = partial.reshape(2, 2, wide, BLOCK_LEN, features).transpose(2, 0, 1, 3, 4)
            here = pick(x, a, 0)
            residual = jnp.where(b == k, pick(here, k, 0), other(pick(here, 1 - k, 0), "k"))
        arrived = exchange(partial.reshape(2 * wide, frames, features), ALONG_TP)
        mixer_out = arrived.astype(f32).sum(axis=0).astype(bf16)
        current = (residual.astype(f32) + mixer_out.astype(f32)).astype(bf16)
        if n + 1 < layers:
            x = to_all(current, ALONG_TP).reshape(tall, 2, frames, features)
    return current, jnp.stack(outputs)


def solution(mesh):
    grp, tp, dp = (mesh.shape[name] for name in ("grp", "tp", "dp"))
    fine = Mesh(mesh.devices.reshape(grp, tp // 2, 2, dp // 2, 2), ("grp", "a", "b", "c", "k"))
    tp, dp = ("a", "b"), ("c", "k")
    group_tp, group_dp = ("grp", *tp), ("grp", *dp)
    placed = (
        P(group_tp, dp),
        P(group_dp),
        P(None, dp),
        P(None, dp, tp),
        P(None, dp, tp),
        P(None, dp, tp),
        P(None, dp, tp),
        P(None, dp, tp),
        P(None, tp),
        P(None, group_dp, tp),
        P(),
        P(None, tp, dp),
        P(None, group_dp, tp, None),
    )
    return jax.shard_map(
        local,
        mesh=fine,
        in_specs=placed,
        out_specs=(P(group_tp, dp), P(None, group_dp, tp, None)),
        check_vma=False,
    )
```

time: 280 us -> 231 us (0.82)
  blocking collectives: 80.4 us -> 0 us
  starting transfers between devices: 84.2 us -> 122 us
  waiting for transfers between devices: 100 us -> 87.6 us
  local copies, waits for them, and re-layouts: 2.78 us -> 11.1 us
    all_to_all x4 -> x0, blocking collectives: 80.4 us -> none  [the longest x3 55.4 us: from_everyone(): lax.all_to_all(jnp.broadcast_to(array[None], (length, *array.shape)), axi...]
    all_to_all x6 -> x8, starting transfers between devices: 69.5 us -> 91.8 us  [exchange(): return lax.all_to_all(array, axes, 0, 0, tiled=True)]
    ppermute x4 -> x12, starting transfers between devices: 14.7 us -> 29.9 us  [other(): return lax.ppermute(array, axis, [(0, 1), (1, 0)])]
    all_to_all x6 -> x8, waiting for transfers between devices: 92.2 us -> 84.9 us  [exchange(): return lax.all_to_all(array, axes, 0, 0, tiled=True)]
    ppermute x4 -> x12, waiting for transfers between devices: 7.81 us -> 2.63 us  [other(): return lax.ppermute(array, axis, [(0, 1), (1, 0)])]
  transfers between devices with their start and end apart: 10 -> 20, of which waited for: 10 -> 10; matrix products, arithmetic and copies ran while one was open for 2% -> 4% of each run, Pallas kernels for 0% -> 0%
where the time goes in v1:
time: 231 us; the launch traced here: 230 us
  starting transfers between devices  122 us (53%)
  waiting for transfers between devices  87.6 us (38%)
  local copies, waits for them, and re-layouts  11.1 us (5%)
  other arithmetic  4.22 us (2%)
  matrix products  3.77 us (2%)
    all_to_all x8, starting transfers between devices, exchange(): return lax.all_to_all(array, axes, 0, 0, tiled=True)  91.8 us
    all_to_all x8, waiting for transfers between devices, exchange(): return lax.all_to_all(array, axes, 0, 0, tiled=True)  84.9 us
    ppermute x12, starting transfers between devices, other(): return lax.ppermute(array, axis, [(0, 1), (1, 0)])  29.9 us
  transfers between devices with their start and end apart: 20, of which 10 were waited for; matrix products, arithmetic and copies ran while one was open for 4% of the time, Pallas kernels for 0%

profile of v1, /device:TPU:80, one launch (start us, length us, event | category | flops | bytes accessed | tf_op | source)
XLA Modules:
  0.0 229.9 jit_solution(16142399681483771322)
XLA Ops:
  0.7 1.5 broadcast_in_dim.96
  2.2 43.7 %all-to-all-start = ((bf16[16,32,256]{2,1,0:T(8,128)(2,1)}), bf16[16,32,256]{2,1,0:T(8,128)(2,1)S(1)}, u32[]{:S(2)}, u32[]{:S(2)}) async-start(bf16[16,32,256]{2,1,0:T(8,128)(2,1)} %broadcast_in_dim.96), calls=%async_computation | async-start | bytes 524288 | tf_op jit(solution)/shard_map/all_to_all | solution.py:20
  45.9 2.0 collective-permute-start.1
  48.9 2.4 %collective-permute-start.2 = (bf16[256,896]{1,0:T(8,128)(2,1)S(1)}, bf16[256,896]{1,0:T(8,128)(2,1)S(1)}, u32[]{:S(2)}, u32[]{:S(2)}) collective-permute-start(bf16[256,896]{1,0:T(8,128)(2,1)S(1)} %get-tuple-element.5), channel_id=1, source_target_pairs={{0,1},{1,0},{2,3},{3,2},{4,5},{5,4},{6,7},{7,6},{8,9},{9,8},{10,11... | collective-permute-start | bytes 1376264 | tf_op jit(solution)/shard_map/ppermute | solution.py:29
  51.4 12.6 %all-to-all-done = bf16[16,32,256]{2,1,0:T(8,128)(2,1)S(1)} async-done(((bf16[16,32,256]{2,1,0:T(8,128)(2,1)}), bf16[16,32,256]{2,1,0:T(8,128)(2,1)S(1)}, u32[]{:S(2)}, u32[]{:S(2)}) %all-to-all-start) | async-done | bytes 262176 | tf_op jit(solution)/shard_map/all_to_all | solution.py:20
  64.0 2.0 collective-permute-start
  66.0 1.3 collective-permute-done
  70.1 8.8 %all-to-all-start.1 = ((bf16[16,16,1024]{2,1,0:T(8,128)(2,1)}), bf16[16,16,1024]{2,1,0:T(8,128)(2,1)S(1)}, u32[]{:S(2)}, u32[]{:S(2)}) async-start(bf16[16,16,1024]{2,1,0:T(8,128)(2,1)} %bitcast.15), calls=%async_computation.1 | async-start | bytes 1048576 | tf_op jit(solution)/shard_map/all_to_all | solution.py:20
  79.0 3.7 %collective-permute-start.4 = (f32[2,16,128]{2,1,0:T(8,128)S(1)}, f32[2,16,128]{2,1,0:T(8,128)S(1)}, u32[]{:S(2)}, u32[]{:S(2)}) collective-permute-start(f32[2,16,128]{2,1,0:T(8,128)S(1)} %get-tuple-element.45), channel_id=1, source_target_pairs={{0,16},{16,0},{1,17},{17,1},{2,18},{18,2},{3,19},{19,3},{4,20},{20... | collective-permute-start | bytes 49160 | tf_op jit(solution)/shard_map/ppermute | solution.py:29
  82.7 2.3 collective-permute-start.3
  85.0 3.7 %collective-permute-start.5 = (bf16[2,128,512]{2,1,0:T(8,128)(2,1)S(1)}, bf16[2,128,512]{2,1,0:T(8,128)(2,1)S(1)}, u32[]{:S(2)}, u32[]{:S(2)}) collective-permute-start(bf16[2,128,512]{2,1,0:T(8,128)(2,1)S(1)} %fusion.16), channel_id=1, source_target_pairs={{0,16},{16,0},{1,17},{17,1},{2,18},{18,2},{3,19},{19,3},{4,20},{20... | collective-permute-start | bytes 786440 | tf_op jit(solution)/shard_map/ppermute | solution.py:29
  90.0 4.0 %all-to-all-done.1 = bf16[16,16,1024]{2,1,0:T(8,128)(2,1)S(1)} async-done(((bf16[16,16,1024]{2,1,0:T(8,128)(2,1)}), bf16[16,16,1024]{2,1,0:T(8,128)(2,1)S(1)}, u32[]{:S(2)}, u32[]{:S(2)}) %all-to-all-start.1) | async-done | bytes 524320 | tf_op jit(solution)/shard_map/all_to_all | solution.py:20
  96.1 7.2 %all-to-all-start.2 = ((bf16[16,16,256]{2,1,0:T(8,128)(2,1)}), bf16[16,16,256]{2,1,0:T(8,128)(2,1)S(1)}, u32[]{:S(2)}, u32[]{:S(2)}) async-start(bf16[16,16,256]{2,1,0:T(8,128)(2,1)} %bitcast.46), calls=%async_computation.2 | async-start | bytes 262144 | tf_op jit(solution)/shard_map/all_to_all | solution.py:20
  103.3 2.0 collective-permute-start.6
  105.3 1.3 collective-permute-done.6
  106.6 5.1 %all-to-all-done.2 = bf16[16,16,256]{2,1,0:T(8,128)(2,1)S(1)} async-done(((bf16[16,16,256]{2,1,0:T(8,128)(2,1)}), bf16[16,16,256]{2,1,0:T(8,128)(2,1)S(1)}, u32[]{:S(2)}, u32[]{:S(2)}) %all-to-all-start.2) | async-done | bytes 131104 | tf_op jit(solution)/shard_map/all_to_all | solution.py:20
  112.7 5.8 %all-to-all-start.3 = ((bf16[16,32,256]{2,1,0:T(8,128)(2,1)}), bf16[16,32,256]{2,1,0:T(8,128)(2,1)S(1)}, u32[]{:S(2)}, u32[]{:S(2)}) async-start(bf16[16,32,256]{2,1,0:T(8,128)(2,1)} %bitcast.50), calls=%async_computation.3 | async-start | bytes 524288 | tf_op jit(solution)/shard_map/all_to_all | solution.py:20
  118.6 16.2 %all-to-all-done.3 = bf16[16,32,256]{2,1,0:T(8,128)(2,1)S(1)} async-done(((bf16[16,32,256]{2,1,0:T(8,128)(2,1)}), bf16[16,32,256]{2,1,0:T(8,128)(2,1)S(1)}, u32[]{:S(2)}, u32[]{:S(2)}) %all-to-all-start.3) | async-done | bytes 262176 | tf_op jit(solution)/shard_map/all_to_all | solution.py:20
  135.6 5.1 %all-to-all-start.4 = ((bf16[16,32,256]{2,1,0:T(8,128)(2,1)}), bf16[16,32,256]{2,1,0:T(8,128)(2,1)S(1)}, u32[]{:S(2)}, u32[]{:S(2)}) async-start(bf16[16,32,256]{2,1,0:T(8,128)(2,1)} %broadcast_in_dim.101), calls=%async_computation.4 | async-start | bytes 524288 | tf_op jit(solution)/shard_map/all_to_all | solution.py:20
  140.7 2.0 collective-permute-start.8
  142.7 14.2 %all-to-all-done.4 = bf16[16,32,256]{2,1,0:T(8,128)(2,1)S(1)} async-done(((bf16[16,32,256]{2,1,0:T(8,128)(2,1)}), bf16[16,32,256]{2,1,0:T(8,128)(2,1)S(1)}, u32[]{:S(2)}, u32[]{:S(2)}) %all-to-all-start.4) | async-done | bytes 262176 | tf_op jit(solution)/shard_map/all_to_all | solution.py:20
  159.6 8.0 %all-to-all-start.5 = ((bf16[16,16,1024]{2,1,0:T(8,128)(2,1)}), bf16[16,16,1024]{2,1,0:T(8,128)(2,1)S(1)}, u32[]{:S(2)}, u32[]{:S(2)}) async-start(bf16[16,16,1024]{2,1,0:T(8,128)(2,1)} %bitcast.63), calls=%async_computation.5 | async-start | bytes 1048576 | tf_op jit(solution)/shard_map/all_to_all | solution.py:20
  167.7 2.0 collective-permute-start.7
  169.7 11.6 %all-to-all-done.5 = bf16[16,16,1024]{2,1,0:T(8,128)(2,1)S(1)} async-done(((bf16[16,16,1024]{2,1,0:T(8,128)(2,1)}), bf16[16,16,1024]{2,1,0:T(8,128)(2,1)S(1)}, u32[]{:S(2)}, u32[]{:S(2)}) %all-to-all-start.5) | async-done | bytes 524320 | tf_op jit(solution)/shard_map/all_to_all | solution.py:20
  183.4 6.3 %all-to-all-start.6 = ((bf16[16,16,256]{2,1,0:T(8,128)(2,1)}), bf16[16,16,256]{2,1,0:T(8,128)(2,1)S(1)}, u32[]{:S(2)}, u32[]{:S(2)}) async-start(bf16[16,16,256]{2,1,0:T(8,128)(2,1)} %bitcast.89), calls=%async_computation.6 | async-start | bytes 262144 | tf_op jit(solution)/shard_map/all_to_all | solution.py:20
  189.8 3.7 %collective-permute-start.11 = (f32[16,768]{1,0:T(8,128)S(1)}, f32[16,768]{1,0:T(8,128)S(1)}, u32[]{:S(2)}, u32[]{:S(2)}) collective-permute-start(f32[16,768]{1,0:T(8,128)S(1)} %maximum_maximum_fusion.1), channel_id=1, source_target_pairs={{0,16},{16,0},{1,17},{17,1},{2,18},{18,2},{3,19},{19,3},{4,20},{20... | collective-permute-start | bytes 147464 | tf_op jit(solution)/shard_map/ppermute | solution.py:29
  193.5 4.5 %all-to-all-done.6 = bf16[16,16,256]{2,1,0:T(8,128)(2,1)S(1)} async-done(((bf16[16,16,256]{2,1,0:T(8,128)(2,1)}), bf16[16,16,256]{2,1,0:T(8,128)(2,1)S(1)}, u32[]{:S(2)}, u32[]{:S(2)}) %all-to-all-start.6) | async-done | bytes 131104 | tf_op jit(solution)/shard_map/all_to_all | solution.py:20
  198.1 1.9 collective-permute-start.9
  200.3 2.6 %collective-permute-start.10 = (f32[16,768]{1,0:T(8,128)S(1)}, f32[16,768]{1,0:T(8,128)S(1)}, u32[]{:S(2)}, u32[]{:S(2)}) collective-permute-start(f32[16,768]{1,0:T(8,128)S(1)} %maximum_maximum_fusion), channel_id=1, source_target_pairs={{0,16},{16,0},{1,17},{17,1},{2,18},{18,2},{3,19},{19,3},{4,20},{20... | collective-permute-start | bytes 147464 | tf_op jit(solution)/shard_map/ppermute | solution.py:29
  204.1 6.7 %all-to-all-start.7 = ((bf16[16,32,256]{2,1,0:T(8,128)(2,1)}), bf16[16,32,256]{2,1,0:T(8,128)(2,1)S(1)}, u32[]{:S(2)}, u32[]{:S(2)}) async-start(bf16[16,32,256]{2,1,0:T(8,128)(2,1)} %bitcast.96), calls=%async_computation.7 | async-start | bytes 524288 | tf_op jit(solution)/shard_map/all_to_all | solution.py:20
  211.4 1.0 pad_maximum_fusion
  212.5 16.8 %all-to-all-done.7 = bf16[16,32,256]{2,1,0:T(8,128)(2,1)S(1)} async-done(((bf16[16,32,256]{2,1,0:T(8,128)(2,1)}), bf16[16,32,256]{2,1,0:T(8,128)(2,1)S(1)}, u32[]{:S(2)}, u32[]{:S(2)}) %all-to-all-start.7) | async-done | bytes 262176 | tf_op jit(solution)/shard_map/all_to_all | solution.py:20
  (145 shorter events, 16.5 us)
Async XLA Ops:
  0.6 48.1 %copy-start.4 = (bf16[2,256,128]{2,1,0:T(8,128)(2,1)S(1)}, bf16[2,256,128]{2,1,0:T(8,128)(2,1)}, u32[]{:S(2)}) copy-start(bf16[2,256,128]{2,1,0:T(8,128)(2,1)} %param.17) | copy-start | bytes 393220
  0.6 48.2 %copy-start.5 = (bf16[2,256,128]{2,1,0:T(8,128)(2,1)S(1)}, bf16[2,256,128]{2,1,0:T(8,128)(2,1)}, u32[]{:S(2)}) copy-start(bf16[2,256,128]{2,1,0:T(8,128)(2,1)} %param.18) | copy-start | bytes 393220
  0.7 48.2 %copy-start.2 = (bf16[2,256,256]{2,1,0:T(8,128)(2,1)S(1)}, bf16[2,256,256]{2,1,0:T(8,128)(2,1)}, u32[]{:S(2)}) copy-start(bf16[2,256,256]{2,1,0:T(8,128)(2,1)} %param.19) | copy-start | bytes 786436
  0.7 48.2 %copy-start.3 = (bf16[2,256,256]{2,1,0:T(8,128)(2,1)S(1)}, bf16[2,256,256]{2,1,0:T(8,128)(2,1)}, u32[]{:S(2)}) copy-start(bf16[2,256,256]{2,1,0:T(8,128)(2,1)} %param.20) | copy-start | bytes 786436
  2.2 61.8 %all-to-all-start = ((bf16[16,32,256]{2,1,0:T(8,128)(2,1)}), bf16[16,32,256]{2,1,0:T(8,128)(2,1)S(1)}, u32[]{:S(2)}, u32[]{:S(2)}) async-start(bf16[16,32,256]{2,1,0:T(8,128)(2,1)} %broadcast_in_dim.96), calls=%async_computation | async-start | bytes 524288 | tf_op jit(solution)/shard_map/all_to_all | solution.py:20
  45.9 5.5 %copy-start.8 = (f32[2,256]{1,0:T(2,128)S(1)}, f32[2,256]{1,0:T(2,128)}, u32[]{:S(2)}) copy-start(f32[2,256]{1,0:T(2,128)} %param.15) | copy-start | bytes 6148
  45.9 5.5 %collective-permute-start.1 = (f32[2,1,256]{2,0,1:T(2,128)}, f32[2,1,256]{2,0,1:T(2,128)S(1)}, u32[]{:S(2)}, u32[]{:S(2)}) collective-permute-start(f32[2,1,256]{2,0,1:T(2,128)} %bitcast.335), channel_id=1, source_target_pairs={{0,1},{1,0},{2,3},{3,2},{4,5},{5,4},{6,7},{7,6},{8,9},{9,8},{10,11... | collective-permute-start | bytes 6152 | tf_op jit(solution)/shard_map/ppermute | solution.py:29
  48.9 18.9 %collective-permute-start.2 = (bf16[256,896]{1,0:T(8,128)(2,1)S(1)}, bf16[256,896]{1,0:T(8,128)(2,1)S(1)}, u32[]{:S(2)}, u32[]{:S(2)}) collective-permute-start(bf16[256,896]{1,0:T(8,128)(2,1)S(1)} %get-tuple-element.5), channel_id=1, source_target_pairs={{0,1},{1,0},{2,3},{3,2},{4,5},{5,4},{6,7},{7,6},{8,9},{9,8},{10,11... | collective-permute-start | bytes 1376264 | tf_op jit(solution)/shard_map/ppermute | solution.py:29
  64.0 3.3 %collective-permute-start = (bf16[8,32,256]{2,1,0:T(8,128)(2,1)S(1)}, bf16[8,32,256]{2,1,0:T(8,128)(2,1)S(1)}, u32[]{:S(2)}, u32[]{:S(2)}) collective-permute-start(bf16[8,32,256]{2,1,0:T(8,128)(2,1)S(1)} %get-tuple-element.8), channel_id=1, source_target_pairs={{0,1},{1,0},{2,3},{3,2},{4,5},{5,4},{6,7},{7,6},{8,9},{9,8},{10,11... | collective-permute-start | bytes 393224 | tf_op jit(solution)/shard_map/ppermute | solution.py:29
  69.0 9.9 %copy-start.6 = (f32[2,32,128]{2,1,0:T(8,128)S(1)}, f32[2,32,128]{2,1,0:T(8,128)}, u32[]{:S(2)}) copy-start(f32[2,32,128]{2,1,0:T(8,128)} %param.22) | copy-start | bytes 98308
  69.1 13.6 %copy-start.9 = (f32[2,128]{1,0:T(2,128)S(1)}, f32[2,128]{1,0:T(2,128)}, u32[]{:S(2)}) copy-start(f32[2,128]{1,0:T(2,128)} %param.21) | copy-start | bytes 3076
  69.1 15.9 %copy-start = (f32[2,2,128,512]{3,2,1,0:T(8,128)S(1)}, f32[2,2,128,512]{3,2,1,0:T(8,128)}, u32[]{:S(2)}) copy-start(f32[2,2,128,512]{3,2,1,0:T(8,128)} %param.25) | copy-start | bytes 3145732
  70.1 18.5 %copy-start.10 = (s32[2]{0:T(128)S(1)}, s32[2]{0:T(128)}, u32[]{:S(2)}) copy-start(s32[2]{0:T(128)} %param.14) | copy-start | bytes 28
  70.1 19.1 %copy-start.7 = (f32[2,512]{1,0:T(2,128)S(1)}, f32[2,512]{1,0:T(2,128)}, u32[]{:S(2)}) copy-start(f32[2,512]{1,0:T(2,128)} %param.23) | copy-start | bytes 12292
  70.1 23.8 %all-to-all-start.1 = ((bf16[16,16,1024]{2,1,0:T(8,128)(2,1)}), bf16[16,16,1024]{2,1,0:T(8,128)(2,1)S(1)}, u32[]{:S(2)}, u32[]{:S(2)}) async-start(bf16[16,16,1024]{2,1,0:T(8,128)(2,1)} %bitcast.15), calls=%async_computation.1 | async-start | bytes 1048576 | tf_op jit(solution)/shard_map/all_to_all | solution.py:20
  79.0 11.0 %collective-permute-start.4 = (f32[2,16,128]{2,1,0:T(8,128)S(1)}, f32[2,16,128]{2,1,0:T(8,128)S(1)}, u32[]{:S(2)}, u32[]{:S(2)}) collective-permute-start(f32[2,16,128]{2,1,0:T(8,128)S(1)} %get-tuple-element.45), channel_id=1, source_target_pairs={{0,16},{16,0},{1,17},{17,1},{2,18},{18,2},{3,19},{19,3},{4,20},{20... | collective-permute-start | bytes 49160 | tf_op jit(solution)/shard_map/ppermute | solution.py:29
  82.7 7.3 %collective-permute-start.3 = (f32[2,128]{1,0:T(2,128)S(1)}, f32[2,128]{1,0:T(2,128)S(1)}, u32[]{:S(2)}, u32[]{:S(2)}) collective-permute-start(f32[2,128]{1,0:T(2,128)S(1)} %copy-done.9), channel_id=1, source_target_pairs={{0,16},{16,0},{1,17},{17,1},{2,18},{18,2},{3,19},{19,3},{4,20},{20... | collective-permute-start | bytes 3080 | tf_op jit(solution)/shard_map/ppermute | solution.py:29
  85.0 10.0 %collective-permute-start.5 = (bf16[2,128,512]{2,1,0:T(8,128)(2,1)S(1)}, bf16[2,128,512]{2,1,0:T(8,128)(2,1)S(1)}, u32[]{:S(2)}, u32[]{:S(2)}) collective-permute-start(bf16[2,128,512]{2,1,0:T(8,128)(2,1)S(1)} %fusion.16), channel_id=1, source_target_pairs={{0,16},{16,0},{1,17},{17,1},{2,18},{18,2},{3,19},{19,3},{4,20},{20... | collective-permute-start | bytes 786440 | tf_op jit(solution)/shard_map/ppermute | solution.py:29
  94.3 9.0 %copy-start.1 = (bf16[2,256,256]{2,1,0:T(8,128)(2,1)S(1)}, bf16[2,256,256]{2,1,0:T(8,128)(2,1)}, u32[]{:S(2)}) copy-start(bf16[2,256,256]{2,1,0:T(8,128)(2,1)} %param.24) | copy-start | bytes 786436
  96.1 15.6 %all-to-all-start.2 = ((bf16[16,16,256]{2,1,0:T(8,128)(2,1)}), bf16[16,16,256]{2,1,0:T(8,128)(2,1)S(1)}, u32[]{:S(2)}, u32[]{:S(2)}) async-start(bf16[16,16,256]{2,1,0:T(8,128)(2,1)} %bitcast.46), calls=%async_computation.2 | async-start | bytes 262144 | tf_op jit(solution)/shard_map/all_to_all | solution.py:20
  103.3 3.3 %collective-permute-start.6 = (bf16[256,256]{1,0:T(8,128)(2,1)S(1)}, bf16[256,256]{1,0:T(8,128)(2,1)S(1)}, u32[]{:S(2)}, u32[]{:S(2)}) collective-permute-start(bf16[256,256]{1,0:T(8,128)(2,1)S(1)} %slice_bitcast_fusion.4), channel_id=1, source_target_pairs={{0,1},{1,0},{2,3},{3,2},{4,5},{5,4},{6,7},{7,6},{8,9},{9,8},{10,11... | collective-permute-start | bytes 393224 | tf_op jit(solution)/shard_map/ppermute | solution.py:29
  112.7 22.1 %all-to-all-start.3 = ((bf16[16,32,256]{2,1,0:T(8,128)(2,1)}), bf16[16,32,256]{2,1,0:T(8,128)(2,1)S(1)}, u32[]{:S(2)}, u32[]{:S(2)}) async-start(bf16[16,32,256]{2,1,0:T(8,128)(2,1)} %bitcast.50), calls=%async_computation.3 | async-start | bytes 524288 | tf_op jit(solution)/shard_map/all_to_all | solution.py:20
  135.6 21.3 %all-to-all-start.4 = ((bf16[16,32,256]{2,1,0:T(8,128)(2,1)}), bf16[16,32,256]{2,1,0:T(8,128)(2,1)S(1)}, u32[]{:S(2)}, u32[]{:S(2)}) async-start(bf16[16,32,256]{2,1,0:T(8,128)(2,1)} %broadcast_in_dim.101), calls=%async_computation.4 | async-start | bytes 524288 | tf_op jit(solution)/shard_map/all_to_all | solution.py:20
  140.7 16.5 %collective-permute-start.8 = (bf16[256,896]{1,0:T(8,128)(2,1)S(1)}, bf16[256,896]{1,0:T(8,128)(2,1)S(1)}, u32[]{:S(2)}, u32[]{:S(2)}) collective-permute-start(bf16[256,896]{1,0:T(8,128)(2,1)S(1)} %get-tuple-element.4), channel_id=1, source_target_pairs={{0,1},{1,0},{2,3},{3,2},{4,5},{5,4},{6,7},{7,6},{8,9},{9,8},{10,11... | collective-permute-start | bytes 1376264 | tf_op jit(solution)/shard_map/ppermute | solution.py:29
  159.6 21.7 %all-to-all-start.5 = ((bf16[16,16,1024]{2,1,0:T(8,128)(2,1)}), bf16[16,16,1024]{2,1,0:T(8,128)(2,1)S(1)}, u32[]{:S(2)}, u32[]{:S(2)}) async-start(bf16[16,16,1024]{2,1,0:T(8,128)(2,1)} %bitcast.63), calls=%async_computation.5 | async-start | bytes 1048576 | tf_op jit(solution)/shard_map/all_to_all | solution.py:20
  167.7 61.6 %collective-permute-start.7 = (bf16[32,256]{1,0:T(8,128)(2,1)S(1)}, bf16[32,256]{1,0:T(8,128)(2,1)S(1)}, u32[]{:S(2)}, u32[]{:S(2)}) collective-permute-start(bf16[32,256]{1,0:T(8,128)(2,1)S(1)} %dynamic-slice_bitcast_fusion.7), channel_id=1, source_target_pairs={{0,1},{1,0},{2,3},{3,2},{4,5},{5,4},{6,7},{7,6},{8,9},{9,8},{10,11... | collective-permute-start | bytes 49160 | tf_op jit(solution)/shard_map/ppermute | solution.py:29
  183.4 14.7 %all-to-all-start.6 = ((bf16[16,16,256]{2,1,0:T(8,128)(2,1)}), bf16[16,16,256]{2,1,0:T(8,128)(2,1)S(1)}, u32[]{:S(2)}, u32[]{:S(2)}) async-start(bf16[16,16,256]{2,1,0:T(8,128)(2,1)} %bitcast.89), calls=%async_computation.6 | async-start | bytes 262144 | tf_op jit(solution)/shard_map/all_to_all | solution.py:20
  189.8 21.0 %collective-permute-start.11 = (f32[16,768]{1,0:T(8,128)S(1)}, f32[16,768]{1,0:T(8,128)S(1)}, u32[]{:S(2)}, u32[]{:S(2)}) collective-permute-start(f32[16,768]{1,0:T(8,128)S(1)} %maximum_maximum_fusion.1), channel_id=1, source_target_pairs={{0,16},{16,0},{1,17},{17,1},{2,18},{18,2},{3,19},{19,3},{4,20},{20... | collective-permute-start | bytes 147464 | tf_op jit(solution)/shard_map/ppermute | solution.py:29
  198.1 5.0 %collective-permute-start.9 = (bf16[16,16,256]{2,1,0:T(8,128)(2,1)S(1)}, bf16[16,16,256]{2,1,0:T(8,128)(2,1)S(1)}, u32[]{:S(2)}, u32[]{:S(2)}) collective-permute-start(bf16[16,16,256]{2,1,0:T(8,128)(2,1)S(1)} %all-to-all-done.6), channel_id=1, source_target_pairs={{0,1},{1,0},{2,3},{3,2},{4,5},{5,4},{6,7},{7,6},{8,9},{9,8},{10,11... | collective-permute-start | bytes 393224 | tf_op jit(solution)/shard_map/ppermute | solution.py:29
  200.3 10.8 %collective-permute-start.10 = (f32[16,768]{1,0:T(8,128)S(1)}, f32[16,768]{1,0:T(8,128)S(1)}, u32[]{:S(2)}, u32[]{:S(2)}) collective-permute-start(f32[16,768]{1,0:T(8,128)S(1)} %maximum_maximum_fusion), channel_id=1, source_target_pairs={{0,16},{16,0},{1,17},{17,1},{2,18},{18,2},{3,19},{19,3},{4,20},{20... | collective-permute-start | bytes 147464 | tf_op jit(solution)/shard_map/ppermute | solution.py:29
  204.1 25.1 %all-to-all-start.7 = ((bf16[16,32,256]{2,1,0:T(8,128)(2,1)}), bf16[16,32,256]{2,1,0:T(8,128)(2,1)S(1)}, u32[]{:S(2)}, u32[]{:S(2)}) async-start(bf16[16,32,256]{2,1,0:T(8,128)(2,1)} %bitcast.96), calls=%async_computation.7 | async-start | bytes 524288 | tf_op jit(solution)/shard_map/all_to_all | solution.py:20

commit v2 on v1

v2 whole, which is shorter than its diff:
```python
import functools

import jax
import jax.numpy as jnp
from jax import lax
from jax.experimental import pallas as pl
from jax.experimental.pallas import tpu as pltpu
from jax.sharding import Mesh
from jax.sharding import PartitionSpec as P

D = 4096
KEY_DIM = 256
VALUE_DIM = 512
BLOCK_LEN = 16

EPS = 1e-06
TIME_CONSTANT = 16.0

ALONG_TP = ("a", "b")
ALONG_X = ("b", "c")


def exchange(array, axes):
    return lax.all_to_all(array, axes, 0, 0, tiled=True)


def to_all(array, axes):
    length = lax.axis_size(axes)
    return exchange(jnp.broadcast_to(array[None], (length, *array.shape)), axes)


def other(array, axis):
    return lax.ppermute(array, axis, [(0, 1), (1, 0)])


def pick(array, index, dim):
    return lax.dynamic_index_in_dim(array, index, dim, keepdims=False)


def ordered(own, theirs, spot, dim):
    return jnp.where(
        spot == 0, jnp.concatenate([own, theirs], dim), jnp.concatenate([theirs, own], dim)
    )


LANES = 128
F32, BF16 = jnp.float32, jnp.bfloat16
EACH_ROW = (((1,), (1,)), ((), ()))
EACH_COLUMN = (((0,), (0,)), ((), ()))


def dot(left, right, dims=(((1,), (0,)), ((), ()))):
    return lax.dot_general(left, right, dims, preferred_element_type=F32)


def kernel(body, outs, *args):
    vmem = pl.BlockSpec(memory_space=pltpu.VMEM)
    return pl.pallas_call(
        body,
        out_shape=jax.tree.map(lambda out: jax.ShapeDtypeStruct(*out), outs, is_leaf=lambda x: isinstance(x[1], type)),
        in_specs=[vmem] * len(args),
        out_specs=jax.tree.map(lambda out: vmem, outs, is_leaf=lambda x: isinstance(x[1], type)),
    )(*args)


def copies_body(in_ref, out_ref):
    value = in_ref[...]
    for spot in range(out_ref.shape[0]):
        out_ref[spot] = value


def project_body(n, x_ref, mine_ref, theirs_ref, gain_ref, gain_next_ref, out_ref):
    k = lax.axis_index("k")
    tall, _, frames, features = x_ref.shape
    wide = out_ref.shape[0] // 2
    tiles = out_ref.shape[1] // BLOCK_LEN
    columns = tiles * LANES
    ones = jnp.ones((8, features), BF16)
    total, power = 0.0, 0.0
    for half, w_ref, g_ref in ((k, mine_ref, gain_ref), (1 - k, theirs_ref, gain_next_ref)):
        x = x_ref[:, half].reshape(tall * frames, features).astype(F32)
        scaled = (x * g_ref[n : n + 1, :]).astype(BF16)
        total = total + dot(scaled, w_ref[:, n * columns : (n + 1) * columns])
        square = x * x
        high = square.astype(BF16)
        low = (square - high.astype(F32)).astype(BF16)
        power = power + dot(ones, high, EACH_ROW) + dot(ones, low, EACH_ROW)
    total = total.astype(BF16)
    high = power.astype(BF16).astype(F32)
    middle = (power - high).astype(BF16).astype(F32)
    low = power - high - middle
    row = lax.broadcasted_iota(jnp.int32, power.shape, 0)
    terms = jnp.where(row == 0, high, jnp.where(row == 1, middle, jnp.where(row == 2, low, 0.0)))
    terms = terms.astype(BF16)
    for spot in range(2 * wide):
        j, c = divmod(spot, wide)
        start = c * frames + j * BLOCK_LEN
        for tile in range(tiles):
            out_ref[spot, tile * BLOCK_LEN : (tile + 1) * BLOCK_LEN, :] = total[
                start : start + BLOCK_LEN, tile * LANES : (tile + 1) * LANES
            ]
        lane = start // LANES * LANES
        out_ref[spot, tiles * BLOCK_LEN :, :] = terms[:, lane : lane + LANES]


def recur_body(n, got_ref, state_ref, state_next_ref, small_ref, gain_ref, out_ref, mine_ref, note_ref):
    b, c = lax.axis_index("b"), lax.axis_index("c")
    wide = got_ref.shape[1]
    frames = 2 * BLOCK_LEN
    summed = []
    for half in range(2):
        value = got_ref[half, 0].astype(F32)
        for spot in range(1, wide):
            value = value + got_ref[half, spot].astype(F32)
        summed.append(value)
    tiles = got_ref.shape[2] // BLOCK_LEN
    power = jnp.sum(summed[0][tiles * BLOCK_LEN :], axis=0, keepdims=True)
    row = lax.broadcasted_iota(jnp.int32, (BLOCK_LEN, LANES), 0)
    lane = lax.broadcasted_iota(jnp.int32, (BLOCK_LEN, LANES), 1)
    first = lax.rem(c * frames, LANES) + b * BLOCK_LEN
    power = jnp.sum(jnp.where(lane == row + first, power, 0.0), axis=1, keepdims=True)
    scale = lax.rsqrt(power / D + EPS)

    def tile(half, spot):
        return summed[half][spot * BLOCK_LEN : (spot + 1) * BLOCK_LEN] * scale

    alive = small_ref[n, 3 * BLOCK_LEN :]
    queries, keys, totals = [], [], []
    for half in range(2):
        queries.append(tile(half, 0) * KEY_DIM ** (-0.5))
        keys.append(tile(half, 1) * alive)
        forget = tile(half, 2) + small_ref[n, 2 * BLOCK_LEN + half : 2 * BLOCK_LEN + half + 1]
        log_gate = jnp.minimum(forget, 0.0) - jnp.log1p(jnp.exp(-jnp.abs(forget)))
        total = (log_gate / TIME_CONSTANT + small_ref[n, half * BLOCK_LEN : (half + 1) * BLOCK_LEN]) * alive
        step = 1
        while step < BLOCK_LEN:
            total = total + jnp.where(row >= step, pltpu.roll(total, step, 0), 0.0)
            step *= 2
        totals.append(total)
    value_tiles = [tile(half, spot) for half in range(2) for spot in (3, 4)]
    values = jnp.concatenate(value_tiles, 1)
    gate = jnp.concatenate([tile(half, spot) for half in range(2) for spot in (5, 6)], 1)

    carried = [queries[half] * jnp.exp(totals[half]) for half in range(2)]
    read = dot(jnp.where(b == 0, carried[0], carried[1]).astype(BF16), state_ref[n])
    read = read + dot(jnp.where(b == 0, carried[1], carried[0]).astype(BF16), state_next_ref[n])
    for spot in range(BLOCK_LEN):
        score = 0.0
        for half in range(2):
            spread = totals[half] - totals[half][spot : spot + 1]
            decay = jnp.exp(jnp.where(row >= spot, spread, 0.0))
            score = score + queries[half] * decay * keys[half][spot : spot + 1]
        score = jnp.sum(jnp.where(row >= spot, score, 0.0), axis=1, keepdims=True)
        read = read + score * values[spot : spot + 1]

    mean = jnp.mean(read * read, axis=1, keepdims=True)
    normed = read * lax.rsqrt(mean + EPS) * gain_ref[n : n + 1, :]
    gated = normed * (gate / (1.0 + jnp.exp(-gate))) * alive[:, :1]
    gated = gated.astype(BF16)
    width = out_ref.shape[2]
    for spot in range(2 * wide):
        half = spot // wide
        out_ref[spot] = gated[:, half * width : (half + 1) * width]

    weighted, kept = [], []
    for half in range(2):
        last = totals[half][BLOCK_LEN - 1 :]
        weighted.append(keys[half] * jnp.exp(last - totals[half]))
        kept.append(jnp.broadcast_to(jnp.exp(last), (BLOCK_LEN, LANES)))
    for ref, test in ((mine_ref, b == 0), (note_ref, b != 0)):
        parts = [jnp.where(test, *weighted), *value_tiles, jnp.where(test, *kept)]
        for spot, part in enumerate(parts):
            ref[spot * BLOCK_LEN : (spot + 1) * BLOCK_LEN] = part


def output_body(at, turns, left_refs, right_refs, out_ref):
    k = lax.axis_index("k")
    wide = out_ref.shape[0] // 2
    for half, left_ref, right_ref in ((k, left_refs[0], right_refs[0]), (1 - k, left_refs[1], right_refs[1])):
        width = out_ref.shape[2]
        left = left_ref[...].reshape(2 * wide * BLOCK_LEN, left_ref.shape[2])
        partial = dot(left, right_ref[:, at : at + width]).astype(BF16)
        for spot in range(2 * wide):
            j, c = divmod(spot, wide)
            out_ref[2 * c + half, j * BLOCK_LEN : (j + 1) * BLOCK_LEN, :] = partial[
                spot * BLOCK_LEN : (spot + 1) * BLOCK_LEN
            ]


def output_same_frames_body(at, left_ref, mine_ref, theirs_ref, out_ref):
    output_body(at, None, (left_ref, left_ref), (mine_ref, theirs_ref), out_ref)


def output_same_features_body(left_ref, left_next_ref, right_ref, out_ref):
    output_body(0, None, (left_ref, left_next_ref), (right_ref, right_ref), out_ref)


def add_up(ref):
    value = ref[0].astype(F32)
    for spot in range(1, ref.shape[0]):
        value = value + ref[spot].astype(F32)
    return value.astype(BF16).astype(F32)


def next_stream_body(got_ref, x_ref, out_ref):
    a, b = lax.axis_index("a"), lax.axis_index("b")
    value = (x_ref[a, b].astype(F32) + add_up(got_ref)).astype(BF16)
    for spot in range(out_ref.shape[0]):
        out_ref[spot] = value


def last_stream_body(got_ref, x_ref, next_ref, out_ref):
    a, b, k = (lax.axis_index(name) for name in "abk")
    residual = jnp.where(b == k, x_ref[a, k].astype(F32), next_ref[...].astype(F32))
    out_ref[...] = (residual + add_up(got_ref)).astype(BF16)


def memory_body(memory_ref, mine_refs, theirs_ref, out_ref):
    b = lax.axis_index("b")
    keys = memory_ref.shape[2]
    row = lax.broadcasted_iota(jnp.int32, (keys, LANES), 0)
    lane = lax.broadcasted_iota(jnp.int32, (keys, LANES), 1)
    for n in range(memory_ref.shape[0]):
        for j, note in ((b, mine_refs[n][...]), (1 - b, theirs_ref[n])):
            parts = [note[at : at + BLOCK_LEN] for at in range(0, note.shape[0], BLOCK_LEN)]
            kept = jnp.sum(jnp.where(row == lane, parts[-1][:1], 0.0), axis=1, keepdims=True)
            values = jnp.concatenate(parts[1:-1], 1).astype(BF16)
            out_ref[n, j] = kept * memory_ref[n, j] + dot(parts[0].astype(BF16), values, EACH_COLUMN)


def memory_two_body(memory_ref, mine_ref, mine_next_ref, theirs_ref, out_ref):
    memory_body(memory_ref, (mine_ref, mine_next_ref), theirs_ref, out_ref)


def local(
    stream,
    lengths,
    input_norm_gain,
    query_projection,
    key_projection,
    forget_gate_weight,
    value_projection,
    output_gate_weight,
    forget_gate_bias,
    extra_frame_decay,
    head_norm_gain,
    output_projection,
    memory,
):
    tall, wide = lax.axis_size("a"), lax.axis_size("c")
    b, k = lax.axis_index("b"), lax.axis_index("k")
    frames, features = stream.shape
    keys = query_projection.shape[2]
    values = value_projection.shape[2]
    layers = memory.shape[0]
    columns = 3 * keys + 2 * values

    sent = kernel(copies_body, ((2 * tall, frames, features), BF16), stream)
    gathered = exchange(sent, ALONG_TP).reshape(tall, 2, frames, features)

    weights = []
    for n in range(layers):
        weights += [
            query_projection[n],
            key_projection[n],
            forget_gate_weight[n],
            value_projection[n],
            output_gate_weight[n],
        ]
    mine = jnp.concatenate([*weights, output_projection[0]], 1)
    theirs = other(mine, "k")
    gain_next = other(input_norm_gain, "k")

    decay = extra_frame_decay.reshape(layers, 2, BLOCK_LEN, keys)
    bias = forget_gate_bias[:, None]
    small_next = other(jnp.concatenate([pick(decay, 1 - b, 1), bias], 1), "b")
    decay = ordered(pick(decay, b, 1), small_next[:, :BLOCK_LEN], b, 1)
    bias = ordered(bias, small_next[:, BLOCK_LEN:], b, 1)
    alive = (jnp.arange(BLOCK_LEN, dtype=jnp.int32) < pick(lengths, b, 0)).astype(F32)
    alive = jnp.broadcast_to(alive[None, :, None], (layers, BLOCK_LEN, keys))
    pad = jnp.zeros((layers, BLOCK_LEN - 2, keys), F32)
    small = jnp.concatenate([decay, bias, pad, alive], 1)
    state = pick(memory, b, 1).astype(BF16)
    state_next = other(pick(memory, 1 - b, 1).astype(BF16), "b")

    gathered, theirs, gain_next, small, state, state_next = lax.optimization_barrier(
        (gathered, theirs, gain_next, small, state, state_next)
    )
    x_own = pick(gathered, k, 1)
    x_other = other(pick(gathered, 1 - k, 1), "k")
    x = jnp.where(k == 0, jnp.stack([x_own, x_other], 1), jnp.stack([x_other, x_own], 1))

    mines, notes = [], []
    for n in range(layers):
        rows = columns // LANES * BLOCK_LEN + 8
        sent = kernel(
            functools.partial(project_body, n),
            ((2 * wide, rows, LANES), BF16),
            x,
            mine,
            theirs,
            input_norm_gain,
            gain_next,
        )
        got = exchange(sent, ALONG_X).reshape(2, wide, rows, LANES)
        note_shape = (6 * BLOCK_LEN, LANES)
        sent, own_note, note = kernel(
            functools.partial(recur_body, n),
            [((2 * wide, BLOCK_LEN, values), BF16), (note_shape, F32), (note_shape, F32)],
            got,
            state,
            state_next,
            small,
            head_norm_gain,
        )
        mines.append(own_note)
        notes.append(note)
        got = exchange(sent, ALONG_X)
        if n + 1 < layers:
            sent = kernel(
                functools.partial(output_same_frames_body, layers * columns),
                ((2 * tall, frames, features), BF16),
                got,
                mine,
                theirs,
            )
            sent = kernel(next_stream_body, ((2 * tall, frames, features), BF16), exchange(sent, ALONG_TP), x)
            x = exchange(sent, ALONG_TP).reshape(tall, 2, frames, features)
        else:
            here = pick(pick(x, lax.axis_index("a"), 0), 1 - k, 0).reshape(2, BLOCK_LEN, features)
            theirs_got = other(jnp.concatenate([got, here], 0), "k")
            sent = kernel(
                output_same_features_body,
                ((2 * tall, frames, features), BF16),
                got,
                theirs_got[: 2 * wide],
                output_projection[n],
            )
            notes, sent = lax.optimization_barrier((notes, sent))
            theirs_note = other(jnp.stack(notes), "b")
            current = kernel(
                last_stream_body,
                (stream.shape, BF16),
                exchange(sent, ALONG_TP),
                x,
                theirs_got[2 * wide :].reshape(frames, features),
            )
            fresh = kernel(memory_two_body, (memory.shape, F32), memory, *mines, theirs_note)
    return current, fresh


def solution(mesh):
    grp, tp, dp = (mesh.shape[name] for name in ("grp", "tp", "dp"))
    fine = Mesh(mesh.devices.reshape(grp, tp // 2, 2, dp // 2, 2), ("grp", "a", "b", "c", "k"))
    tp, dp = ("a", "b"), ("c", "k")
    group_tp, group_dp = ("grp", *tp), ("grp", *dp)
    placed = (
        P(group_tp, dp),
        P(group_dp),
        P(None, dp),
        P(None, dp, tp),
        P(None, dp, tp),
        P(None, dp, tp),
        P(None, dp, tp),
        P(None, dp, tp),
        P(None, tp),
        P(None, group_dp, tp),
        P(),
        P(None, tp, dp),
        P(None, group_dp, tp, None),
    )
    return jax.shard_map(
        local,
        mesh=fine,
        in_specs=placed,
        out_specs=(P(group_tp, dp), P(None, group_dp, tp, None)),
        check_vma=False,
    )
```

time: 231 us -> 248 us (1.074)
  blocking collectives: 0 us -> 107 us
  waiting for transfers between devices: 87.6 us -> 28.9 us
  starting transfers between devices: 122 us -> 74 us
  Pallas kernels: 0 us -> 22.5 us
  matrix products: 3.77 us -> 0 us
    all_to_all x0 -> x5, blocking collectives: none -> 107 us  [exchange(): return lax.all_to_all(array, axes, 0, 0, tiled=True)]
    all_to_all x8 -> x3, waiting for transfers between devices: 84.9 us -> 7.67 us  [exchange(): return lax.all_to_all(array, axes, 0, 0, tiled=True)]
    all_to_all x8 -> x3, starting transfers between devices: 91.8 us -> 56.3 us  [exchange(): return lax.all_to_all(array, axes, 0, 0, tiled=True)]
    pallas_call x0 -> x10, Pallas kernels: none -> 22.5 us  [kernel(): pl.pallas_call(body, out_shape=jax.tree.map(lambda out: jax.ShapeDtypeStr...]
    ppermute x12 -> x7, waiting for transfers between devices: 2.63 us -> 21.3 us  [other(): return lax.ppermute(array, axis, [(0, 1), (1, 0)])]
    ppermute x12 -> x7, starting transfers between devices: 29.9 us -> 17.7 us  [other(): return lax.ppermute(array, axis, [(0, 1), (1, 0)])]
    unnamed x30 -> x52, local copies, waits for them, and re-layouts: 1.12 us -> 6.45 us
    dot_general x16 -> x0, matrix products: 3.77 us -> none  [the longest x2 0.97 us: local(): jnp.dot(scaled, weights[n], preferred_element_type=f32).astype(bf16)]
  transfers between devices with their start and end apart: 20 -> 10, of which waited for: 10 -> 6; matrix products, arithmetic and copies ran while one was open for 4% -> 2% of each run, Pallas kernels for 0% -> 2%
where the time goes in v2:
time: 248 us; the launch traced here: 246 us
  blocking collectives  107 us (43%)
  starting transfers between devices  74 us (30%)
  waiting for transfers between devices  28.9 us (12%)
  Pallas kernels  22.5 us (9%)
  local copies, waits for them, and re-layouts  10.8 us (4%)
    all_to_all x5, blocking collectives, exchange(): return lax.all_to_all(array, axes, 0, 0, tiled=True)  107 us
    all_to_all x3, starting transfers between devices, exchange(): return lax.all_to_all(array, axes, 0, 0, tiled=True)  56.3 us
    pallas_call x10, Pallas kernels, kernel(): pl.pallas_call(body, out_shape=jax.tree.map(lambda out: jax.ShapeDtypeStr...  22.5 us
    ppermute x7, waiting for transfers between devices, other(): return lax.ppermute(array, axis, [(0, 1), (1, 0)])  21.3 us
    ppermute x7, starting transfers between devices, other(): return lax.ppermute(array, axis, [(0, 1), (1, 0)])  17.7 us
    all_to_all x3, waiting for transfers between devices, exchange(): return lax.all_to_all(array, axes, 0, 0, tiled=True)  7.67 us
    unnamed x52, local copies, waits for them, and re-layouts  6.45 us
  transfers between devices with their start and end apart: 10, of which 6 were waited for; matrix products, arithmetic and copies ran while one was open for 2% of the time, Pallas kernels for 2%

profile of v2, /device:TPU:80, one launch (start us, length us, event | category | flops | bytes accessed | tf_op | source)
XLA Modules:
  0.0 246.3 jit_solution(7699514733901192556)
XLA Ops:
  0.6 0.9 bitcast_dynamic-update-slice_fusion.10
  1.5 0.9 bitcast_dynamic-update-slice_fusion.9
  4.5 2.1 collective-permute-start
  6.6 1.5 shard_map.140
  8.1 43.8 %all-to-all-start = ((bf16[16,32,256]{2,1,0:T(8,128)(2,1)}), bf16[16,32,256]{2,1,0:T(8,128)(2,1)S(1)}, u32[]{:S(2)}, u32[]{:S(2)}) async-start(bf16[16,32,256]{2,1,0:T(8,128)(2,1)} %shard_map.140), calls=%async_computation | async-start | bytes 524288 | tf_op jit(solution)/shard_map/all_to_all | solution.py:24
  52.6 3.8 %collective-permute-start.2 = (f32[2,17,128]{2,1,0:T(8,128)S(1)}, f32[2,17,128]{2,1,0:T(8,128)S(1)}, u32[]{:S(2)}, u32[]{:S(2)}) collective-permute-start(f32[2,17,128]{2,1,0:T(8,128)S(1)} %pad_maximum_fusion.2), channel_id=1, source_target_pairs={{0,16},{16,0},{1,17},{17,1},{2,18},{18,2},{3,19},{19,3},{4,20},{20... | collective-permute-start | bytes 52232 | tf_op jit(solution)/shard_map/ppermute | solution.py:33
  57.3 2.4 collective-permute-start.3
  59.7 2.0 collective-permute-start.1
  63.1 3.7 %collective-permute-done.2 = f32[2,17,128]{2,1,0:T(8,128)S(1)} collective-permute-done((f32[2,17,128]{2,1,0:T(8,128)S(1)}, f32[2,17,128]{2,1,0:T(8,128)S(1)}, u32[]{:S(2)}, u32[]{:S(2)}) %collective-permute-start.2) | collective-permute-done | bytes 17440 | tf_op jit(solution)/shard_map/ppermute | solution.py:33
  67.5 4.5 %collective-permute-done.3.state_next_ref = bf16[2,128,512]{2,1,0:T(8,128)(2,1)S(1)} collective-permute-done((bf16[2,128,512]{2,1,0:T(8,128)(2,1)}, bf16[2,128,512]{2,1,0:T(8,128)(2,1)S(1)}, u32[]{:S(2)}, u32[]{:S(2)}) %collective-permute-start.3) | collective-permute-done | bytes 262176 | tf_op jit(solution)/shard_map/ppermute | solution.py:33
  72.1 2.0 collective-permute-start.4
  74.1 1.3 collective-permute-done.4
  76.1 3.0 %shard_map.141 = bf16[16,120,128]{2,1,0:T(8,128)(2,1)} custom-call(bf16[8,2,32,256]{3,2,1,0:T(8,128)(2,1)} %maximum_select_fusion.x_ref, bf16[256,2048]{1,0:T(8,128)(2,1)} %copy-done, bf16[256,2048]{1,0:T(8,128)(2,1)} %copy-done.1, f32[2,256]{1,0:T(2,128)} %gain_ref.6, f32[2,256]{1,0:T(2,128)} %copy-done.18), custom_call_target="tpu_custom_call" | custom-call | tf_op jit(solution)/shard_map/pallas_call | solution.py:58
  79.1 22.8 %all_to_all.40 = bf16[16,120,128]{2,1,0:T(8,128)(2,1)} all-to-all(bf16[16,120,128]{2,1,0:T(8,128)(2,1)} %shard_map.141), channel_id=1, replica_groups=mesh['grp'=2,'a'=8,'b'=2,'c'=8,'k'=2] {'b','c'}, dimensions={0} | all-to-all | bytes 983040 | tf_op jit(solution)/shard_map/all_to_all | solution.py:24
  101.9 2.3 shard_map.142
  104.2 14.2 %all_to_all.41.left_ref = bf16[16,16,256]{2,1,0:T(8,128)(2,1)} all-to-all(bf16[16,16,256]{2,1,0:T(8,128)(2,1)} %get-tuple-element.24), channel_id=1, replica_groups=mesh['grp'=2,'a'=8,'b'=2,'c'=8,'k'=2] {'b','c'}, dimensions={0} | all-to-all | bytes 262144 | tf_op jit(solution)/shard_map/all_to_all | solution.py:24
  118.4 2.5 %shard_map.143 = bf16[16,32,256]{2,1,0:T(8,128)(2,1)} custom-call(bf16[16,16,256]{2,1,0:T(8,128)(2,1)} %all_to_all.41.left_ref, bf16[256,2048]{1,0:T(8,128)(2,1)} %copy-done, bf16[256,2048]{1,0:T(8,128)(2,1)} %copy-done.1), custom_call_target="tpu_custom_call" | custom-call | tf_op jit(solution)/shard_map/pallas_call | solution.py:58
  121.0 28.3 %all_to_all.42.got_ref = bf16[16,32,256]{2,1,0:T(8,128)(2,1)} all-to-all(bf16[16,32,256]{2,1,0:T(8,128)(2,1)} %shard_map.143), channel_id=1, replica_groups=mesh['grp'=2,'a'=8,'b'=2,'c'=8,'k'=2] {'a','b'}, dimensions={0} | all-to-all | bytes 524288 | tf_op jit(solution)/shard_map/all_to_all | solution.py:24
  149.3 1.8 shard_map.144
  151.1 23.0 %all_to_all.43 = bf16[16,32,256]{2,1,0:T(8,128)(2,1)} all-to-all(bf16[16,32,256]{2,1,0:T(8,128)(2,1)} %shard_map.144), channel_id=1, replica_groups=mesh['grp'=2,'a'=8,'b'=2,'c'=8,'k'=2] {'a','b'}, dimensions={0} | all-to-all | bytes 524288 | tf_op jit(solution)/shard_map/all_to_all | solution.py:24
  174.1 3.0 %shard_map.145 = bf16[16,120,128]{2,1,0:T(8,128)(2,1)} custom-call(bf16[8,2,32,256]{3,2,1,0:T(8,128)(2,1)} %bitcast.58, bf16[256,2048]{1,0:T(8,128)(2,1)} %copy-done, bf16[256,2048]{1,0:T(8,128)(2,1)} %copy-done.1, f32[2,256]{1,0:T(2,128)} %gain_ref.6, f32[2,256]{1,0:T(2,128)} %copy-done.18), custom_call_target="tpu_custom_call" | custom-call | tf_op jit(solution)/shard_map/pallas_call | solution.py:58
  177.0 18.5 %all_to_all.44 = bf16[16,120,128]{2,1,0:T(8,128)(2,1)} all-to-all(bf16[16,120,128]{2,1,0:T(8,128)(2,1)} %shard_map.145), channel_id=1, replica_groups=mesh['grp'=2,'a'=8,'b'=2,'c'=8,'k'=2] {'b','c'}, dimensions={0} | all-to-all | bytes 983040 | tf_op jit(solution)/shard_map/all_to_all | solution.py:24
  195.6 2.3 shard_map.146
  197.8 6.1 %all-to-all-start.6 = ((bf16[16,16,256]{2,1,0:T(8,128)(2,1)}), bf16[16,16,256]{2,1,0:T(8,128)(2,1)S(1)}, u32[]{:S(2)}, u32[]{:S(2)}) async-start(bf16[16,16,256]{2,1,0:T(8,128)(2,1)} %get-tuple-element.26), calls=%async_computation.6 | async-start | bytes 262144 | tf_op jit(solution)/shard_map/all_to_all | solution.py:24
  204.7 7.7 %all-to-all-done.6.left_ref = bf16[16,16,256]{2,1,0:T(8,128)(2,1)S(1)} async-done(((bf16[16,16,256]{2,1,0:T(8,128)(2,1)}), bf16[16,16,256]{2,1,0:T(8,128)(2,1)S(1)}, u32[]{:S(2)}, u32[]{:S(2)}) %all-to-all-start.6) | async-done | bytes 131104 | tf_op jit(solution)/shard_map/all_to_all | solution.py:24
  213.0 1.9 collective-permute-start.5
  217.0 2.0 shard_map.147
  218.9 6.4 %all-to-all-start.7 = ((bf16[16,32,256]{2,1,0:T(8,128)(2,1)}), bf16[16,32,256]{2,1,0:T(8,128)(2,1)S(1)}, u32[]{:S(2)}, u32[]{:S(2)}) async-start(bf16[16,32,256]{2,1,0:T(8,128)(2,1)} %shard_map.147), calls=%async_computation.7 | async-start | bytes 524288 | tf_op jit(solution)/shard_map/all_to_all | solution.py:24
  225.3 3.7 %collective-permute-start.6 = (f32[2,96,128]{2,1,0:T(8,128)S(1)}, f32[2,96,128]{2,1,0:T(8,128)S(1)}, u32[]{:S(2)}, u32[]{:S(2)}) collective-permute-start(f32[2,96,128]{2,1,0:T(8,128)S(1)} %pad_maximum_fusion.1), channel_id=1, source_target_pairs={{0,16},{16,0},{1,17},{17,1},{2,18},{18,2},{3,19},{19,3},{4,20},{20... | collective-permute-start | bytes 294920 | tf_op jit(solution)/shard_map/ppermute | solution.py:33
  229.6 11.1 %collective-permute-done.6.theirs_ref = f32[2,96,128]{2,1,0:T(8,128)S(1)} collective-permute-done((f32[2,96,128]{2,1,0:T(8,128)S(1)}, f32[2,96,128]{2,1,0:T(8,128)S(1)}, u32[]{:S(2)}, u32[]{:S(2)}) %collective-permute-start.6) | collective-permute-done | bytes 98336 | tf_op jit(solution)/shard_map/ppermute | solution.py:33
  241.3 2.6 %shard_map.149 = f32[2,2,128,512]{3,2,1,0:T(8,128)} custom-call(f32[2,2,128,512]{3,2,1,0:T(8,128)} %memory_ref.1, f32[96,128]{1,0:T(8,128)} %get-tuple-element.28.mine_ref, f32[96,128]{1,0:T(8,128)} %get-tuple-element.29.mine_next_ref, f32[2,96,128]{2,1,0:T(8,128)} %copy-done.13), custom_call_target="tpu_custom_call" | custom-call | tf_op jit(solution)/shard_map/pallas_call | solution.py:58
  244.6 1.7 shard_map.148
  (77 shorter events, 11.8 us)
Async XLA Ops:
  0.6 2.7 %copy-start.6 = (bf16[2,256,256]{2,1,0:T(8,128)(2,1)S(1)}, bf16[2,256,256]{2,1,0:T(8,128)(2,1)}, u32[]{:S(2)}) copy-start(bf16[2,256,256]{2,1,0:T(8,128)(2,1)} %param.19) | copy-start | bytes 786436
  1.5 1.8 copy-start.7
  3.3 0.9 copy-start.10
  3.3 1.0 copy-start.11
  3.4 1.0 copy-start.12
  3.4 1.1 copy-start.8
  4.2 52.2 %copy-start.2 = (f32[2,2,128,512]{3,2,1,0:T(8,128)S(1)}, f32[2,2,128,512]{3,2,1,0:T(8,128)}, u32[]{:S(2)}) copy-start(f32[2,2,128,512]{3,2,1,0:T(8,128)} %memory_ref.1) | copy-start | bytes 3145732
  4.5 62.2 %copy-start = (bf16[256,2048]{1,0:T(8,128)(2,1)}, bf16[256,2048]{1,0:T(8,128)(2,1)S(1)}, u32[]{:S(2)}) copy-start(bf16[256,2048]{1,0:T(8,128)(2,1)S(1)} %bitcast_dynamic-update-slice_fusion.mine_ref) | copy-start | bytes 3145732
  4.5 67.5 %collective-permute-start = (bf16[256,2048]{1,0:T(8,128)(2,1)S(1)}, bf16[256,2048]{1,0:T(8,128)(2,1)S(1)}, u32[]{:S(2)}, u32[]{:S(2)}) collective-permute-start(bf16[256,2048]{1,0:T(8,128)(2,1)S(1)} %bitcast_dynamic-update-slice_fusion.mine_ref), channel_id=1, source_target_pairs={{0,1},{1,0},{2,3},{3,2},{4,5},{5,4},{6,7},{7,6},{8,9},{9,8},{10,11... | collective-permute-start | bytes 3145736 | tf_op jit(solution)/shard_map/ppermute | solution.py:33
  8.1 43.8 %copy-start.16 = (f32[2,32,128]{2,1,0:T(8,128)S(1)}, f32[2,32,128]{2,1,0:T(8,128)}, u32[]{:S(2)}) copy-start(f32[2,32,128]{2,1,0:T(8,128)} %param.22) | copy-start | bytes 98308
  8.1 64.0 %all-to-all-start = ((bf16[16,32,256]{2,1,0:T(8,128)(2,1)}), bf16[16,32,256]{2,1,0:T(8,128)(2,1)S(1)}, u32[]{:S(2)}, u32[]{:S(2)}) async-start(bf16[16,32,256]{2,1,0:T(8,128)(2,1)} %shard_map.140), calls=%async_computation | async-start | bytes 524288 | tf_op jit(solution)/shard_map/all_to_all | solution.py:24
  51.9 0.7 copy-start.19
  52.6 7.1 %copy-start.17 = (f32[2,256]{1,0:T(2,128)S(1)}, f32[2,256]{1,0:T(2,128)}, u32[]{:S(2)}) copy-start(f32[2,256]{1,0:T(2,128)} %gain_ref.6) | copy-start | bytes 6148
  52.6 14.1 %collective-permute-start.2 = (f32[2,17,128]{2,1,0:T(8,128)S(1)}, f32[2,17,128]{2,1,0:T(8,128)S(1)}, u32[]{:S(2)}, u32[]{:S(2)}) collective-permute-start(f32[2,17,128]{2,1,0:T(8,128)S(1)} %pad_maximum_fusion.2), channel_id=1, source_target_pairs={{0,16},{16,0},{1,17},{17,1},{2,18},{18,2},{3,19},{19,3},{4,20},{20... | collective-permute-start | bytes 52232 | tf_op jit(solution)/shard_map/ppermute | solution.py:33
  57.3 4.4 %copy-start.20 = (s32[2]{0:T(128)S(1)}, s32[2]{0:T(128)}, u32[]{:S(2)}) copy-start(s32[2]{0:T(128)} %param.14) | copy-start | bytes 28
  57.3 14.7 %collective-permute-start.3 = (bf16[2,128,512]{2,1,0:T(8,128)(2,1)}, bf16[2,128,512]{2,1,0:T(8,128)(2,1)S(1)}, u32[]{:S(2)}, u32[]{:S(2)}) collective-permute-start(bf16[2,128,512]{2,1,0:T(8,128)(2,1)} %get-tuple-element.32), channel_id=1, source_target_pairs={{0,16},{16,0},{1,17},{17,1},{2,18},{18,2},{3,19},{19,3},{4,20},{20... | collective-permute-start | bytes 786440 | tf_op jit(solution)/shard_map/ppermute | solution.py:33
  59.7 7.8 %collective-permute-start.1 = (f32[2,256]{1,0:T(2,128)S(1)}, f32[2,256]{1,0:T(2,128)S(1)}, u32[]{:S(2)}, u32[]{:S(2)}) collective-permute-start(f32[2,256]{1,0:T(2,128)S(1)} %copy-done.17), channel_id=1, source_target_pairs={{0,1},{1,0},{2,3},{3,2},{4,5},{5,4},{6,7},{7,6},{8,9},{9,8},{10,11... | collective-permute-start | bytes 6152 | tf_op jit(solution)/shard_map/ppermute | solution.py:33
  67.5 4.6 %copy-start.18 = (f32[2,256]{1,0:T(2,128)}, f32[2,256]{1,0:T(2,128)S(1)}, u32[]{:S(2)}) copy-start(f32[2,256]{1,0:T(2,128)S(1)} %collective-permute-done.1.gain_next_ref) | copy-start | bytes 6148
  72.0 7.0 %copy-start.5 = (bf16[2,128,512]{2,1,0:T(8,128)(2,1)}, bf16[2,128,512]{2,1,0:T(8,128)(2,1)S(1)}, u32[]{:S(2)}) copy-start(bf16[2,128,512]{2,1,0:T(8,128)(2,1)S(1)} %collective-permute-done.3.state_next_ref) | copy-start | bytes 786436
  72.0 4.1 %copy-start.1 = (bf16[256,2048]{1,0:T(8,128)(2,1)}, bf16[256,2048]{1,0:T(8,128)(2,1)S(1)}, u32[]{:S(2)}) copy-start(bf16[256,2048]{1,0:T(8,128)(2,1)S(1)} %collective-permute-done.theirs_ref) | copy-start | bytes 3145732
  72.1 3.3 %collective-permute-start.4 = (bf16[8,32,256]{2,1,0:T(8,128)(2,1)S(1)}, bf16[8,32,256]{2,1,0:T(8,128)(2,1)S(1)}, u32[]{:S(2)}, u32[]{:S(2)}) collective-permute-start(bf16[8,32,256]{2,1,0:T(8,128)(2,1)S(1)} %get-tuple-element.35), channel_id=1, source_target_pairs={{0,1},{1,0},{2,3},{3,2},{4,5},{5,4},{6,7},{7,6},{8,9},{9,8},{10,11... | collective-permute-start | bytes 393224 | tf_op jit(solution)/shard_map/ppermute | solution.py:33
  197.8 17.1 %copy-start.9 = (bf16[2,256,256]{2,1,0:T(8,128)(2,1)S(1)}, bf16[2,256,256]{2,1,0:T(8,128)(2,1)}, u32[]{:S(2)}) copy-start(bf16[2,256,256]{2,1,0:T(8,128)(2,1)} %param.24) | copy-start | bytes 786436
  197.8 14.5 %all-to-all-start.6 = ((bf16[16,16,256]{2,1,0:T(8,128)(2,1)}), bf16[16,16,256]{2,1,0:T(8,128)(2,1)S(1)}, u32[]{:S(2)}, u32[]{:S(2)}) async-start(bf16[16,16,256]{2,1,0:T(8,128)(2,1)} %get-tuple-element.26), calls=%async_computation.6 | async-start | bytes 262144 | tf_op jit(solution)/shard_map/all_to_all | solution.py:24
  212.4 0.7 copy-start.3
  213.0 3.3 %collective-permute-start.5 = (bf16[18,16,256]{2,1,0:T(8,128)(2,1)S(1)}, bf16[18,16,256]{2,1,0:T(8,128)(2,1)S(1)}, u32[]{:S(2)}, u32[]{:S(2)}) collective-permute-start(bf16[18,16,256]{2,1,0:T(8,128)(2,1)S(1)} %pad_maximum_fusion), channel_id=1, source_target_pairs={{0,1},{1,0},{2,3},{3,2},{4,5},{5,4},{6,7},{7,6},{8,9},{9,8},{10,11... | collective-permute-start | bytes 442376 | tf_op jit(solution)/shard_map/ppermute | solution.py:33
  218.9 6.4 %copy-start.14 = (f32[96,128]{1,0:T(8,128)S(1)}, f32[96,128]{1,0:T(8,128)}, u32[]{:S(2)}) copy-start(f32[96,128]{1,0:T(8,128)} %get-tuple-element.30) | copy-start | bytes 147460
  218.9 6.4 %copy-start.15 = (f32[96,128]{1,0:T(8,128)S(1)}, f32[96,128]{1,0:T(8,128)}, u32[]{:S(2)}) copy-start(f32[96,128]{1,0:T(8,128)} %get-tuple-element.31) | copy-start | bytes 147460
  218.9 25.0 %all-to-all-start.7 = ((bf16[16,32,256]{2,1,0:T(8,128)(2,1)}), bf16[16,32,256]{2,1,0:T(8,128)(2,1)S(1)}, u32[]{:S(2)}, u32[]{:S(2)}) async-start(bf16[16,32,256]{2,1,0:T(8,128)(2,1)} %shard_map.147), calls=%async_computation.7 | async-start | bytes 524288 | tf_op jit(solution)/shard_map/all_to_all | solution.py:24
  225.3 15.4 %collective-permute-start.6 = (f32[2,96,128]{2,1,0:T(8,128)S(1)}, f32[2,96,128]{2,1,0:T(8,128)S(1)}, u32[]{:S(2)}, u32[]{:S(2)}) collective-permute-start(f32[2,96,128]{2,1,0:T(8,128)S(1)} %pad_maximum_fusion.1), channel_id=1, source_target_pairs={{0,16},{16,0},{1,17},{17,1},{2,18},{18,2},{3,19},{19,3},{4,20},{20... | collective-permute-start | bytes 294920 | tf_op jit(solution)/shard_map/ppermute | solution.py:33
  240.7 0.7 copy-start.13
  243.9 0.7 copy-start.4

commit v3 on v2

--- a/solution.py
+++ b/solution.py
@@ -8,9 +8,9 @@
 from jax.sharding import Mesh
 from jax.sharding import PartitionSpec as P
 
+
 D = 4096
 KEY_DIM = 256
-VALUE_DIM = 512
 BLOCK_LEN = 16
 
 EPS = 1e-06
@@ -22,11 +22,6 @@
 
 def exchange(array, axes):
     return lax.all_to_all(array, axes, 0, 0, tiled=True)
-
-
-def to_all(array, axes):
-    length = lax.axis_size(axes)
-    return exchange(jnp.broadcast_to(array[None], (length, *array.shape)), axes)
 
 
 def other(array, axis):
@@ -44,6 +39,7 @@
 
 
 LANES = 128
+VMEM_LIMIT = 8 * 2**20
 F32, BF16 = jnp.float32, jnp.bfloat16
 EACH_ROW = (((1,), (1,)), ((), ()))
 EACH_COLUMN = (((0,), (0,)), ((), ()))
@@ -60,6 +56,7 @@
         out_shape=jax.tree.map(lambda out: jax.ShapeDtypeStruct(*out), outs, is_leaf=lambda x: isinstance(x[1], type)),
         in_specs=[vmem] * len(args),
         out_specs=jax.tree.map(lambda out: vmem, outs, is_leaf=lambda x: isinstance(x[1], type)),
+        compiler_params=pltpu.CompilerParams(vmem_limit_bytes=VMEM_LIMIT),
     )(*args)
 
 
@@ -69,7 +66,7 @@
         out_ref[spot] = value
 
 
-def project_body(n, x_ref, mine_ref, theirs_ref, gain_ref, gain_next_ref, out_ref):
+def project_body(n, first, x_ref, x_next_ref, mine_ref, theirs_ref, gain_ref, gain_next_ref, out_ref, here_ref):
     k = lax.axis_index("k")
     tall, _, frames, features = x_ref.shape
     wide = out_ref.shape[0] // 2
@@ -78,13 +75,15 @@
     ones = jnp.ones((8, features), BF16)
     total, power = 0.0, 0.0
     for half, w_ref, g_ref in ((k, mine_ref, gain_ref), (1 - k, theirs_ref, gain_next_ref)):
-        x = x_ref[:, half].reshape(tall * frames, features).astype(F32)
+        x = x_next_ref[...] if first and half is not k else x_ref[:, half]
+        x = x.reshape(tall * frames, features).astype(F32)
         scaled = (x * g_ref[n : n + 1, :]).astype(BF16)
         total = total + dot(scaled, w_ref[:, n * columns : (n + 1) * columns])
         square = x * x
         high = square.astype(BF16)
         low = (square - high.astype(F32)).astype(BF16)
         power = power + dot(ones, high, EACH_ROW) + dot(ones, low, EACH_ROW)
+    here_ref[...] = x_ref[lax.axis_index("a"), 1 - k]
     total = total.astype(BF16)
     high = power.astype(BF16).astype(F32)
     middle = (power - high).astype(BF16).astype(F32)
@@ -173,7 +172,7 @@
             ref[spot * BLOCK_LEN : (spot + 1) * BLOCK_LEN] = part
 
 
-def output_body(at, turns, left_refs, right_refs, out_ref):
+def output_body(at, left_refs, right_refs, out_ref):
     k = lax.axis_index("k")
     wide = out_ref.shape[0] // 2
     for half, left_ref, right_ref in ((k, left_refs[0], right_refs[0]), (1 - k, left_refs[1], right_refs[1])):
@@ -188,11 +187,11 @@
 
 
 def output_same_frames_body(at, left_ref, mine_ref, theirs_ref, out_ref):
-    output_body(at, None, (left_ref, left_ref), (mine_ref, theirs_ref), out_ref)
+    output_body(at, (left_ref, left_ref), (mine_ref, theirs_ref), out_ref)
 
 
 def output_same_features_body(left_ref, left_next_ref, right_ref, out_ref):
-    output_body(0, None, (left_ref, left_next_ref), (right_ref, right_ref), out_ref)
+    output_body(0, (left_ref, left_next_ref), (right_ref, right_ref), out_ref)
 
 
 def add_up(ref):
@@ -202,9 +201,10 @@
     return value.astype(BF16).astype(F32)
 
 
-def next_stream_body(got_ref, x_ref, out_ref):
-    a, b = lax.axis_index("a"), lax.axis_index("b")
-    value = (x_ref[a, b].astype(F32) + add_up(got_ref)).astype(BF16)
+def next_stream_body(got_ref, x_ref, x_next_ref, out_ref):
+    a, b, k = (lax.axis_index(name) for name in "abk")
+    residual = jnp.where(b == k, x_ref[a, k].astype(F32), x_next_ref[a].astype(F32))
+    value = (residual + add_up(got_ref)).astype(BF16)
     for spot in range(out_ref.shape[0]):
         out_ref[spot] = value
 
@@ -256,18 +256,23 @@
     columns = 3 * keys + 2 * values
 
     sent = kernel(copies_body, ((2 * tall, frames, features), BF16), stream)
+    sent, *weights_in = lax.optimization_barrier(
+        (
+            sent,
+            query_projection,
+            key_projection,
+            forget_gate_weight,
+            value_projection,
+            output_gate_weight,
+            output_projection,
+        )
+    )
     gathered = exchange(sent, ALONG_TP).reshape(tall, 2, frames, features)
 
     weights = []
     for n in range(layers):
-        weights += [
-            query_projection[n],
-            key_projection[n],
-            forget_gate_weight[n],
-            value_projection[n],
-            output_gate_weight[n],
-        ]
-    mine = jnp.concatenate([*weights, output_projection[0]], 1)
+        weights += [weight[n] for weight in weights_in[:-1]]
+    mine = jnp.concatenate([*weights, weights_in[-1][0]], 1)
     theirs = other(mine, "k")
     gain_next = other(input_norm_gain, "k")
 
@@ -286,17 +291,16 @@
     gathered, theirs, gain_next, small, state, state_next = lax.optimization_barrier(
         (gathered, theirs, gain_next, small, state, state_next)
     )
-    x_own = pick(gathered, k, 1)
-    x_other = other(pick(gathered, 1 - k, 1), "k")
-    x = jnp.where(k == 0, jnp.stack([x_own, x_other], 1), jnp.stack([x_other, x_own], 1))
+    x, x_next = gathered, other(pick(gathered, 1 - k, 1), "k")
 
     mines, notes = [], []
     for n in range(layers):
         rows = columns // LANES * BLOCK_LEN + 8
-        sent = kernel(
-            functools.partial(project_body, n),
-            ((2 * wide, rows, LANES), BF16),
+        sent, here = kernel(
+            functools.partial(project_body, n, n == 0),
+            [((2 * wide, rows, LANES), BF16), ((frames, features), BF16)],
             x,
+            x_next,
             mine,
             theirs,
             input_norm_gain,
@@ -324,11 +328,10 @@
                 mine,
                 theirs,
             )
-            sent = kernel(next_stream_body, ((2 * tall, frames, features), BF16), exchange(sent, ALONG_TP), x)
+            sent = kernel(next_stream_body, ((2 * tall, frames, features), BF16), exchange(sent, ALONG_TP), x, x_next)
             x = exchange(sent, ALONG_TP).reshape(tall, 2, frames, features)
         else:
-            here = pick(pick(x, lax.axis_index("a"), 0), 1 - k, 0).reshape(2, BLOCK_LEN, features)
-            theirs_got = other(jnp.concatenate([got, here], 0), "k")
+            theirs_got = other(jnp.concatenate([got, here.reshape(2, BLOCK_LEN, features)], 0), "k")
             sent = kernel(
                 output_same_features_body,
                 ((2 * tall, frames, features), BF16),
@@ -369,6 +372,7 @@
         P(None, tp, dp),
         P(None, group_dp, tp, None),
     )
+
     return jax.shard_map(
         local,
         mesh=fine,

time: 248 us -> 228 us (0.919)
  Pallas kernels: 22.5 us -> 7.45 us
  blocking collectives: 107 us -> 120 us
  starting transfers between devices: 74 us -> 67.5 us
  local copies, waits for them, and re-layouts: 10.8 us -> 5.96 us
  waiting for transfers between devices: 28.9 us -> 24.8 us
    pallas_call x10, Pallas kernels: 22.5 us -> 7.45 us  [kernel(): pl.pallas_call(body, out_shape=jax.tree.map(lambda out: jax.ShapeDtypeStr...]
    all_to_all x5 -> x6, blocking collectives: 107 us -> 120 us  [exchange(): return lax.all_to_all(array, axes, 0, 0, tiled=True)]
    all_to_all x3 -> x2, starting transfers between devices: 56.3 us -> 49.9 us  [exchange(): return lax.all_to_all(array, axes, 0, 0, tiled=True)]
    all_to_all x3 -> x2, waiting for transfers between devices: 7.67 us -> 1.48 us  [exchange(): return lax.all_to_all(array, axes, 0, 0, tiled=True)]
    unnamed x52 -> x46, local copies, waits for them, and re-layouts: 6.45 us -> 4.29 us
  transfers between devices with their start and end apart: 10 -> 9, of which waited for: 6 -> 6; matrix products, arithmetic and copies ran while one was open for 2% -> 1% of each run, Pallas kernels for 2% -> 1%
where the time goes in v3:
time: 228 us; the launch traced here: 227 us
  blocking collectives  120 us (53%)
  starting transfers between devices  67.5 us (30%)
  waiting for transfers between devices  24.8 us (11%)
  Pallas kernels  7.45 us (3%)
  local copies, waits for them, and re-layouts  5.96 us (3%)
    all_to_all x6, blocking collectives, exchange(): return lax.all_to_all(array, axes, 0, 0, tiled=True)  120 us
    all_to_all x2, starting transfers between devices, exchange(): return lax.all_to_all(array, axes, 0, 0, tiled=True)  49.9 us
    ppermute x7, waiting for transfers between devices, other(): return lax.ppermute(array, axis, [(0, 1), (1, 0)])  23.3 us
    ppermute x7, starting transfers between devices, other(): return lax.ppermute(array, axis, [(0, 1), (1, 0)])  17.6 us
    pallas_call x10, Pallas kernels, kernel(): pl.pallas_call(body, out_shape=jax.tree.map(lambda out: jax.ShapeDtypeStr...  7.45 us
  transfers between devices with their start and end apart: 9, of which 6 were waited for; matrix products, arithmetic and copies ran while one was open for 1% of the time, Pallas kernels for 1%

profile of v3, /device:TPU:80, one launch (start us, length us, event | category | flops | bytes accessed | tf_op | source)
XLA Modules:
  0.0 227.3 jit_solution(10033542379187574166)
XLA Ops:
  0.6 0.7 copy-done.6
  1.4 0.9 copy-done.12
  3.5 0.8 copy-done.10
  4.3 2.0 collective-permute-start
  6.3 43.7 %all-to-all-start = ((bf16[16,32,256]{2,1,0:T(8,128)(2,1)}), bf16[16,32,256]{2,1,0:T(8,128)(2,1)S(1)}, u32[]{:S(2)}, u32[]{:S(2)}) async-start(bf16[16,32,256]{2,1,0:T(8,128)(2,1)} %copy-done.2), calls=%async_computation | async-start | bytes 524288 | tf_op jit(solution)/shard_map/all_to_all | solution.py:24
  50.0 0.7 copy-done.16
  50.7 3.8 %collective-permute-start.2 = (f32[2,17,128]{2,1,0:T(8,128)S(1)}, f32[2,17,128]{2,1,0:T(8,128)S(1)}, u32[]{:S(2)}, u32[]{:S(2)}) collective-permute-start(f32[2,17,128]{2,1,0:T(8,128)S(1)} %pad_maximum_fusion.2), channel_id=1, source_target_pairs={{0,16},{16,0},{1,17},{17,1},{2,18},{18,2},{3,19},{19,3},{4,20},{20... | collective-permute-start | bytes 52232 | tf_op jit(solution)/shard_map/ppermute | solution.py:28
  54.5 0.9 fusion.1
  55.4 2.4 %collective-permute-start.3 = (bf16[2,128,512]{2,1,0:T(8,128)(2,1)}, bf16[2,128,512]{2,1,0:T(8,128)(2,1)}, u32[]{:S(2)}, u32[]{:S(2)}) collective-permute-start(bf16[2,128,512]{2,1,0:T(8,128)(2,1)} %get-tuple-element.52), channel_id=1, source_target_pairs={{0,16},{16,0},{1,17},{17,1},{2,18},{18,2},{3,19},{19,3},{4,20},{20... | collective-permute-start | bytes 786440 | tf_op jit(solution)/shard_map/ppermute | solution.py:28
  57.8 2.0 collective-permute-start.1
  61.1 3.7 %collective-permute-done.2 = f32[2,17,128]{2,1,0:T(8,128)S(1)} collective-permute-done((f32[2,17,128]{2,1,0:T(8,128)S(1)}, f32[2,17,128]{2,1,0:T(8,128)S(1)}, u32[]{:S(2)}, u32[]{:S(2)}) %collective-permute-start.2) | collective-permute-done | bytes 17440 | tf_op jit(solution)/shard_map/ppermute | solution.py:28
  64.9 5.3 %collective-permute-done.3.state_next_ref = bf16[2,128,512]{2,1,0:T(8,128)(2,1)} collective-permute-done((bf16[2,128,512]{2,1,0:T(8,128)(2,1)}, bf16[2,128,512]{2,1,0:T(8,128)(2,1)}, u32[]{:S(2)}, u32[]{:S(2)}) %collective-permute-start.3) | collective-permute-done | bytes 262176 | tf_op jit(solution)/shard_map/ppermute | solution.py:28
  70.2 2.0 collective-permute-start.4
  72.2 1.3 collective-permute-done.4.x_next_ref
  73.5 1.1 shard_map.141
  74.6 22.6 %all_to_all.40 = bf16[16,120,128]{2,1,0:T(8,128)(2,1)S(1)} all-to-all(bf16[16,120,128]{2,1,0:T(8,128)(2,1)S(1)} %get-tuple-element.37), channel_id=1, replica_groups=mesh['grp'=2,'a'=8,'b'=2,'c'=8,'k'=2] {'b','c'}, dimensions={0} | all-to-all | bytes 983040 | tf_op jit(solution)/shard_map/all_to_all | solution.py:24
  97.2 1.3 shard_map.142
  98.5 13.9 %all_to_all.41.left_ref = bf16[16,16,256]{2,1,0:T(8,128)(2,1)S(1)} all-to-all(bf16[16,16,256]{2,1,0:T(8,128)(2,1)S(1)} %get-tuple-element.42), channel_id=1, replica_groups=mesh['grp'=2,'a'=8,'b'=2,'c'=8,'k'=2] {'b','c'}, dimensions={0} | all-to-all | bytes 262144 | tf_op jit(solution)/shard_map/all_to_all | solution.py:24
  112.7 28.1 %all_to_all.42.got_ref = bf16[16,32,256]{2,1,0:T(8,128)(2,1)S(1)} all-to-all(bf16[16,32,256]{2,1,0:T(8,128)(2,1)S(1)} %shard_map.143), channel_id=1, replica_groups=mesh['grp'=2,'a'=8,'b'=2,'c'=8,'k'=2] {'a','b'}, dimensions={0} | all-to-all | bytes 524288 | tf_op jit(solution)/shard_map/all_to_all | solution.py:24
  140.8 22.7 %all_to_all.43 = bf16[16,32,256]{2,1,0:T(8,128)(2,1)S(1)} all-to-all(bf16[16,32,256]{2,1,0:T(8,128)(2,1)S(1)} %shard_map.144), channel_id=1, replica_groups=mesh['grp'=2,'a'=8,'b'=2,'c'=8,'k'=2] {'a','b'}, dimensions={0} | all-to-all | bytes 524288 | tf_op jit(solution)/shard_map/all_to_all | solution.py:24
  164.1 18.2 %all_to_all.44 = bf16[16,120,128]{2,1,0:T(8,128)(2,1)S(1)} all-to-all(bf16[16,120,128]{2,1,0:T(8,128)(2,1)S(1)} %get-tuple-element.43), channel_id=1, replica_groups=mesh['grp'=2,'a'=8,'b'=2,'c'=8,'k'=2] {'b','c'}, dimensions={0} | all-to-all | bytes 983040 | tf_op jit(solution)/shard_map/all_to_all | solution.py:24
  182.3 1.3 shard_map.146
  183.6 14.3 %all_to_all.45.left_ref = bf16[16,16,256]{2,1,0:T(8,128)(2,1)S(1)} all-to-all(bf16[16,16,256]{2,1,0:T(8,128)(2,1)S(1)} %get-tuple-element.45), channel_id=1, replica_groups=mesh['grp'=2,'a'=8,'b'=2,'c'=8,'k'=2] {'b','c'}, dimensions={0} | all-to-all | bytes 262144 | tf_op jit(solution)/shard_map/all_to_all | solution.py:24
  198.0 2.0 collective-permute-start.5
  200.0 1.3 collective-permute-done.5
  201.3 0.9 shard_map.147
  202.2 6.2 %all-to-all-start.7 = ((bf16[16,32,256]{2,1,0:T(8,128)(2,1)}), bf16[16,32,256]{2,1,0:T(8,128)(2,1)S(1)}, u32[]{:S(2)}, u32[]{:S(2)}) async-start(bf16[16,32,256]{2,1,0:T(8,128)(2,1)} %shard_map.147), calls=%async_computation.7 | async-start | bytes 524288 | tf_op jit(solution)/shard_map/all_to_all | solution.py:24
  208.5 3.7 %collective-permute-start.6 = (f32[2,96,128]{2,1,0:T(8,128)S(1)}, f32[2,96,128]{2,1,0:T(8,128)S(1)}, u32[]{:S(2)}, u32[]{:S(2)}) collective-permute-start(f32[2,96,128]{2,1,0:T(8,128)S(1)} %pad_maximum_fusion.1), channel_id=1, source_target_pairs={{0,16},{16,0},{1,17},{17,1},{2,18},{18,2},{3,19},{19,3},{4,20},{20... | collective-permute-start | bytes 294920 | tf_op jit(solution)/shard_map/ppermute | solution.py:28
  212.2 11.7 %collective-permute-done.6.theirs_ref = f32[2,96,128]{2,1,0:T(8,128)S(1)} collective-permute-done((f32[2,96,128]{2,1,0:T(8,128)S(1)}, f32[2,96,128]{2,1,0:T(8,128)S(1)}, u32[]{:S(2)}, u32[]{:S(2)}) %collective-permute-start.6) | collective-permute-done | bytes 98336 | tf_op jit(solution)/shard_map/ppermute | solution.py:28
  223.8 1.3 shard_map.149
  225.2 1.5 all-to-all-done.7.got_ref
  226.6 0.6 shard_map.148
  (68 shorter events, 3.7 us)
Async XLA Ops:
  0.6 0.7 copy-start.6
  1.3 0.9 copy-start.12
  1.4 1.0 copy-start.13
  1.4 1.0 copy-start.14
  2.3 0.7 copy-start.2
  2.3 1.1 copy-start.8
  2.3 1.1 copy-start.9
  3.3 1.0 copy-start.10
  3.4 51.1 %copy-start = (f32[2,2,128,512]{3,2,1,0:T(8,128)S(1)}, f32[2,2,128,512]{3,2,1,0:T(8,128)}, u32[]{:S(2)}) copy-start(f32[2,2,128,512]{3,2,1,0:T(8,128)} %memory_ref.1) | copy-start | bytes 3145732
  4.3 65.9 %collective-permute-start = (bf16[256,2048]{1,0:T(8,128)(2,1)S(1)}, bf16[256,2048]{1,0:T(8,128)(2,1)S(1)}, u32[]{:S(2)}, u32[]{:S(2)}) collective-permute-start(bf16[256,2048]{1,0:T(8,128)(2,1)S(1)} %bitcast_dynamic-update-slice_fusion.mine_ref), channel_id=1, source_target_pairs={{0,1},{1,0},{2,3},{3,2},{4,5},{5,4},{6,7},{7,6},{8,9},{9,8},{10,11... | collective-permute-start | bytes 3145736 | tf_op jit(solution)/shard_map/ppermute | solution.py:28
  6.3 43.7 %copy-start.15 = (f32[2,32,128]{2,1,0:T(8,128)S(1)}, f32[2,32,128]{2,1,0:T(8,128)}, u32[]{:S(2)}) copy-start(f32[2,32,128]{2,1,0:T(8,128)} %param.22) | copy-start | bytes 98308
  6.3 63.9 %all-to-all-start = ((bf16[16,32,256]{2,1,0:T(8,128)(2,1)}), bf16[16,32,256]{2,1,0:T(8,128)(2,1)S(1)}, u32[]{:S(2)}, u32[]{:S(2)}) async-start(bf16[16,32,256]{2,1,0:T(8,128)(2,1)} %copy-done.2), calls=%async_computation | async-start | bytes 524288 | tf_op jit(solution)/shard_map/all_to_all | solution.py:24
  50.0 0.7 copy-start.16
  50.7 7.0 %copy-start.7 = (f32[2,256]{1,0:T(2,128)S(1)}, f32[2,256]{1,0:T(2,128)}, u32[]{:S(2)}) copy-start(f32[2,256]{1,0:T(2,128)} %gain_ref.6) | copy-start | bytes 6148
  50.7 14.1 %collective-permute-start.2 = (f32[2,17,128]{2,1,0:T(8,128)S(1)}, f32[2,17,128]{2,1,0:T(8,128)S(1)}, u32[]{:S(2)}, u32[]{:S(2)}) collective-permute-start(f32[2,17,128]{2,1,0:T(8,128)S(1)} %pad_maximum_fusion.2), channel_id=1, source_target_pairs={{0,16},{16,0},{1,17},{17,1},{2,18},{18,2},{3,19},{19,3},{4,20},{20... | collective-permute-start | bytes 52232 | tf_op jit(solution)/shard_map/ppermute | solution.py:28
  55.4 4.4 %copy-start.17 = (s32[2]{0:T(128)S(1)}, s32[2]{0:T(128)}, u32[]{:S(2)}) copy-start(s32[2]{0:T(128)} %param.14) | copy-start | bytes 28
  55.4 14.9 %collective-permute-start.3 = (bf16[2,128,512]{2,1,0:T(8,128)(2,1)}, bf16[2,128,512]{2,1,0:T(8,128)(2,1)}, u32[]{:S(2)}, u32[]{:S(2)}) collective-permute-start(bf16[2,128,512]{2,1,0:T(8,128)(2,1)} %get-tuple-element.52), channel_id=1, source_target_pairs={{0,16},{16,0},{1,17},{17,1},{2,18},{18,2},{3,19},{19,3},{4,20},{20... | collective-permute-start | bytes 786440 | tf_op jit(solution)/shard_map/ppermute | solution.py:28
  57.8 7.2 %collective-permute-start.1 = (f32[2,256]{1,0:T(2,128)S(1)}, f32[2,256]{1,0:T(2,128)S(1)}, u32[]{:S(2)}, u32[]{:S(2)}) collective-permute-start(f32[2,256]{1,0:T(2,128)S(1)} %copy-done.7), channel_id=1, source_target_pairs={{0,1},{1,0},{2,3},{3,2},{4,5},{5,4},{6,7},{7,6},{8,9},{9,8},{10,11... | collective-permute-start | bytes 6152 | tf_op jit(solution)/shard_map/ppermute | solution.py:28
  70.2 3.3 %collective-permute-start.4 = (bf16[8,32,256]{2,1,0:T(8,128)(2,1)S(1)}, bf16[8,32,256]{2,1,0:T(8,128)(2,1)S(1)}, u32[]{:S(2)}, u32[]{:S(2)}) collective-permute-start(bf16[8,32,256]{2,1,0:T(8,128)(2,1)S(1)} %dynamic-slice_bitcast_fusion), channel_id=1, source_target_pairs={{0,1},{1,0},{2,3},{3,2},{4,5},{5,4},{6,7},{7,6},{8,9},{9,8},{10,11... | collective-permute-start | bytes 393224 | tf_op jit(solution)/shard_map/ppermute | solution.py:28
  74.6 22.6 %copy-start.1 = (bf16[2,128,512]{2,1,0:T(8,128)(2,1)S(1)}, bf16[2,128,512]{2,1,0:T(8,128)(2,1)}, u32[]{:S(2)}) copy-start(bf16[2,128,512]{2,1,0:T(8,128)(2,1)} %get-tuple-element.38.state_ref) | copy-start | bytes 786436
  74.6 22.6 %copy-start.5 = (f32[2,512]{1,0:T(2,128)S(1)}, f32[2,512]{1,0:T(2,128)}, u32[]{:S(2)}) copy-start(f32[2,512]{1,0:T(2,128)} %gain_ref.7) | copy-start | bytes 12292
  98.5 13.9 %copy-start.3 = (f32[96,128]{1,0:T(8,128)}, f32[96,128]{1,0:T(8,128)S(1)}, u32[]{:S(2)}) copy-start(f32[96,128]{1,0:T(8,128)S(1)} %get-tuple-element.48.mine_ref) | copy-start | bytes 147460
  183.6 16.3 %copy-start.11 = (bf16[2,256,256]{2,1,0:T(8,128)(2,1)S(1)}, bf16[2,256,256]{2,1,0:T(8,128)(2,1)}, u32[]{:S(2)}) copy-start(bf16[2,256,256]{2,1,0:T(8,128)(2,1)} %param.24) | copy-start | bytes 786436
  198.0 3.3 %collective-permute-start.5 = (bf16[18,16,256]{2,1,0:T(8,128)(2,1)S(1)}, bf16[18,16,256]{2,1,0:T(8,128)(2,1)S(1)}, u32[]{:S(2)}, u32[]{:S(2)}) collective-permute-start(bf16[18,16,256]{2,1,0:T(8,128)(2,1)S(1)} %pad_maximum_fusion), channel_id=1, source_target_pairs={{0,1},{1,0},{2,3},{3,2},{4,5},{5,4},{6,7},{7,6},{8,9},{9,8},{10,11... | collective-permute-start | bytes 442376 | tf_op jit(solution)/shard_map/ppermute | solution.py:28
  202.2 24.4 %all-to-all-start.7 = ((bf16[16,32,256]{2,1,0:T(8,128)(2,1)}), bf16[16,32,256]{2,1,0:T(8,128)(2,1)S(1)}, u32[]{:S(2)}, u32[]{:S(2)}) async-start(bf16[16,32,256]{2,1,0:T(8,128)(2,1)} %shard_map.147), calls=%async_computation.7 | async-start | bytes 524288 | tf_op jit(solution)/shard_map/all_to_all | solution.py:24
  208.5 15.4 %copy-start.4 = (f32[96,128]{1,0:T(8,128)S(1)}, f32[96,128]{1,0:T(8,128)}, u32[]{:S(2)}) copy-start(f32[96,128]{1,0:T(8,128)} %copy-done.3) | copy-start | bytes 147460
  208.5 15.4 %collective-permute-start.6 = (f32[2,96,128]{2,1,0:T(8,128)S(1)}, f32[2,96,128]{2,1,0:T(8,128)S(1)}, u32[]{:S(2)}, u32[]{:S(2)}) collective-permute-start(f32[2,96,128]{2,1,0:T(8,128)S(1)} %pad_maximum_fusion.1), channel_id=1, source_target_pairs={{0,16},{16,0},{1,17},{17,1},{2,18},{18,2},{3,19},{19,3},{4,20},{20... | collective-permute-start | bytes 294920 | tf_op jit(solution)/shard_map/ppermute | solution.py:28

commit v4 on v3

--- a/solution.py
+++ b/solution.py
@@ -11,12 +11,15 @@
 
 D = 4096
 KEY_DIM = 256
+VALUE_DIM = 512
 BLOCK_LEN = 16
 
 EPS = 1e-06
 TIME_CONSTANT = 16.0
 
-ALONG_TP = ("a", "b")
+ALONG_TP = ("far", "near", "b")
+QUAD = ("near", "b")
+HEAD = ("far", "near")
 ALONG_X = ("b", "c")
 
 
@@ -26,16 +29,6 @@
 
 def other(array, axis):
     return lax.ppermute(array, axis, [(0, 1), (1, 0)])
-
-
-def pick(array, index, dim):
-    return lax.dynamic_index_in_dim(array, index, dim, keepdims=False)
-
-
-def ordered(own, theirs, spot, dim):
-    return jnp.where(
-        spot == 0, jnp.concatenate([own, theirs], dim), jnp.concatenate([theirs, own], dim)
-    )
 
 
 LANES = 128
@@ -51,22 +44,48 @@
 
 def kernel(body, outs, *args):
     vmem = pl.BlockSpec(memory_space=pltpu.VMEM)
+    several = isinstance(outs, list)
+    shapes = [jax.ShapeDtypeStruct(*out) for out in (outs if several else [outs])]
     return pl.pallas_call(
         body,
-        out_shape=jax.tree.map(lambda out: jax.ShapeDtypeStruct(*out), outs, is_leaf=lambda x: isinstance(x[1], type)),
+        out_shape=shapes if several else shapes[0],
         in_specs=[vmem] * len(args),
-        out_specs=jax.tree.map(lambda out: vmem, outs, is_leaf=lambda x: isinstance(x[1], type)),
+        out_specs=[vmem] * len(shapes) if several else vmem,
         compiler_params=pltpu.CompilerParams(vmem_limit_bytes=VMEM_LIMIT),
     )(*args)
 
 
-def copies_body(in_ref, out_ref):
-    value = in_ref[...]
+def three_terms(value):
+    high = value.astype(BF16).astype(F32)
+    middle = (value - high).astype(BF16).astype(F32)
+    return high, middle, value - high - middle
+
+
+def head_index():
+    return lax.axis_index("far") * lax.axis_size("near") + lax.axis_index("near")
+
+
+def write_copies(out_ref, value):
     for spot in range(out_ref.shape[0]):
         out_ref[spot] = value
 
 
-def project_body(n, first, x_ref, x_next_ref, mine_ref, theirs_ref, gain_ref, gain_next_ref, out_ref, here_ref):
+def copies_body(in_ref, out_ref):
+    write_copies(out_ref, in_ref[...])
+
+
+def pack_state_body(memory_ref, decay_ref, bias_ref, out_ref):
+    j = 1 - lax.axis_index("b")
+    keys = memory_ref.shape[2]
+    for n in range(memory_ref.shape[0]):
+        out_ref[n, :keys] = memory_ref[n, j].astype(BF16)
+        bias = jnp.broadcast_to(bias_ref[n : n + 1, :], (BLOCK_LEN, keys))
+        for at, value in ((keys, decay_ref[n, j]), (keys + BLOCK_LEN, bias)):
+            for spot, term in enumerate(three_terms(value)):
+                out_ref[n, at : at + BLOCK_LEN, spot * keys : (spot + 1) * keys] = term.astype(BF16)
+
+
+def project_body(n, first, x_ref, x_next_ref, mine_ref, theirs_ref, out_ref, here_ref):
     k = lax.axis_index("k")
     tall, _, frames, features = x_ref.shape
     wide = out_ref.shape[0] // 2
@@ -74,20 +93,17 @@
     columns = tiles * LANES
     ones = jnp.ones((8, features), BF16)
     total, power = 0.0, 0.0
-    for half, w_ref, g_ref in ((k, mine_ref, gain_ref), (1 - k, theirs_ref, gain_next_ref)):
+    for half, w_ref in ((k, mine_ref), (1 - k, theirs_ref)):
         x = x_next_ref[...] if first and half is not k else x_ref[:, half]
-        x = x.reshape(tall * frames, features).astype(F32)
-        scaled = (x * g_ref[n : n + 1, :]).astype(BF16)
-        total = total + dot(scaled, w_ref[:, n * columns : (n + 1) * columns])
-        square = x * x
+        x = x.reshape(tall * frames, features)
+        total = total + dot(x, w_ref[:, n * columns : (n + 1) * columns])
+        square = x.astype(F32) * x.astype(F32)
         high = square.astype(BF16)
         low = (square - high.astype(F32)).astype(BF16)
         power = power + dot(ones, high, EACH_ROW) + dot(ones, low, EACH_ROW)
-    here_ref[...] = x_ref[lax.axis_index("a"), 1 - k]
+    here_ref[...] = x_ref[head_index(), 1 - k]
     total = total.astype(BF16)
-    high = power.astype(BF16).astype(F32)
-    middle = (power - high).astype(BF16).astype(F32)
-    low = power - high - middle
+    high, middle, low = three_terms(power)
     row = lax.broadcasted_iota(jnp.int32, power.shape, 0)
     terms = jnp.where(row == 0, high, jnp.where(row == 1, middle, jnp.where(row == 2, low, 0.0)))
     terms = terms.astype(BF16)
@@ -102,7 +118,19 @@
         out_ref[spot, tiles * BLOCK_LEN :, :] = terms[:, lane : lane + LANES]
 
 
-def recur_body(n, got_ref, state_ref, state_next_ref, small_ref, gain_ref, out_ref, mine_ref, note_ref):
+def recur_body(
+    n,
+    got_ref,
+    memory_ref,
+    packet_ref,
+    decay_ref,
+    bias_ref,
+    lengths_ref,
+    gain_ref,
+    out_ref,
+    mine_ref,
+    note_ref,
+):
     b, c = lax.axis_index("b"), lax.axis_index("c")
     wide = got_ref.shape[1]
     frames = 2 * BLOCK_LEN
@@ -123,14 +151,24 @@
     def tile(half, spot):
         return summed[half][spot * BLOCK_LEN : (spot + 1) * BLOCK_LEN] * scale
 
-    alive = small_ref[n, 3 * BLOCK_LEN :]
+    def unpacked(at):
+        block = packet_ref[n, at : at + BLOCK_LEN, : 3 * LANES].astype(F32)
+        return block[:, :LANES] + block[:, LANES : 2 * LANES] + block[:, 2 * LANES :]
+
+    own_keys = memory_ref.shape[2]
+    length = lengths_ref[...].astype(F32)
+    here = lax.broadcasted_iota(jnp.int32, length.shape, 1) == b
+    length = jnp.sum(jnp.where(here, length, 0.0), axis=1, keepdims=True)
+    alive = jnp.where(row.astype(F32) < length, 1.0, 0.0)
+    extra = (decay_ref[n, b], unpacked(own_keys))
+    bias = (jnp.broadcast_to(bias_ref[n : n + 1, :], extra[0].shape), unpacked(own_keys + BLOCK_LEN))
     queries, keys, totals = [], [], []
     for half in range(2):
         queries.append(tile(half, 0) * KEY_DIM ** (-0.5))
         keys.append(tile(half, 1) * alive)
-        forget = tile(half, 2) + small_ref[n, 2 * BLOCK_LEN + half : 2 * BLOCK_LEN + half + 1]
+        forget = tile(half, 2) + jnp.where(b == half, *bias)
         log_gate = jnp.minimum(forget, 0.0) - jnp.log1p(jnp.exp(-jnp.abs(forget)))
-        total = (log_gate / TIME_CONSTANT + small_ref[n, half * BLOCK_LEN : (half + 1) * BLOCK_LEN]) * alive
+        total = (log_gate / TIME_CONSTANT + jnp.where(b == half, *extra)) * alive
         step = 1
         while step < BLOCK_LEN:
             total = total + jnp.where(row >= step, pltpu.roll(total, step, 0), 0.0)
@@ -141,8 +179,8 @@
     gate = jnp.concatenate([tile(half, spot) for half in range(2) for spot in (5, 6)], 1)
 
     carried = [queries[half] * jnp.exp(totals[half]) for half in range(2)]
-    read = dot(jnp.where(b == 0, carried[0], carried[1]).astype(BF16), state_ref[n])
-    read = read + dot(jnp.where(b == 0, carried[1], carried[0]).astype(BF16), state_next_ref[n])
+    read = dot(jnp.where(b == 0, carried[0], carried[1]).astype(BF16), memory_ref[n, b].astype(BF16))
+    read = read + dot(jnp.where(b == 0, carried[1], carried[0]).astype(BF16), packet_ref[n, :own_keys])
     for spot in range(BLOCK_LEN):
         score = 0.0
         for half in range(2):
@@ -201,16 +239,27 @@
     return value.astype(BF16).astype(F32)
 
 
+def quad_sum_body(got_ref, out_ref):
+    write_copies(out_ref, add_up(got_ref).astype(BF16))
+
+
 def next_stream_body(got_ref, x_ref, x_next_ref, out_ref):
-    a, b, k = (lax.axis_index(name) for name in "abk")
-    residual = jnp.where(b == k, x_ref[a, k].astype(F32), x_next_ref[a].astype(F32))
-    value = (residual + add_up(got_ref)).astype(BF16)
-    for spot in range(out_ref.shape[0]):
-        out_ref[spot] = value
+    b, k = lax.axis_index("b"), lax.axis_index("k")
+    frames = x_ref.shape[2]
+    blocks = got_ref.shape[1] // frames
+    first = (2 * lax.axis_index("near") + b) * (blocks // 2)
+    summed = add_up(got_ref)
+    for block in range(blocks):
+        c, half = first + block // 2, block % 2
+        residual = jnp.where(k == half, x_ref[c, k].astype(F32), x_next_ref[c].astype(F32))
+        rows = slice(block * frames, (block + 1) * frames)
+        value = (residual + summed[rows]).astype(BF16)
+        for spot in range(out_ref.shape[0]):
+            out_ref[spot, rows, :] = value
 
 
 def last_stream_body(got_ref, x_ref, next_ref, out_ref):
-    a, b, k = (lax.axis_index(name) for name in "abk")
+    a, b, k = head_index(), lax.axis_index("b"), lax.axis_index("k")
     residual = jnp.where(b == k, x_ref[a, k].astype(F32), next_ref[...].astype(F32))
     out_ref[...] = (residual + add_up(got_ref)).astype(BF16)
 
@@ -247,51 +296,36 @@
     output_projection,
     memory,
 ):
-    tall, wide = lax.axis_size("a"), lax.axis_size("c")
-    b, k = lax.axis_index("b"), lax.axis_index("k")
+    quads, quad = lax.axis_size("far"), lax.axis_size(QUAD)
+    tall, wide = lax.axis_size(HEAD), lax.axis_size("c")
+    k = lax.axis_index("k")
     frames, features = stream.shape
     keys = query_projection.shape[2]
     values = value_projection.shape[2]
     layers = memory.shape[0]
     columns = 3 * keys + 2 * values
+    decay = extra_frame_decay.reshape(layers, 2, BLOCK_LEN, keys)
 
     sent = kernel(copies_body, ((2 * tall, frames, features), BF16), stream)
-    sent, *weights_in = lax.optimization_barrier(
-        (
-            sent,
-            query_projection,
-            key_projection,
-            forget_gate_weight,
-            value_projection,
-            output_gate_weight,
-            output_projection,
-        )
-    )
-    gathered = exchange(sent, ALONG_TP).reshape(tall, 2, frames, features)
-
-    weights = []
-    for n in range(layers):
-        weights += [weight[n] for weight in weights_in[:-1]]
-    mine = jnp.concatenate([*weights, weights_in[-1][0]], 1)
+    x = exchange(sent, ALONG_TP).reshape(tall, 2, frames, features)
+    packet = kernel(pack_state_body, ((layers, keys + 2 * BLOCK_LEN, VALUE_DIM), BF16), memory, decay, forget_gate_bias)
+    weights = [
+        query_projection,
+        key_projection,
+        forget_gate_weight,
+        value_projection,
+        output_gate_weight,
+    ]
+    weights = [
+        (weight[n].astype(F32) * input_norm_gain[n][:, None]).astype(BF16)
+        for n in range(layers)
+        for weight in weights
+    ]
+    mine = jnp.concatenate([*weights, output_projection[0]], 1)
     theirs = other(mine, "k")
-    gain_next = other(input_norm_gain, "k")
-
-    decay = extra_frame_decay.reshape(layers, 2, BLOCK_LEN, keys)
-    bias = forget_gate_bias[:, None]
-    small_next = other(jnp.concatenate([pick(decay, 1 - b, 1), bias], 1), "b")
-    decay = ordered(pick(decay, b, 1), small_next[:, :BLOCK_LEN], b, 1)
-    bias = ordered(bias, small_next[:, BLOCK_LEN:], b, 1)
-    alive = (jnp.arange(BLOCK_LEN, dtype=jnp.int32) < pick(lengths, b, 0)).astype(F32)
-    alive = jnp.broadcast_to(alive[None, :, None], (layers, BLOCK_LEN, keys))
-    pad = jnp.zeros((layers, BLOCK_LEN - 2, keys), F32)
-    small = jnp.concatenate([decay, bias, pad, alive], 1)
-    state = pick(memory, b, 1).astype(BF16)
-    state_next = other(pick(memory, 1 - b, 1).astype(BF16), "b")
-
-    gathered, theirs, gain_next, small, state, state_next = lax.optimization_barrier(
-        (gathered, theirs, gain_next, small, state, state_next)
-    )
-    x, x_next = gathered, other(pick(gathered, 1 - k, 1), "k")
+    packet = other(packet, "b")
+    x, theirs, packet = lax.optimization_barrier((x, theirs, packet))
+    x_next = other(lax.dynamic_index_in_dim(x, 1 - k, 1, keepdims=False), "k")
 
     mines, notes = [], []
     for n in range(layers):
@@ -303,8 +337,6 @@
             x_next,
             mine,
             theirs,
-            input_norm_gain,
-            gain_next,
         )
         got = exchange(sent, ALONG_X).reshape(2, wide, rows, LANES)
         note_shape = (6 * BLOCK_LEN, LANES)
@@ -312,9 +344,11 @@
             functools.partial(recur_body, n),
             [((2 * wide, BLOCK_LEN, values), BF16), (note_shape, F32), (note_shape, F32)],
             got,
-            state,
-            state_next,
-            small,
+            memory,
+            packet,
+            decay,
+            forget_gate_bias,
+            lengths[None],
             head_norm_gain,
         )
         mines.append(own_note)
@@ -328,8 +362,11 @@
                 mine,
                 theirs,
             )
-            sent = kernel(next_stream_body, ((2 * tall, frames, features), BF16), exchange(sent, ALONG_TP), x, x_next)
-            x = exchange(sent, ALONG_TP).reshape(tall, 2, frames, features)
+            shape = (frames * 2 * tall // quad, features)
+            got = exchange(sent.reshape(quad, *shape), QUAD)
+            sent = kernel(quad_sum_body, ((quads, *shape), BF16), got)
+            sent = kernel(next_stream_body, ((quad, *shape), BF16), exchange(sent, "far"), x, x_next)
+            x = exchange(sent, QUAD).reshape(tall, 2, frames, features)
         else:
             theirs_got = other(jnp.concatenate([got, here.reshape(2, BLOCK_LEN, features)], 0), "k")
             sent = kernel(
@@ -354,8 +391,10 @@
 
 def solution(mesh):
     grp, tp, dp = (mesh.shape[name] for name in ("grp", "tp", "dp"))
-    fine = Mesh(mesh.devices.reshape(grp, tp // 2, 2, dp // 2, 2), ("grp", "a", "b", "c", "k"))
-    tp, dp = ("a", "b"), ("c", "k")
+    fine = Mesh(
+        mesh.devices.reshape(grp, tp // 4, 2, 2, dp // 2, 2), ("grp", *ALONG_TP, "c", "k")
+    )
+    tp, dp = ALONG_TP, ("c", "k")
     group_tp, group_dp = ("grp", *tp), ("grp", *dp)
     placed = (
         P(group_tp, dp),

time: 228 us -> 227 us (level)
  waiting for transfers between devices: 24.8 us -> 31.8 us
  blocking collectives: 120 us -> 115 us
  starting transfers between devices: 67.5 us -> 63.3 us
  other arithmetic: 0.77 us -> 3.62 us
  local copies, waits for them, and re-layouts: 5.96 us -> 3.52 us
    ppermute x7 -> x5, waiting for transfers between devices: 23.3 us -> 30.4 us  [other(): return lax.ppermute(array, axis, [(0, 1), (1, 0)])]
    all_to_all x6 -> x7, blocking collectives: 120 us -> 115 us  [exchange(): return lax.all_to_all(array, axes, 0, 0, tiled=True)]
    ppermute x7 -> x5, starting transfers between devices: 17.6 us -> 13.2 us  [other(): return lax.ppermute(array, axis, [(0, 1), (1, 0)])]
    unnamed x0 -> x10, other arithmetic: none -> 3.6 us
    pallas_call x10 -> x12, Pallas kernels: 7.45 us -> 8.32 us  [kernel(): pl.pallas_call(body, out_shape=shapes if several else shapes[0], in_specs...]
  transfers between devices with their start and end apart: 9 -> 7, of which waited for: 6 -> 5; matrix products, arithmetic and copies ran while one was open for 1% -> 0% of each run, Pallas kernels for 1% -> 1%
where the time goes in v4:
time: 227 us; the launch traced here: 226 us
  blocking collectives  115 us (51%)
  starting transfers between devices  63.3 us (28%)
  waiting for transfers between devices  31.8 us (14%)
  Pallas kernels  8.32 us (4%)
  other arithmetic  3.62 us (2%)
  local copies, waits for them, and re-layouts  3.52 us (2%)
    all_to_all x7, blocking collectives, exchange(): return lax.all_to_all(array, axes, 0, 0, tiled=True)  115 us
    all_to_all x2, starting transfers between devices, exchange(): return lax.all_to_all(array, axes, 0, 0, tiled=True)  50.2 us
    ppermute x5, waiting for transfers between devices, other(): return lax.ppermute(array, axis, [(0, 1), (1, 0)])  30.4 us
    ppermute x5, starting transfers between devices, other(): return lax.ppermute(array, axis, [(0, 1), (1, 0)])  13.2 us
    pallas_call x12, Pallas kernels, kernel(): pl.pallas_call(body, out_shape=shapes if several else shapes[0], in_specs...  8.32 us
  transfers between devices with their start and end apart: 7, of which 5 were waited for; matrix products, arithmetic and copies ran while one was open for 0% of the time, Pallas kernels for 1%

profile of v4, /device:TPU:80, one launch (start us, length us, event | category | flops | bytes accessed | tf_op | source)
XLA Modules:
  0.0 226.2 jit_solution(16806287165830617417)
XLA Ops:
  0.7 0.8 fusion.20
  1.4 0.9 fusion.14
  2.5 1.0 fusion.16
  4.6 1.0 fusion.19
  5.8 2.0 collective-permute-start
  7.8 0.7 copy-done.1
  8.6 43.8 %all-to-all-start = ((bf16[16,32,256]{2,1,0:T(8,128)(2,1)}), bf16[16,32,256]{2,1,0:T(8,128)(2,1)S(1)}, u32[]{:S(2)}, u32[]{:S(2)}) async-start(bf16[16,32,256]{2,1,0:T(8,128)(2,1)} %copy-done.1), calls=%async_computation | async-start | bytes 524288 | tf_op jit(solution)/shard_map/all_to_all | solution.py:27
  52.4 0.7 copy-done.5
  53.1 0.8 shard_map.141
  53.8 3.6 %collective-permute-start.1 = (bf16[2,160,512]{2,1,0:T(8,128)(2,1)}, bf16[2,160,512]{2,1,0:T(8,128)(2,1)}, u32[]{:S(2)}, u32[]{:S(2)}) collective-permute-start(bf16[2,160,512]{2,1,0:T(8,128)(2,1)} %shard_map.141), channel_id=1, source_target_pairs={{0,16},{16,0},{1,17},{17,1},{2,18},{18,2},{3,19},{19,3},{4,20},{20... | collective-permute-start | bytes 983048 | tf_op jit(solution)/shard_map/ppermute | solution.py:31
  57.5 16.0 %collective-permute-done.1.packet_ref = bf16[2,160,512]{2,1,0:T(8,128)(2,1)} collective-permute-done((bf16[2,160,512]{2,1,0:T(8,128)(2,1)}, bf16[2,160,512]{2,1,0:T(8,128)(2,1)}, u32[]{:S(2)}, u32[]{:S(2)}) %collective-permute-start.1) | collective-permute-done | bytes 327712 | tf_op jit(solution)/shard_map/ppermute | solution.py:31
  73.5 2.0 collective-permute-start.2
  75.5 1.3 collective-permute-done.2.x_next_ref
  76.8 1.1 shard_map.142
  77.9 21.9 %all_to_all.45 = bf16[16,120,128]{2,1,0:T(8,128)(2,1)S(1)} all-to-all(bf16[16,120,128]{2,1,0:T(8,128)(2,1)S(1)} %get-tuple-element.19), channel_id=1, replica_groups=mesh['grp'=2,'far'=4,'near'=2,'b'=2,'c'=8,'k'=2] {'b','c'}, dimensions={0} | all-to-all | bytes 983040 | tf_op jit(solution)/shard_map/all_to_all | solution.py:27
  99.8 0.7 copy-done.6
  100.4 1.4 shard_map.143
  101.8 13.9 %all_to_all.46.left_ref = bf16[16,16,256]{2,1,0:T(8,128)(2,1)S(1)} all-to-all(bf16[16,16,256]{2,1,0:T(8,128)(2,1)S(1)} %get-tuple-element.22), channel_id=1, replica_groups=mesh['grp'=2,'far'=4,'near'=2,'b'=2,'c'=8,'k'=2] {'b','c'}, dimensions={0} | all-to-all | bytes 262144 | tf_op jit(solution)/shard_map/all_to_all | solution.py:27
  116.0 11.5 %all_to_all.47.got_ref = bf16[4,128,256]{2,1,0:T(8,128)(2,1)S(1)} all-to-all(bf16[4,128,256]{2,1,0:T(8,128)(2,1)S(1)} %bitcast.56), channel_id=1, replica_groups=mesh['grp'=2,'far'=4,'near'=2,'b'=2,'c'=8,'k'=2] {'near','b'}, dimensions={0} | all-to-all | bytes 524288 | tf_op jit(solution)/shard_map/all_to_all | solution.py:27
  127.5 28.2 %all_to_all.48.got_ref = bf16[4,128,256]{2,1,0:T(8,128)(2,1)S(1)} all-to-all(bf16[4,128,256]{2,1,0:T(8,128)(2,1)S(1)} %shard_map.145), channel_id=1, replica_groups=mesh['grp'=2,'far'=4,'near'=2,'b'=2,'c'=8,'k'=2] {'far'}, dimensions={0} | all-to-all | bytes 524288 | tf_op jit(solution)/shard_map/all_to_all | solution.py:27
  155.7 9.5 %all_to_all.49 = bf16[4,128,256]{2,1,0:T(8,128)(2,1)S(1)} all-to-all(bf16[4,128,256]{2,1,0:T(8,128)(2,1)S(1)} %shard_map.146), channel_id=1, replica_groups=mesh['grp'=2,'far'=4,'near'=2,'b'=2,'c'=8,'k'=2] {'near','b'}, dimensions={0} | all-to-all | bytes 524288 | tf_op jit(solution)/shard_map/all_to_all | solution.py:27
  165.8 15.9 %all_to_all.50 = bf16[16,120,128]{2,1,0:T(8,128)(2,1)S(1)} all-to-all(bf16[16,120,128]{2,1,0:T(8,128)(2,1)S(1)} %get-tuple-element.23), channel_id=1, replica_groups=mesh['grp'=2,'far'=4,'near'=2,'b'=2,'c'=8,'k'=2] {'b','c'}, dimensions={0} | all-to-all | bytes 983040 | tf_op jit(solution)/shard_map/all_to_all | solution.py:27
  181.7 1.4 shard_map.148
  183.1 13.7 %all_to_all.51.left_ref = bf16[16,16,256]{2,1,0:T(8,128)(2,1)S(1)} all-to-all(bf16[16,16,256]{2,1,0:T(8,128)(2,1)S(1)} %get-tuple-element.25), channel_id=1, replica_groups=mesh['grp'=2,'far'=4,'near'=2,'b'=2,'c'=8,'k'=2] {'b','c'}, dimensions={0} | all-to-all | bytes 262144 | tf_op jit(solution)/shard_map/all_to_all | solution.py:27
  196.8 2.0 collective-permute-start.3
  198.8 1.3 collective-permute-done.3
  200.1 0.9 shard_map.149
  201.0 6.3 %all-to-all-start.8 = ((bf16[16,32,256]{2,1,0:T(8,128)(2,1)}), bf16[16,32,256]{2,1,0:T(8,128)(2,1)S(1)}, u32[]{:S(2)}, u32[]{:S(2)}) async-start(bf16[16,32,256]{2,1,0:T(8,128)(2,1)} %shard_map.149), calls=%async_computation.8 | async-start | bytes 524288 | tf_op jit(solution)/shard_map/all_to_all | solution.py:27
  207.4 3.7 %collective-permute-start.4 = (f32[2,96,128]{2,1,0:T(8,128)S(1)}, f32[2,96,128]{2,1,0:T(8,128)S(1)}, u32[]{:S(2)}, u32[]{:S(2)}) collective-permute-start(f32[2,96,128]{2,1,0:T(8,128)S(1)} %pad_maximum_fusion.1), channel_id=1, source_target_pairs={{0,16},{16,0},{1,17},{17,1},{2,18},{18,2},{3,19},{19,3},{4,20},{20... | collective-permute-start | bytes 294920 | tf_op jit(solution)/shard_map/ppermute | solution.py:31
  211.1 11.7 %collective-permute-done.4.theirs_ref = f32[2,96,128]{2,1,0:T(8,128)S(1)} collective-permute-done((f32[2,96,128]{2,1,0:T(8,128)S(1)}, f32[2,96,128]{2,1,0:T(8,128)S(1)}, u32[]{:S(2)}, u32[]{:S(2)}) %collective-permute-start.4) | collective-permute-done | bytes 98336 | tf_op jit(solution)/shard_map/ppermute | solution.py:31
  222.8 1.3 shard_map.151
  224.1 1.5 all-to-all-done.8.got_ref
  (45 shorter events, 3.0 us)
Async XLA Ops:
  0.6 1.7 copy-start.12
  0.6 2.8 %copy-start.7 = (bf16[2,256,256]{2,1,0:T(8,128)(2,1)S(1)}, bf16[2,256,256]{2,1,0:T(8,128)(2,1)}, u32[]{:S(2)}) copy-start(bf16[2,256,256]{2,1,0:T(8,128)(2,1)} %param.19) | copy-start | bytes 786436
  2.4 1.2 copy-start.8
  3.5 0.9 copy-start.11
  3.6 2.2 copy-start.9
  3.7 48.7 %copy-start = (f32[2,2,128,512]{3,2,1,0:T(8,128)S(1)}, f32[2,2,128,512]{3,2,1,0:T(8,128)}, u32[]{:S(2)}) copy-start(f32[2,2,128,512]{3,2,1,0:T(8,128)} %memory_ref.7) | copy-start | bytes 3145732
  5.8 2.0 copy-start.4
  5.8 67.7 %collective-permute-start = (bf16[256,2048]{1,0:T(8,128)(2,1)S(1)}, bf16[256,2048]{1,0:T(8,128)(2,1)S(1)}, u32[]{:S(2)}, u32[]{:S(2)}) collective-permute-start(bf16[256,2048]{1,0:T(8,128)(2,1)S(1)} %bitcast_dynamic-update-slice_fusion.mine_ref), channel_id=1, source_target_pairs={{0,1},{1,0},{2,3},{3,2},{4,5},{5,4},{6,7},{7,6},{8,9},{9,8},{10,11... | collective-permute-start | bytes 3145736 | tf_op jit(solution)/shard_map/ppermute | solution.py:31
  7.8 0.7 copy-start.1
  8.6 43.8 %copy-start.2 = (f32[2,32,128]{2,1,0:T(8,128)S(1)}, f32[2,32,128]{2,1,0:T(8,128)}, u32[]{:S(2)}) copy-start(f32[2,32,128]{2,1,0:T(8,128)} %param.22) | copy-start | bytes 98308
  8.6 64.9 %all-to-all-start = ((bf16[16,32,256]{2,1,0:T(8,128)(2,1)}), bf16[16,32,256]{2,1,0:T(8,128)(2,1)S(1)}, u32[]{:S(2)}, u32[]{:S(2)}) async-start(bf16[16,32,256]{2,1,0:T(8,128)(2,1)} %copy-done.1), calls=%async_computation | async-start | bytes 524288 | tf_op jit(solution)/shard_map/all_to_all | solution.py:27
  52.4 0.7 copy-start.5
  53.8 19.7 %collective-permute-start.1 = (bf16[2,160,512]{2,1,0:T(8,128)(2,1)}, bf16[2,160,512]{2,1,0:T(8,128)(2,1)}, u32[]{:S(2)}, u32[]{:S(2)}) collective-permute-start(bf16[2,160,512]{2,1,0:T(8,128)(2,1)} %shard_map.141), channel_id=1, source_target_pairs={{0,16},{16,0},{1,17},{17,1},{2,18},{18,2},{3,19},{19,3},{4,20},{20... | collective-permute-start | bytes 983048 | tf_op jit(solution)/shard_map/ppermute | solution.py:31
  73.5 3.3 %collective-permute-start.2 = (bf16[8,32,256]{2,1,0:T(8,128)(2,1)S(1)}, bf16[8,32,256]{2,1,0:T(8,128)(2,1)S(1)}, u32[]{:S(2)}, u32[]{:S(2)}) collective-permute-start(bf16[8,32,256]{2,1,0:T(8,128)(2,1)S(1)} %dynamic-slice_bitcast_fusion), channel_id=1, source_target_pairs={{0,1},{1,0},{2,3},{3,2},{4,5},{5,4},{6,7},{7,6},{8,9},{9,8},{10,11... | collective-permute-start | bytes 393224 | tf_op jit(solution)/shard_map/ppermute | solution.py:31
  77.9 21.9 %copy-start.3 = (f32[2,512]{1,0:T(2,128)S(1)}, f32[2,512]{1,0:T(2,128)}, u32[]{:S(2)}) copy-start(f32[2,512]{1,0:T(2,128)} %gain_ref.3) | copy-start | bytes 12292
  99.8 0.7 copy-start.6
  183.1 15.7 %copy-start.10 = (bf16[2,256,256]{2,1,0:T(8,128)(2,1)S(1)}, bf16[2,256,256]{2,1,0:T(8,128)(2,1)}, u32[]{:S(2)}) copy-start(bf16[2,256,256]{2,1,0:T(8,128)(2,1)} %param.24) | copy-start | bytes 786436
  196.8 3.3 %collective-permute-start.3 = (bf16[18,16,256]{2,1,0:T(8,128)(2,1)S(1)}, bf16[18,16,256]{2,1,0:T(8,128)(2,1)S(1)}, u32[]{:S(2)}, u32[]{:S(2)}) collective-permute-start(bf16[18,16,256]{2,1,0:T(8,128)(2,1)S(1)} %pad_maximum_fusion), channel_id=1, source_target_pairs={{0,1},{1,0},{2,3},{3,2},{4,5},{5,4},{6,7},{7,6},{8,9},{9,8},{10,11... | collective-permute-start | bytes 442376 | tf_op jit(solution)/shard_map/ppermute | solution.py:31
  201.0 24.5 %all-to-all-start.8 = ((bf16[16,32,256]{2,1,0:T(8,128)(2,1)}), bf16[16,32,256]{2,1,0:T(8,128)(2,1)S(1)}, u32[]{:S(2)}, u32[]{:S(2)}) async-start(bf16[16,32,256]{2,1,0:T(8,128)(2,1)} %shard_map.149), calls=%async_computation.8 | async-start | bytes 524288 | tf_op jit(solution)/shard_map/all_to_all | solution.py:27
  207.4 15.4 %collective-permute-start.4 = (f32[2,96,128]{2,1,0:T(8,128)S(1)}, f32[2,96,128]{2,1,0:T(8,128)S(1)}, u32[]{:S(2)}, u32[]{:S(2)}) collective-permute-start(f32[2,96,128]{2,1,0:T(8,128)S(1)} %pad_maximum_fusion.1), channel_id=1, source_target_pairs={{0,16},{16,0},{1,17},{17,1},{2,18},{18,2},{3,19},{19,3},{4,20},{20... | collective-permute-start | bytes 294920 | tf_op jit(solution)/shard_map/ppermute | solution.py:31

commit v5 on v4

--- a/solution.py
+++ b/solution.py
@@ -118,6 +118,14 @@
         out_ref[spot, tiles * BLOCK_LEN :, :] = terms[:, lane : lane + LANES]
 
 
+def chips_sum_body(got_ref, out_ref):
+    for half in range(2):
+        value = got_ref[half, 0].astype(F32)
+        for spot in range(1, got_ref.shape[1]):
+            value = value + got_ref[half, spot].astype(F32)
+        out_ref[half] = value
+
+
 def recur_body(
     n,
     got_ref,
@@ -132,15 +140,10 @@
     note_ref,
 ):
     b, c = lax.axis_index("b"), lax.axis_index("c")
-    wide = got_ref.shape[1]
+    wide = out_ref.shape[0] // 2
     frames = 2 * BLOCK_LEN
-    summed = []
-    for half in range(2):
-        value = got_ref[half, 0].astype(F32)
-        for spot in range(1, wide):
-            value = value + got_ref[half, spot].astype(F32)
-        summed.append(value)
-    tiles = got_ref.shape[2] // BLOCK_LEN
+    summed = [got_ref[half] for half in range(2)]
+    tiles = got_ref.shape[1] // BLOCK_LEN
     power = jnp.sum(summed[0][tiles * BLOCK_LEN :], axis=0, keepdims=True)
     row = lax.broadcasted_iota(jnp.int32, (BLOCK_LEN, LANES), 0)
     lane = lax.broadcasted_iota(jnp.int32, (BLOCK_LEN, LANES), 1)
@@ -324,7 +327,7 @@
     mine = jnp.concatenate([*weights, output_projection[0]], 1)
     theirs = other(mine, "k")
     packet = other(packet, "b")
-    x, theirs, packet = lax.optimization_barrier((x, theirs, packet))
+    x, theirs = lax.optimization_barrier((x, theirs))
     x_next = other(lax.dynamic_index_in_dim(x, 1 - k, 1, keepdims=False), "k")
 
     mines, notes = [], []
@@ -339,6 +342,7 @@
             theirs,
         )
         got = exchange(sent, ALONG_X).reshape(2, wide, rows, LANES)
+        got = kernel(chips_sum_body, ((2, rows, LANES), F32), got)
         note_shape = (6 * BLOCK_LEN, LANES)
         sent, own_note, note = kernel(
             functools.partial(recur_body, n),

time: 227 us -> 225 us (level)
  blocking collectives: 115 us -> 88.6 us
  waiting for transfers between devices: 31.8 us -> 43 us
  starting transfers between devices: 63.3 us -> 72.4 us
  local copies, waits for them, and re-layouts: 3.52 us -> 5.86 us
    all_to_all x2 -> x3, waiting for transfers between devices: 1.48 us -> 28.7 us  [exchange(): return lax.all_to_all(array, axes, 0, 0, tiled=True)]
    all_to_all x7 -> x6, blocking collectives: 115 us -> 88.6 us  [exchange(): return lax.all_to_all(array, axes, 0, 0, tiled=True)]
    ppermute x5, waiting for transfers between devices: 30.4 us -> 14.3 us  [other(): return lax.ppermute(array, axis, [(0, 1), (1, 0)])]
    all_to_all x2 -> x3, starting transfers between devices: 50.2 us -> 59.2 us  [exchange(): return lax.all_to_all(array, axes, 0, 0, tiled=True)]
    unnamed x26 -> x38, local copies, waits for them, and re-layouts: 2.71 us -> 5.05 us
    pallas_call x12 -> x14, Pallas kernels: 8.32 us -> 10.2 us  [kernel(): pl.pallas_call(body, out_shape=shapes if several else shapes[0], in_specs...]
  transfers between devices with their start and end apart: 7 -> 8, of which waited for: 5 -> 6; matrix products, arithmetic and copies ran while one was open for 0% -> 0% of each run, Pallas kernels for 1% -> 2%
where the time goes in v5:
time: 225 us; the launch traced here: 224 us
  blocking collectives  88.6 us (39%)
  starting transfers between devices  72.4 us (32%)
  waiting for transfers between devices  43 us (19%)
  Pallas kernels  10.2 us (5%)
  local copies, waits for them, and re-layouts  5.86 us (3%)
  other arithmetic  2.78 us (1%)
    all_to_all x6, blocking collectives, exchange(): return lax.all_to_all(array, axes, 0, 0, tiled=True)  88.6 us
    all_to_all x3, starting transfers between devices, exchange(): return lax.all_to_all(array, axes, 0, 0, tiled=True)  59.2 us
    all_to_all x3, waiting for transfers between devices, exchange(): return lax.all_to_all(array, axes, 0, 0, tiled=True)  28.7 us
    ppermute x5, waiting for transfers between devices, other(): return lax.ppermute(array, axis, [(0, 1), (1, 0)])  14.3 us
    ppermute x5, starting transfers between devices, other(): return lax.ppermute(array, axis, [(0, 1), (1, 0)])  13.2 us
    pallas_call x14, Pallas kernels, kernel(): pl.pallas_call(body, out_shape=shapes if several else shapes[0], in_specs...  10.2 us
    unnamed x38, local copies, waits for them, and re-layouts  5.05 us
  transfers between devices with their start and end apart: 8, of which 6 were waited for; matrix products, arithmetic and copies ran while one was open for 0% of the time, Pallas kernels for 2%

profile of v5, /device:TPU:80, one launch (start us, length us, event | category | flops | bytes accessed | tf_op | source)
XLA Modules:
  0.0 223.8 jit_solution(13673249384581810419)
XLA Ops:
  0.7 0.8 fusion.20
  1.4 0.9 fusion.14
  2.5 1.0 fusion.16
  3.7 0.8 copy-done.16
  6.5 2.0 collective-permute-start
  9.2 43.7 %all-to-all-start = ((bf16[16,32,256]{2,1,0:T(8,128)(2,1)}), bf16[16,32,256]{2,1,0:T(8,128)(2,1)S(1)}, u32[]{:S(2)}, u32[]{:S(2)}) async-start(bf16[16,32,256]{2,1,0:T(8,128)(2,1)} %shard_map.140), calls=%async_computation | async-start | bytes 524288 | tf_op jit(solution)/shard_map/all_to_all | solution.py:27
  52.9 18.6 %all-to-all-done = bf16[16,32,256]{2,1,0:T(8,128)(2,1)S(1)} async-done(((bf16[16,32,256]{2,1,0:T(8,128)(2,1)}), bf16[16,32,256]{2,1,0:T(8,128)(2,1)S(1)}, u32[]{:S(2)}, u32[]{:S(2)}) %all-to-all-start) | async-done | bytes 262176 | tf_op jit(solution)/shard_map/all_to_all | solution.py:27
  71.5 2.0 collective-permute-start.1
  73.5 1.3 collective-permute-done.1.x_next_ref
  74.8 1.1 shard_map.141
  75.9 0.8 copy-done.1
  76.6 8.9 %all-to-all-start.1 = ((bf16[16,120,128]{2,1,0:T(8,128)(2,1)}), bf16[16,120,128]{2,1,0:T(8,128)(2,1)}, u32[]{:S(2)}, u32[]{:S(2)}) async-start(bf16[16,120,128]{2,1,0:T(8,128)(2,1)} %copy-done.1), calls=%async_computation.1 | async-start | bytes 983040 | tf_op jit(solution)/shard_map/all_to_all | solution.py:27
  87.0 0.8 shard_map.143
  87.8 3.6 %collective-permute-start.2 = (bf16[2,160,512]{2,1,0:T(8,128)(2,1)}, bf16[2,160,512]{2,1,0:T(8,128)(2,1)}, u32[]{:S(2)}, u32[]{:S(2)}) collective-permute-start(bf16[2,160,512]{2,1,0:T(8,128)(2,1)} %shard_map.143), channel_id=1, source_target_pairs={{0,16},{16,0},{1,17},{17,1},{2,18},{18,2},{3,19},{19,3},{4,20},{20... | collective-permute-start | bytes 983048 | tf_op jit(solution)/shard_map/ppermute | solution.py:31
  91.4 8.6 %all-to-all-done.1 = bf16[16,120,128]{2,1,0:T(8,128)(2,1)} async-done(((bf16[16,120,128]{2,1,0:T(8,128)(2,1)}), bf16[16,120,128]{2,1,0:T(8,128)(2,1)}, u32[]{:S(2)}, u32[]{:S(2)}) %all-to-all-start.1) | async-done | bytes 491552 | tf_op jit(solution)/shard_map/all_to_all | solution.py:27
  100.0 1.1 shard_map.142.got_ref
  101.8 1.4 shard_map.144
  103.2 13.9 %all_to_all.45.left_ref = bf16[16,16,256]{2,1,0:T(8,128)(2,1)S(1)} all-to-all(bf16[16,16,256]{2,1,0:T(8,128)(2,1)S(1)} %get-tuple-element.20), channel_id=1, replica_groups=mesh['grp'=2,'far'=4,'near'=2,'b'=2,'c'=8,'k'=2] {'b','c'}, dimensions={0} | all-to-all | bytes 262144 | tf_op jit(solution)/shard_map/all_to_all | solution.py:27
  117.3 11.3 %all_to_all.46.got_ref = bf16[4,128,256]{2,1,0:T(8,128)(2,1)S(1)} all-to-all(bf16[4,128,256]{2,1,0:T(8,128)(2,1)S(1)} %bitcast.55), channel_id=1, replica_groups=mesh['grp'=2,'far'=4,'near'=2,'b'=2,'c'=8,'k'=2] {'near','b'}, dimensions={0} | all-to-all | bytes 524288 | tf_op jit(solution)/shard_map/all_to_all | solution.py:27
  128.7 22.5 %all_to_all.47.got_ref = bf16[4,128,256]{2,1,0:T(8,128)(2,1)S(1)} all-to-all(bf16[4,128,256]{2,1,0:T(8,128)(2,1)S(1)} %shard_map.146), channel_id=1, replica_groups=mesh['grp'=2,'far'=4,'near'=2,'b'=2,'c'=8,'k'=2] {'far'}, dimensions={0} | all-to-all | bytes 524288 | tf_op jit(solution)/shard_map/all_to_all | solution.py:27
  151.2 10.7 %all_to_all.48 = bf16[4,128,256]{2,1,0:T(8,128)(2,1)S(1)} all-to-all(bf16[4,128,256]{2,1,0:T(8,128)(2,1)S(1)} %shard_map.147), channel_id=1, replica_groups=mesh['grp'=2,'far'=4,'near'=2,'b'=2,'c'=8,'k'=2] {'near','b'}, dimensions={0} | all-to-all | bytes 524288 | tf_op jit(solution)/shard_map/all_to_all | solution.py:27
  162.4 15.8 %all_to_all.49 = bf16[16,120,128]{2,1,0:T(8,128)(2,1)S(1)} all-to-all(bf16[16,120,128]{2,1,0:T(8,128)(2,1)S(1)} %get-tuple-element.21), channel_id=1, replica_groups=mesh['grp'=2,'far'=4,'near'=2,'b'=2,'c'=8,'k'=2] {'b','c'}, dimensions={0} | all-to-all | bytes 983040 | tf_op jit(solution)/shard_map/all_to_all | solution.py:27
  178.2 1.4 shard_map.150
  179.6 14.4 %all_to_all.50.left_ref = bf16[16,16,256]{2,1,0:T(8,128)(2,1)S(1)} all-to-all(bf16[16,16,256]{2,1,0:T(8,128)(2,1)S(1)} %get-tuple-element.23), channel_id=1, replica_groups=mesh['grp'=2,'far'=4,'near'=2,'b'=2,'c'=8,'k'=2] {'b','c'}, dimensions={0} | all-to-all | bytes 262144 | tf_op jit(solution)/shard_map/all_to_all | solution.py:27
  194.1 2.0 collective-permute-start.3
  196.1 1.3 collective-permute-done.3
  197.4 0.9 shard_map.151
  198.3 6.6 %all-to-all-start.8 = ((bf16[16,32,256]{2,1,0:T(8,128)(2,1)}), bf16[16,32,256]{2,1,0:T(8,128)(2,1)S(1)}, u32[]{:S(2)}, u32[]{:S(2)}) async-start(bf16[16,32,256]{2,1,0:T(8,128)(2,1)} %shard_map.151), calls=%async_computation.8 | async-start | bytes 524288 | tf_op jit(solution)/shard_map/all_to_all | solution.py:27
  205.0 3.7 %collective-permute-start.4 = (f32[2,96,128]{2,1,0:T(8,128)S(1)}, f32[2,96,128]{2,1,0:T(8,128)S(1)}, u32[]{:S(2)}, u32[]{:S(2)}) collective-permute-start(f32[2,96,128]{2,1,0:T(8,128)S(1)} %pad_maximum_fusion.1), channel_id=1, source_target_pairs={{0,16},{16,0},{1,17},{17,1},{2,18},{18,2},{3,19},{19,3},{4,20},{20... | collective-permute-start | bytes 294920 | tf_op jit(solution)/shard_map/ppermute | solution.py:31
  208.7 11.7 %collective-permute-done.4.theirs_ref = f32[2,96,128]{2,1,0:T(8,128)S(1)} collective-permute-done((f32[2,96,128]{2,1,0:T(8,128)S(1)}, f32[2,96,128]{2,1,0:T(8,128)S(1)}, u32[]{:S(2)}, u32[]{:S(2)}) %collective-permute-start.4) | collective-permute-done | bytes 98336 | tf_op jit(solution)/shard_map/ppermute | solution.py:31
  220.3 1.3 shard_map.153
  221.6 1.5 all-to-all-done.8.got_ref
  (60 shorter events, 6.7 us)
Async XLA Ops:
  0.6 1.7 copy-start.17
  0.6 2.8 %copy-start.12 = (bf16[2,256,256]{2,1,0:T(8,128)(2,1)S(1)}, bf16[2,256,256]{2,1,0:T(8,128)(2,1)}, u32[]{:S(2)}) copy-start(bf16[2,256,256]{2,1,0:T(8,128)(2,1)} %param.19) | copy-start | bytes 786436
  2.4 1.2 copy-start.13
  3.6 0.9 copy-start.16
  4.5 0.9 copy-start.18
  5.5 1.0 copy-start.14
  6.5 2.0 copy-start.9
  6.5 65.0 %collective-permute-start = (bf16[256,2048]{1,0:T(8,128)(2,1)S(1)}, bf16[256,2048]{1,0:T(8,128)(2,1)S(1)}, u32[]{:S(2)}, u32[]{:S(2)}) collective-permute-start(bf16[256,2048]{1,0:T(8,128)(2,1)S(1)} %bitcast_dynamic-update-slice_fusion.mine_ref), channel_id=1, source_target_pairs={{0,1},{1,0},{2,3},{3,2},{4,5},{5,4},{6,7},{7,6},{8,9},{9,8},{10,11... | collective-permute-start | bytes 3145736 | tf_op jit(solution)/shard_map/ppermute | solution.py:31
  9.2 62.3 %all-to-all-start = ((bf16[16,32,256]{2,1,0:T(8,128)(2,1)}), bf16[16,32,256]{2,1,0:T(8,128)(2,1)S(1)}, u32[]{:S(2)}, u32[]{:S(2)}) async-start(bf16[16,32,256]{2,1,0:T(8,128)(2,1)} %shard_map.140), calls=%async_computation | async-start | bytes 524288 | tf_op jit(solution)/shard_map/all_to_all | solution.py:27
  71.5 3.3 %collective-permute-start.1 = (bf16[8,32,256]{2,1,0:T(8,128)(2,1)S(1)}, bf16[8,32,256]{2,1,0:T(8,128)(2,1)S(1)}, u32[]{:S(2)}, u32[]{:S(2)}) collective-permute-start(bf16[8,32,256]{2,1,0:T(8,128)(2,1)S(1)} %dynamic-slice_bitcast_fusion), channel_id=1, source_target_pairs={{0,1},{1,0},{2,3},{3,2},{4,5},{5,4},{6,7},{7,6},{8,9},{9,8},{10,11... | collective-permute-start | bytes 393224 | tf_op jit(solution)/shard_map/ppermute | solution.py:31
  74.8 10.8 %copy-start = (f32[2,2,128,512]{3,2,1,0:T(8,128)S(1)}, f32[2,2,128,512]{3,2,1,0:T(8,128)}, u32[]{:S(2)}) copy-start(f32[2,2,128,512]{3,2,1,0:T(8,128)} %memory_ref.7) | copy-start | bytes 3145732
  75.9 0.8 copy-start.1
  76.6 23.4 %all-to-all-start.1 = ((bf16[16,120,128]{2,1,0:T(8,128)(2,1)}), bf16[16,120,128]{2,1,0:T(8,128)(2,1)}, u32[]{:S(2)}, u32[]{:S(2)}) async-start(bf16[16,120,128]{2,1,0:T(8,128)(2,1)} %copy-done.1), calls=%async_computation.1 | async-start | bytes 983040 | tf_op jit(solution)/shard_map/all_to_all | solution.py:27
  85.5 0.7 copy-start.10
  86.2 0.8 copy-start.2
  87.8 13.4 %collective-permute-start.2 = (bf16[2,160,512]{2,1,0:T(8,128)(2,1)}, bf16[2,160,512]{2,1,0:T(8,128)(2,1)}, u32[]{:S(2)}, u32[]{:S(2)}) collective-permute-start(bf16[2,160,512]{2,1,0:T(8,128)(2,1)} %shard_map.143), channel_id=1, source_target_pairs={{0,16},{16,0},{1,17},{17,1},{2,18},{18,2},{3,19},{19,3},{4,20},{20... | collective-permute-start | bytes 983048 | tf_op jit(solution)/shard_map/ppermute | solution.py:31
  100.0 1.1 copy-start.3
  100.0 1.1 copy-start.8
  101.1 0.7 copy-start.11
  103.1 14.0 %copy-start.4 = (f32[96,128]{1,0:T(8,128)}, f32[96,128]{1,0:T(8,128)S(1)}, u32[]{:S(2)}) copy-start(f32[96,128]{1,0:T(8,128)S(1)} %get-tuple-element.28) | copy-start | bytes 147460
  103.2 13.9 %copy-start.6 = (f32[96,128]{1,0:T(8,128)}, f32[96,128]{1,0:T(8,128)S(1)}, u32[]{:S(2)}) copy-start(f32[96,128]{1,0:T(8,128)S(1)} %get-tuple-element.26.mine_ref) | copy-start | bytes 147460
  179.6 16.4 %copy-start.15 = (bf16[2,256,256]{2,1,0:T(8,128)(2,1)S(1)}, bf16[2,256,256]{2,1,0:T(8,128)(2,1)}, u32[]{:S(2)}) copy-start(bf16[2,256,256]{2,1,0:T(8,128)(2,1)} %param.24) | copy-start | bytes 786436
  194.1 3.3 %collective-permute-start.3 = (bf16[18,16,256]{2,1,0:T(8,128)(2,1)S(1)}, bf16[18,16,256]{2,1,0:T(8,128)(2,1)S(1)}, u32[]{:S(2)}, u32[]{:S(2)}) collective-permute-start(bf16[18,16,256]{2,1,0:T(8,128)(2,1)S(1)} %pad_maximum_fusion), channel_id=1, source_target_pairs={{0,1},{1,0},{2,3},{3,2},{4,5},{5,4},{6,7},{7,6},{8,9},{9,8},{10,11... | collective-permute-start | bytes 442376 | tf_op jit(solution)/shard_map/ppermute | solution.py:31
  198.3 6.6 %copy-start.5 = (f32[96,128]{1,0:T(8,128)S(1)}, f32[96,128]{1,0:T(8,128)}, u32[]{:S(2)}) copy-start(f32[96,128]{1,0:T(8,128)} %copy-done.4) | copy-start | bytes 147460
  198.3 24.8 %all-to-all-start.8 = ((bf16[16,32,256]{2,1,0:T(8,128)(2,1)}), bf16[16,32,256]{2,1,0:T(8,128)(2,1)S(1)}, u32[]{:S(2)}, u32[]{:S(2)}) async-start(bf16[16,32,256]{2,1,0:T(8,128)(2,1)} %shard_map.151), calls=%async_computation.8 | async-start | bytes 524288 | tf_op jit(solution)/shard_map/all_to_all | solution.py:27
  205.0 15.4 %copy-start.7 = (f32[96,128]{1,0:T(8,128)S(1)}, f32[96,128]{1,0:T(8,128)}, u32[]{:S(2)}) copy-start(f32[96,128]{1,0:T(8,128)} %copy-done.6) | copy-start | bytes 147460
  205.0 15.4 %collective-permute-start.4 = (f32[2,96,128]{2,1,0:T(8,128)S(1)}, f32[2,96,128]{2,1,0:T(8,128)S(1)}, u32[]{:S(2)}, u32[]{:S(2)}) collective-permute-start(f32[2,96,128]{2,1,0:T(8,128)S(1)} %pad_maximum_fusion.1), channel_id=1, source_target_pairs={{0,16},{16,0},{1,17},{17,1},{2,18},{18,2},{3,19},{19,3},{4,20},{20... | collective-permute-start | bytes 294920 | tf_op jit(solution)/shard_map/ppermute | solution.py:31

commit v6 on v5

--- a/solution.py
+++ b/solution.py
@@ -74,8 +74,14 @@
     write_copies(out_ref, in_ref[...])
 
 
-def pack_state_body(memory_ref, decay_ref, bias_ref, out_ref):
+def pack_state_body(memory_ref, decay_ref, bias_ref, lengths_ref, gain_ref, out_ref, alive_ref, kept_gain_ref):
     j = 1 - lax.axis_index("b")
+    length = lengths_ref[...].astype(F32)
+    here = lax.broadcasted_iota(jnp.int32, length.shape, 1) != j
+    length = jnp.sum(jnp.where(here, length, 0.0), axis=1, keepdims=True)
+    row = lax.broadcasted_iota(jnp.int32, alive_ref.shape, 0).astype(F32)
+    alive_ref[...] = jnp.where(row < length, 1.0, 0.0)
+    kept_gain_ref[...] = gain_ref[...]
     keys = memory_ref.shape[2]
     for n in range(memory_ref.shape[0]):
         out_ref[n, :keys] = memory_ref[n, j].astype(BF16)
@@ -85,7 +91,7 @@
                 out_ref[n, at : at + BLOCK_LEN, spot * keys : (spot + 1) * keys] = term.astype(BF16)
 
 
-def project_body(n, first, x_ref, x_next_ref, mine_ref, theirs_ref, out_ref, here_ref):
+def project_body(n, first, x_ref, x_next_ref, mine_ref, theirs_ref, out_ref, here_ref=None):
     k = lax.axis_index("k")
     tall, _, frames, features = x_ref.shape
     wide = out_ref.shape[0] // 2
@@ -101,7 +107,8 @@
         high = square.astype(BF16)
         low = (square - high.astype(F32)).astype(BF16)
         power = power + dot(ones, high, EACH_ROW) + dot(ones, low, EACH_ROW)
-    here_ref[...] = x_ref[head_index(), 1 - k]
+    if here_ref is not None:
+        here_ref[...] = x_ref[head_index(), 1 - k]
     total = total.astype(BF16)
     high, middle, low = three_terms(power)
     row = lax.broadcasted_iota(jnp.int32, power.shape, 0)
@@ -133,7 +140,7 @@
     packet_ref,
     decay_ref,
     bias_ref,
-    lengths_ref,
+    alive_ref,
     gain_ref,
     out_ref,
     mine_ref,
@@ -159,10 +166,7 @@
         return block[:, :LANES] + block[:, LANES : 2 * LANES] + block[:, 2 * LANES :]
 
     own_keys = memory_ref.shape[2]
-    length = lengths_ref[...].astype(F32)
-    here = lax.broadcasted_iota(jnp.int32, length.shape, 1) == b
-    length = jnp.sum(jnp.where(here, length, 0.0), axis=1, keepdims=True)
-    alive = jnp.where(row.astype(F32) < length, 1.0, 0.0)
+    alive = alive_ref[...]
     extra = (decay_ref[n, b], unpacked(own_keys))
     bias = (jnp.broadcast_to(bias_ref[n : n + 1, :], extra[0].shape), unpacked(own_keys + BLOCK_LEN))
     queries, keys, totals = [], [], []
@@ -311,7 +315,19 @@
 
     sent = kernel(copies_body, ((2 * tall, frames, features), BF16), stream)
     x = exchange(sent, ALONG_TP).reshape(tall, 2, frames, features)
-    packet = kernel(pack_state_body, ((layers, keys + 2 * BLOCK_LEN, VALUE_DIM), BF16), memory, decay, forget_gate_bias)
+    packet, alive, kept_gain = kernel(
+        pack_state_body,
+        [
+            ((layers, keys + 2 * BLOCK_LEN, VALUE_DIM), BF16),
+            ((BLOCK_LEN, LANES), F32),
+            (head_norm_gain.shape, F32),
+        ],
+        memory,
+        decay,
+        forget_gate_bias,
+        lengths[None],
+        head_norm_gain,
+    )
     weights = [
         query_projection,
         key_projection,
@@ -333,9 +349,10 @@
     mines, notes = [], []
     for n in range(layers):
         rows = columns // LANES * BLOCK_LEN + 8
-        sent, here = kernel(
+        outs = [((2 * wide, rows, LANES), BF16), ((frames, features), BF16)]
+        sent, *here = kernel(
             functools.partial(project_body, n, n == 0),
-            [((2 * wide, rows, LANES), BF16), ((frames, features), BF16)],
+            outs if n + 1 == layers else outs[:1],
             x,
             x_next,
             mine,
@@ -352,8 +369,8 @@
             packet,
             decay,
             forget_gate_bias,
-            lengths[None],
-            head_norm_gain,
+            alive,
+            kept_gain,
         )
         mines.append(own_note)
         notes.append(note)
@@ -372,7 +389,7 @@
             sent = kernel(next_stream_body, ((quad, *shape), BF16), exchange(sent, "far"), x, x_next)
             x = exchange(sent, QUAD).reshape(tall, 2, frames, features)
         else:
-            theirs_got = other(jnp.concatenate([got, here.reshape(2, BLOCK_LEN, features)], 0), "k")
+            theirs_got = other(jnp.concatenate([got, here[0].reshape(2, BLOCK_LEN, features)], 0), "k")
             sent = kernel(
                 output_same_features_body,
                 ((2 * tall, frames, features), BF16),

time: 225 us -> 220 us (0.978)
  starting transfers between devices: 72.4 us -> 69.5 us
    all_to_all x3, starting transfers between devices: 59.2 us -> 56.7 us  [exchange(): return lax.all_to_all(array, axes, 0, 0, tiled=True)]
where the time goes in v6:
time: 220 us; the launch traced here: 219 us
  blocking collectives  86.5 us (39%)
  starting transfers between devices  69.5 us (32%)
  waiting for transfers between devices  42.7 us (19%)
  Pallas kernels  9.68 us (4%)
  local copies, waits for them, and re-layouts  6.52 us (3%)
  other arithmetic  2.78 us (1%)
    all_to_all x6, blocking collectives, exchange(): return lax.all_to_all(array, axes, 0, 0, tiled=True)  86.5 us
    all_to_all x3, starting transfers between devices, exchange(): return lax.all_to_all(array, axes, 0, 0, tiled=True)  56.7 us
    all_to_all x3, waiting for transfers between devices, exchange(): return lax.all_to_all(array, axes, 0, 0, tiled=True)  28.1 us
    ppermute x5, waiting for transfers between devices, other(): return lax.ppermute(array, axis, [(0, 1), (1, 0)])  14.6 us
    ppermute x5, starting transfers between devices, other(): return lax.ppermute(array, axis, [(0, 1), (1, 0)])  12.8 us
    pallas_call x14, Pallas kernels, kernel(): pl.pallas_call(body, out_shape=shapes if several else shapes[0], in_specs...  9.68 us
    unnamed x38, local copies, waits for them, and re-layouts  5.72 us
  transfers between devices with their start and end apart: 8, of which 6 were waited for; matrix products, arithmetic and copies ran while one was open for 0% of the time, Pallas kernels for 2%

profile of v6, /device:TPU:80, one launch (start us, length us, event | category | flops | bytes accessed | tf_op | source)
XLA Modules:
  0.0 218.7 jit_solution(8987360691432308401)
XLA Ops:
  0.7 0.8 fusion.20
  1.4 0.9 fusion.14
  2.5 1.0 fusion.16
  3.7 0.8 copy-done.16
  6.5 2.0 collective-permute-start
  9.2 43.7 %all-to-all-start = ((bf16[16,32,256]{2,1,0:T(8,128)(2,1)}), bf16[16,32,256]{2,1,0:T(8,128)(2,1)S(1)}, u32[]{:S(2)}, u32[]{:S(2)}) async-start(bf16[16,32,256]{2,1,0:T(8,128)(2,1)} %shard_map.140), calls=%async_computation | async-start | bytes 524288 | tf_op jit(solution)/shard_map/all_to_all | solution.py:27
  52.9 18.6 %all-to-all-done = bf16[16,32,256]{2,1,0:T(8,128)(2,1)S(1)} async-done(((bf16[16,32,256]{2,1,0:T(8,128)(2,1)}), bf16[16,32,256]{2,1,0:T(8,128)(2,1)S(1)}, u32[]{:S(2)}, u32[]{:S(2)}) %all-to-all-start) | async-done | bytes 262176 | tf_op jit(solution)/shard_map/all_to_all | solution.py:27
  71.5 2.0 collective-permute-start.1
  73.5 1.3 collective-permute-done.1.x_next_ref
  75.3 0.8 copy-done.1
  76.1 8.9 %all-to-all-start.1 = ((bf16[16,120,128]{2,1,0:T(8,128)(2,1)}), bf16[16,120,128]{2,1,0:T(8,128)(2,1)}, u32[]{:S(2)}, u32[]{:S(2)}) async-start(bf16[16,120,128]{2,1,0:T(8,128)(2,1)} %copy-done.1), calls=%async_computation.1 | async-start | bytes 983040 | tf_op jit(solution)/shard_map/all_to_all | solution.py:27
  85.7 0.8 copy-done.2
  87.1 0.8 shard_map.143
  87.9 3.6 %collective-permute-start.2 = (bf16[2,160,512]{2,1,0:T(8,128)(2,1)}, bf16[2,160,512]{2,1,0:T(8,128)(2,1)}, u32[]{:S(2)}, u32[]{:S(2)}) collective-permute-start(bf16[2,160,512]{2,1,0:T(8,128)(2,1)} %get-tuple-element.20), channel_id=1, source_target_pairs={{0,16},{16,0},{1,17},{17,1},{2,18},{18,2},{3,19},{19,3},{4,20},{20... | collective-permute-start | bytes 983048 | tf_op jit(solution)/shard_map/ppermute | solution.py:31
  91.6 7.9 %all-to-all-done.1 = bf16[16,120,128]{2,1,0:T(8,128)(2,1)} async-done(((bf16[16,120,128]{2,1,0:T(8,128)(2,1)}), bf16[16,120,128]{2,1,0:T(8,128)(2,1)}, u32[]{:S(2)}, u32[]{:S(2)}) %all-to-all-start.1) | async-done | bytes 491552 | tf_op jit(solution)/shard_map/all_to_all | solution.py:27
  99.5 1.1 shard_map.142.got_ref
  100.6 1.4 shard_map.144
  102.6 15.0 %all_to_all.45.left_ref = bf16[16,16,256]{2,1,0:T(8,128)(2,1)S(1)} all-to-all(bf16[16,16,256]{2,1,0:T(8,128)(2,1)S(1)} %get-tuple-element.24), channel_id=1, replica_groups=mesh['grp'=2,'far'=4,'near'=2,'b'=2,'c'=8,'k'=2] {'b','c'}, dimensions={0} | all-to-all | bytes 262144 | tf_op jit(solution)/shard_map/all_to_all | solution.py:27
  117.9 10.8 %all_to_all.46.got_ref = bf16[4,128,256]{2,1,0:T(8,128)(2,1)S(1)} all-to-all(bf16[4,128,256]{2,1,0:T(8,128)(2,1)S(1)} %bitcast.55), channel_id=1, replica_groups=mesh['grp'=2,'far'=4,'near'=2,'b'=2,'c'=8,'k'=2] {'near','b'}, dimensions={0} | all-to-all | bytes 524288 | tf_op jit(solution)/shard_map/all_to_all | solution.py:27
  128.7 20.3 %all_to_all.47.got_ref = bf16[4,128,256]{2,1,0:T(8,128)(2,1)S(1)} all-to-all(bf16[4,128,256]{2,1,0:T(8,128)(2,1)S(1)} %shard_map.146), channel_id=1, replica_groups=mesh['grp'=2,'far'=4,'near'=2,'b'=2,'c'=8,'k'=2] {'far'}, dimensions={0} | all-to-all | bytes 524288 | tf_op jit(solution)/shard_map/all_to_all | solution.py:27
  149.1 12.5 %all_to_all.48 = bf16[4,128,256]{2,1,0:T(8,128)(2,1)S(1)} all-to-all(bf16[4,128,256]{2,1,0:T(8,128)(2,1)S(1)} %shard_map.147), channel_id=1, replica_groups=mesh['grp'=2,'far'=4,'near'=2,'b'=2,'c'=8,'k'=2] {'near','b'}, dimensions={0} | all-to-all | bytes 524288 | tf_op jit(solution)/shard_map/all_to_all | solution.py:27
  162.2 13.9 %all_to_all.49 = bf16[16,120,128]{2,1,0:T(8,128)(2,1)S(1)} all-to-all(bf16[16,120,128]{2,1,0:T(8,128)(2,1)S(1)} %get-tuple-element.25), channel_id=1, replica_groups=mesh['grp'=2,'far'=4,'near'=2,'b'=2,'c'=8,'k'=2] {'b','c'}, dimensions={0} | all-to-all | bytes 983040 | tf_op jit(solution)/shard_map/all_to_all | solution.py:27
  176.1 1.4 shard_map.150
  177.5 13.9 %all_to_all.50.left_ref = bf16[16,16,256]{2,1,0:T(8,128)(2,1)S(1)} all-to-all(bf16[16,16,256]{2,1,0:T(8,128)(2,1)S(1)} %get-tuple-element.27), channel_id=1, replica_groups=mesh['grp'=2,'far'=4,'near'=2,'b'=2,'c'=8,'k'=2] {'b','c'}, dimensions={0} | all-to-all | bytes 262144 | tf_op jit(solution)/shard_map/all_to_all | solution.py:27
  191.5 2.0 collective-permute-start.3
  193.5 1.3 collective-permute-done.3
  194.8 0.9 shard_map.151
  195.7 4.1 %all-to-all-start.8 = ((bf16[16,32,256]{2,1,0:T(8,128)(2,1)}), bf16[16,32,256]{2,1,0:T(8,128)(2,1)S(1)}, u32[]{:S(2)}, u32[]{:S(2)}) async-start(bf16[16,32,256]{2,1,0:T(8,128)(2,1)} %shard_map.151), calls=%async_computation.8 | async-start | bytes 524288 | tf_op jit(solution)/shard_map/all_to_all | solution.py:27
  199.9 3.3 %collective-permute-start.4 = (f32[2,96,128]{2,1,0:T(8,128)S(1)}, f32[2,96,128]{2,1,0:T(8,128)S(1)}, u32[]{:S(2)}, u32[]{:S(2)}) collective-permute-start(f32[2,96,128]{2,1,0:T(8,128)S(1)} %pad_maximum_fusion.1), channel_id=1, source_target_pairs={{0,16},{16,0},{1,17},{17,1},{2,18},{18,2},{3,19},{19,3},{4,20},{20... | collective-permute-start | bytes 294920 | tf_op jit(solution)/shard_map/ppermute | solution.py:31
  203.2 12.0 %collective-permute-done.4.theirs_ref = f32[2,96,128]{2,1,0:T(8,128)S(1)} collective-permute-done((f32[2,96,128]{2,1,0:T(8,128)S(1)}, f32[2,96,128]{2,1,0:T(8,128)S(1)}, u32[]{:S(2)}, u32[]{:S(2)}) %collective-permute-start.4) | collective-permute-done | bytes 98336 | tf_op jit(solution)/shard_map/ppermute | solution.py:31
  215.1 1.3 shard_map.153
  216.4 1.6 all-to-all-done.8.got_ref
  (60 shorter events, 7.1 us)
Async XLA Ops:
  0.6 1.7 copy-start.17
  0.6 2.8 %copy-start.12 = (bf16[2,256,256]{2,1,0:T(8,128)(2,1)S(1)}, bf16[2,256,256]{2,1,0:T(8,128)(2,1)}, u32[]{:S(2)}) copy-start(bf16[2,256,256]{2,1,0:T(8,128)(2,1)} %param.19) | copy-start | bytes 786436
  2.4 1.2 copy-start.13
  3.6 0.9 copy-start.16
  4.5 0.9 copy-start.18
  5.5 1.0 copy-start.14
  6.5 2.0 copy-start.8
  6.5 65.0 %collective-permute-start = (bf16[256,2048]{1,0:T(8,128)(2,1)S(1)}, bf16[256,2048]{1,0:T(8,128)(2,1)S(1)}, u32[]{:S(2)}, u32[]{:S(2)}) collective-permute-start(bf16[256,2048]{1,0:T(8,128)(2,1)S(1)} %bitcast_dynamic-update-slice_fusion.mine_ref), channel_id=1, source_target_pairs={{0,1},{1,0},{2,3},{3,2},{4,5},{5,4},{6,7},{7,6},{8,9},{9,8},{10,11... | collective-permute-start | bytes 3145736 | tf_op jit(solution)/shard_map/ppermute | solution.py:31
  9.2 62.3 %all-to-all-start = ((bf16[16,32,256]{2,1,0:T(8,128)(2,1)}), bf16[16,32,256]{2,1,0:T(8,128)(2,1)S(1)}, u32[]{:S(2)}, u32[]{:S(2)}) async-start(bf16[16,32,256]{2,1,0:T(8,128)(2,1)} %shard_map.140), calls=%async_computation | async-start | bytes 524288 | tf_op jit(solution)/shard_map/all_to_all | solution.py:27
  71.5 3.3 %collective-permute-start.1 = (bf16[8,32,256]{2,1,0:T(8,128)(2,1)S(1)}, bf16[8,32,256]{2,1,0:T(8,128)(2,1)S(1)}, u32[]{:S(2)}, u32[]{:S(2)}) collective-permute-start(bf16[8,32,256]{2,1,0:T(8,128)(2,1)S(1)} %dynamic-slice_bitcast_fusion), channel_id=1, source_target_pairs={{0,1},{1,0},{2,3},{3,2},{4,5},{5,4},{6,7},{7,6},{8,9},{9,8},{10,11... | collective-permute-start | bytes 393224 | tf_op jit(solution)/shard_map/ppermute | solution.py:31
  74.8 10.2 %copy-start = (f32[2,2,128,512]{3,2,1,0:T(8,128)S(1)}, f32[2,2,128,512]{3,2,1,0:T(8,128)}, u32[]{:S(2)}) copy-start(f32[2,2,128,512]{3,2,1,0:T(8,128)} %memory_ref.7) | copy-start | bytes 3145732
  75.3 0.8 copy-start.1
  76.1 23.4 %all-to-all-start.1 = ((bf16[16,120,128]{2,1,0:T(8,128)(2,1)}), bf16[16,120,128]{2,1,0:T(8,128)(2,1)}, u32[]{:S(2)}, u32[]{:S(2)}) async-start(bf16[16,120,128]{2,1,0:T(8,128)(2,1)} %copy-done.1), calls=%async_computation.1 | async-start | bytes 983040 | tf_op jit(solution)/shard_map/all_to_all | solution.py:27
  85.0 0.7 copy-start.9
  85.0 0.7 copy-start.11
  85.7 0.8 copy-start.2
  86.5 0.7 copy-start.10
  87.9 12.7 %collective-permute-start.2 = (bf16[2,160,512]{2,1,0:T(8,128)(2,1)}, bf16[2,160,512]{2,1,0:T(8,128)(2,1)}, u32[]{:S(2)}, u32[]{:S(2)}) collective-permute-start(bf16[2,160,512]{2,1,0:T(8,128)(2,1)} %get-tuple-element.20), channel_id=1, source_target_pairs={{0,16},{16,0},{1,17},{17,1},{2,18},{18,2},{3,19},{19,3},{4,20},{20... | collective-permute-start | bytes 983048 | tf_op jit(solution)/shard_map/ppermute | solution.py:31
  99.5 1.1 copy-start.3
  102.0 0.6 copy-start.6
  102.6 15.0 %copy-start.4 = (f32[96,128]{1,0:T(8,128)}, f32[96,128]{1,0:T(8,128)S(1)}, u32[]{:S(2)}) copy-start(f32[96,128]{1,0:T(8,128)S(1)} %get-tuple-element.32) | copy-start | bytes 147460
  177.5 15.9 %copy-start.15 = (bf16[2,256,256]{2,1,0:T(8,128)(2,1)S(1)}, bf16[2,256,256]{2,1,0:T(8,128)(2,1)}, u32[]{:S(2)}) copy-start(bf16[2,256,256]{2,1,0:T(8,128)(2,1)} %param.24) | copy-start | bytes 786436
  191.5 3.3 %collective-permute-start.3 = (bf16[18,16,256]{2,1,0:T(8,128)(2,1)S(1)}, bf16[18,16,256]{2,1,0:T(8,128)(2,1)S(1)}, u32[]{:S(2)}, u32[]{:S(2)}) collective-permute-start(bf16[18,16,256]{2,1,0:T(8,128)(2,1)S(1)} %pad_maximum_fusion), channel_id=1, source_target_pairs={{0,1},{1,0},{2,3},{3,2},{4,5},{5,4},{6,7},{7,6},{8,9},{9,8},{10,11... | collective-permute-start | bytes 442376 | tf_op jit(solution)/shard_map/ppermute | solution.py:31
  195.7 4.1 %copy-start.5 = (f32[96,128]{1,0:T(8,128)S(1)}, f32[96,128]{1,0:T(8,128)}, u32[]{:S(2)}) copy-start(f32[96,128]{1,0:T(8,128)} %copy-done.4) | copy-start | bytes 147460
  195.7 22.3 %all-to-all-start.8 = ((bf16[16,32,256]{2,1,0:T(8,128)(2,1)}), bf16[16,32,256]{2,1,0:T(8,128)(2,1)S(1)}, u32[]{:S(2)}, u32[]{:S(2)}) async-start(bf16[16,32,256]{2,1,0:T(8,128)(2,1)} %shard_map.151), calls=%async_computation.8 | async-start | bytes 524288 | tf_op jit(solution)/shard_map/all_to_all | solution.py:27
  199.8 15.3 %copy-start.7 = (f32[96,128]{1,0:T(8,128)S(1)}, f32[96,128]{1,0:T(8,128)}, u32[]{:S(2)}) copy-start(f32[96,128]{1,0:T(8,128)} %copy-done.6) | copy-start | bytes 147460
  199.9 15.3 %collective-permute-start.4 = (f32[2,96,128]{2,1,0:T(8,128)S(1)}, f32[2,96,128]{2,1,0:T(8,128)S(1)}, u32[]{:S(2)}, u32[]{:S(2)}) collective-permute-start(f32[2,96,128]{2,1,0:T(8,128)S(1)} %pad_maximum_fusion.1), channel_id=1, source_target_pairs={{0,16},{16,0},{1,17},{17,1},{2,18},{18,2},{3,19},{19,3},{4,20},{20... | collective-permute-start | bytes 294920 | tf_op jit(solution)/shard_map/ppermute | solution.py:31

commit v7 on v6

--- a/solution.py
+++ b/solution.py
@@ -210,11 +210,14 @@
     for half in range(2):
         last = totals[half][BLOCK_LEN - 1 :]
         weighted.append(keys[half] * jnp.exp(last - totals[half]))
-        kept.append(jnp.broadcast_to(jnp.exp(last), (BLOCK_LEN, LANES)))
+        block = jnp.zeros((BLOCK_LEN, LANES), F32)
+        for spot, term in enumerate(three_terms(jnp.exp(last))):
+            block = jnp.where(row == spot, term, block)
+        kept.append(block)
     for ref, test in ((mine_ref, b == 0), (note_ref, b != 0)):
         parts = [jnp.where(test, *weighted), *value_tiles, jnp.where(test, *kept)]
         for spot, part in enumerate(parts):
-            ref[spot * BLOCK_LEN : (spot + 1) * BLOCK_LEN] = part
+            ref[spot * BLOCK_LEN : (spot + 1) * BLOCK_LEN] = part.astype(BF16)
 
 
 def output_body(at, left_refs, right_refs, out_ref):
@@ -279,9 +282,10 @@
     for n in range(memory_ref.shape[0]):
         for j, note in ((b, mine_refs[n][...]), (1 - b, theirs_ref[n])):
             parts = [note[at : at + BLOCK_LEN] for at in range(0, note.shape[0], BLOCK_LEN)]
-            kept = jnp.sum(jnp.where(row == lane, parts[-1][:1], 0.0), axis=1, keepdims=True)
-            values = jnp.concatenate(parts[1:-1], 1).astype(BF16)
-            out_ref[n, j] = kept * memory_ref[n, j] + dot(parts[0].astype(BF16), values, EACH_COLUMN)
+            kept = jnp.sum(parts[-1].astype(F32), axis=0, keepdims=True)
+            kept = jnp.sum(jnp.where(row == lane, kept, 0.0), axis=1, keepdims=True)
+            values = jnp.concatenate(parts[1:-1], 1)
+            out_ref[n, j] = kept * memory_ref[n, j] + dot(parts[0], values, EACH_COLUMN)
 
 
 def memory_two_body(memory_ref, mine_ref, mine_next_ref, theirs_ref, out_ref):
@@ -363,7 +367,7 @@
         note_shape = (6 * BLOCK_LEN, LANES)
         sent, own_note, note = kernel(
             functools.partial(recur_body, n),
-            [((2 * wide, BLOCK_LEN, values), BF16), (note_shape, F32), (note_shape, F32)],
+            [((2 * wide, BLOCK_LEN, values), BF16), (note_shape, BF16), (note_shape, BF16)],
             got,
             memory,
             packet,

time: 220 us -> 220 us (level)
  no operation moved by 1% of the time
where the time goes in v7:
time: 220 us; the launch traced here: 219 us
  blocking collectives  86.5 us (39%)
  starting transfers between devices  69.5 us (32%)
  waiting for transfers between devices  42.7 us (19%)
  Pallas kernels  9.67 us (4%)
  local copies, waits for them, and re-layouts  7.11 us (3%)
  other arithmetic  2.77 us (1%)
    all_to_all x6, blocking collectives, exchange(): return lax.all_to_all(array, axes, 0, 0, tiled=True)  86.5 us
    all_to_all x3, starting transfers between devices, exchange(): return lax.all_to_all(array, axes, 0, 0, tiled=True)  56.7 us
    all_to_all x3, waiting for transfers between devices, exchange(): return lax.all_to_all(array, axes, 0, 0, tiled=True)  29.5 us
    ppermute x5, waiting for transfers between devices, other(): return lax.ppermute(array, axis, [(0, 1), (1, 0)])  13.2 us
    ppermute x5, starting transfers between devices, other(): return lax.ppermute(array, axis, [(0, 1), (1, 0)])  12.8 us
    pallas_call x14, Pallas kernels, kernel(): pl.pallas_call(body, out_shape=shapes if several else shapes[0], in_specs...  9.67 us
    unnamed x38, local copies, waits for them, and re-layouts  6.31 us
  transfers between devices with their start and end apart: 8, of which 6 were waited for; matrix products, arithmetic and copies ran while one was open for 0% of the time, Pallas kernels for 2%

profile of v7, /device:TPU:80, one launch (start us, length us, event | category | flops | bytes accessed | tf_op | source)
XLA Modules:
  0.0 219.3 jit_solution(3797354120685401687)
XLA Ops:
  0.7 0.8 fusion.20
  1.4 0.9 fusion.14
  2.5 1.0 fusion.16
  3.7 0.8 copy-done.16
  6.5 2.0 collective-permute-start
  9.2 43.7 %all-to-all-start = ((bf16[16,32,256]{2,1,0:T(8,128)(2,1)}), bf16[16,32,256]{2,1,0:T(8,128)(2,1)S(1)}, u32[]{:S(2)}, u32[]{:S(2)}) async-start(bf16[16,32,256]{2,1,0:T(8,128)(2,1)} %shard_map.140), calls=%async_computation | async-start | bytes 524288 | tf_op jit(solution)/shard_map/all_to_all | solution.py:27
  52.9 18.6 %all-to-all-done = bf16[16,32,256]{2,1,0:T(8,128)(2,1)S(1)} async-done(((bf16[16,32,256]{2,1,0:T(8,128)(2,1)}), bf16[16,32,256]{2,1,0:T(8,128)(2,1)S(1)}, u32[]{:S(2)}, u32[]{:S(2)}) %all-to-all-start) | async-done | bytes 262176 | tf_op jit(solution)/shard_map/all_to_all | solution.py:27
  71.5 2.0 collective-permute-start.1
  73.5 1.3 collective-permute-done.1.x_next_ref
  75.3 0.8 copy-done.1
  76.1 8.9 %all-to-all-start.1 = ((bf16[16,120,128]{2,1,0:T(8,128)(2,1)}), bf16[16,120,128]{2,1,0:T(8,128)(2,1)}, u32[]{:S(2)}, u32[]{:S(2)}) async-start(bf16[16,120,128]{2,1,0:T(8,128)(2,1)} %copy-done.1), calls=%async_computation.1 | async-start | bytes 983040 | tf_op jit(solution)/shard_map/all_to_all | solution.py:27
  85.7 0.8 copy-done.2
  87.1 0.8 shard_map.143
  87.9 3.6 %collective-permute-start.2 = (bf16[2,160,512]{2,1,0:T(8,128)(2,1)}, bf16[2,160,512]{2,1,0:T(8,128)(2,1)}, u32[]{:S(2)}, u32[]{:S(2)}) collective-permute-start(bf16[2,160,512]{2,1,0:T(8,128)(2,1)} %get-tuple-element.20), channel_id=1, source_target_pairs={{0,16},{16,0},{1,17},{17,1},{2,18},{18,2},{3,19},{19,3},{4,20},{20... | collective-permute-start | bytes 983048 | tf_op jit(solution)/shard_map/ppermute | solution.py:31
  91.6 7.9 %all-to-all-done.1 = bf16[16,120,128]{2,1,0:T(8,128)(2,1)} async-done(((bf16[16,120,128]{2,1,0:T(8,128)(2,1)}), bf16[16,120,128]{2,1,0:T(8,128)(2,1)}, u32[]{:S(2)}, u32[]{:S(2)}) %all-to-all-start.1) | async-done | bytes 491552 | tf_op jit(solution)/shard_map/all_to_all | solution.py:27
  99.5 1.1 shard_map.142.got_ref
  100.6 1.4 shard_map.144
  103.2 15.0 %all_to_all.45.left_ref = bf16[16,16,256]{2,1,0:T(8,128)(2,1)S(1)} all-to-all(bf16[16,16,256]{2,1,0:T(8,128)(2,1)S(1)} %get-tuple-element.24), channel_id=1, replica_groups=mesh['grp'=2,'far'=4,'near'=2,'b'=2,'c'=8,'k'=2] {'b','c'}, dimensions={0} | all-to-all | bytes 262144 | tf_op jit(solution)/shard_map/all_to_all | solution.py:27
  118.5 10.8 %all_to_all.46.got_ref = bf16[4,128,256]{2,1,0:T(8,128)(2,1)S(1)} all-to-all(bf16[4,128,256]{2,1,0:T(8,128)(2,1)S(1)} %bitcast.55), channel_id=1, replica_groups=mesh['grp'=2,'far'=4,'near'=2,'b'=2,'c'=8,'k'=2] {'near','b'}, dimensions={0} | all-to-all | bytes 524288 | tf_op jit(solution)/shard_map/all_to_all | solution.py:27
  129.3 20.3 %all_to_all.47.got_ref = bf16[4,128,256]{2,1,0:T(8,128)(2,1)S(1)} all-to-all(bf16[4,128,256]{2,1,0:T(8,128)(2,1)S(1)} %shard_map.146), channel_id=1, replica_groups=mesh['grp'=2,'far'=4,'near'=2,'b'=2,'c'=8,'k'=2] {'far'}, dimensions={0} | all-to-all | bytes 524288 | tf_op jit(solution)/shard_map/all_to_all | solution.py:27
  149.7 12.5 %all_to_all.48 = bf16[4,128,256]{2,1,0:T(8,128)(2,1)S(1)} all-to-all(bf16[4,128,256]{2,1,0:T(8,128)(2,1)S(1)} %shard_map.147), channel_id=1, replica_groups=mesh['grp'=2,'far'=4,'near'=2,'b'=2,'c'=8,'k'=2] {'near','b'}, dimensions={0} | all-to-all | bytes 524288 | tf_op jit(solution)/shard_map/all_to_all | solution.py:27
  162.7 13.9 %all_to_all.49 = bf16[16,120,128]{2,1,0:T(8,128)(2,1)S(1)} all-to-all(bf16[16,120,128]{2,1,0:T(8,128)(2,1)S(1)} %get-tuple-element.25), channel_id=1, replica_groups=mesh['grp'=2,'far'=4,'near'=2,'b'=2,'c'=8,'k'=2] {'b','c'}, dimensions={0} | all-to-all | bytes 983040 | tf_op jit(solution)/shard_map/all_to_all | solution.py:27
  176.7 1.4 shard_map.150
  178.1 13.9 %all_to_all.50.left_ref = bf16[16,16,256]{2,1,0:T(8,128)(2,1)S(1)} all-to-all(bf16[16,16,256]{2,1,0:T(8,128)(2,1)S(1)} %get-tuple-element.27), channel_id=1, replica_groups=mesh['grp'=2,'far'=4,'near'=2,'b'=2,'c'=8,'k'=2] {'b','c'}, dimensions={0} | all-to-all | bytes 262144 | tf_op jit(solution)/shard_map/all_to_all | solution.py:27
  192.0 2.0 collective-permute-start.3
  194.0 1.3 collective-permute-done.3
  195.4 0.9 shard_map.151
  196.3 4.1 %all-to-all-start.8 = ((bf16[16,32,256]{2,1,0:T(8,128)(2,1)}), bf16[16,32,256]{2,1,0:T(8,128)(2,1)S(1)}, u32[]{:S(2)}, u32[]{:S(2)}) async-start(bf16[16,32,256]{2,1,0:T(8,128)(2,1)} %shard_map.151), calls=%async_computation.8 | async-start | bytes 524288 | tf_op jit(solution)/shard_map/all_to_all | solution.py:27
  200.4 3.3 %collective-permute-start.4 = (bf16[2,96,128]{2,1,0:T(8,128)(2,1)S(1)}, bf16[2,96,128]{2,1,0:T(8,128)(2,1)S(1)}, u32[]{:S(2)}, u32[]{:S(2)}) collective-permute-start(bf16[2,96,128]{2,1,0:T(8,128)(2,1)S(1)} %pad_maximum_fusion.1), channel_id=1, source_target_pairs={{0,16},{16,0},{1,17},{17,1},{2,18},{18,2},{3,19},{19,3},{4,20},{20... | collective-permute-start | bytes 147464 | tf_op jit(solution)/shard_map/ppermute | solution.py:31
  203.8 10.6 %collective-permute-done.4.theirs_ref = bf16[2,96,128]{2,1,0:T(8,128)(2,1)S(1)} collective-permute-done((bf16[2,96,128]{2,1,0:T(8,128)(2,1)S(1)}, bf16[2,96,128]{2,1,0:T(8,128)(2,1)S(1)}, u32[]{:S(2)}, u32[]{:S(2)}) %collective-permute-start.4) | collective-permute-done | bytes 49184 | tf_op jit(solution)/shard_map/ppermute | solution.py:31
  214.3 1.3 shard_map.153
  215.6 3.0 %all-to-all-done.8.got_ref = bf16[16,32,256]{2,1,0:T(8,128)(2,1)S(1)} async-done(((bf16[16,32,256]{2,1,0:T(8,128)(2,1)}), bf16[16,32,256]{2,1,0:T(8,128)(2,1)S(1)}, u32[]{:S(2)}, u32[]{:S(2)}) %all-to-all-start.8) | async-done | bytes 262176 | tf_op jit(solution)/shard_map/all_to_all | solution.py:27
  (60 shorter events, 7.7 us)
Async XLA Ops:
  0.6 1.7 copy-start.17
  0.6 2.8 %copy-start.12 = (bf16[2,256,256]{2,1,0:T(8,128)(2,1)S(1)}, bf16[2,256,256]{2,1,0:T(8,128)(2,1)}, u32[]{:S(2)}) copy-start(bf16[2,256,256]{2,1,0:T(8,128)(2,1)} %param.19) | copy-start | bytes 786436
  2.4 1.2 copy-start.13
  3.6 0.9 copy-start.16
  4.5 0.9 copy-start.18
  5.5 1.0 copy-start.14
  6.5 2.0 copy-start.8
  6.5 65.0 %collective-permute-start = (bf16[256,2048]{1,0:T(8,128)(2,1)S(1)}, bf16[256,2048]{1,0:T(8,128)(2,1)S(1)}, u32[]{:S(2)}, u32[]{:S(2)}) collective-permute-start(bf16[256,2048]{1,0:T(8,128)(2,1)S(1)} %bitcast_dynamic-update-slice_fusion.mine_ref), channel_id=1, source_target_pairs={{0,1},{1,0},{2,3},{3,2},{4,5},{5,4},{6,7},{7,6},{8,9},{9,8},{10,11... | collective-permute-start | bytes 3145736 | tf_op jit(solution)/shard_map/ppermute | solution.py:31
  9.2 62.3 %all-to-all-start = ((bf16[16,32,256]{2,1,0:T(8,128)(2,1)}), bf16[16,32,256]{2,1,0:T(8,128)(2,1)S(1)}, u32[]{:S(2)}, u32[]{:S(2)}) async-start(bf16[16,32,256]{2,1,0:T(8,128)(2,1)} %shard_map.140), calls=%async_computation | async-start | bytes 524288 | tf_op jit(solution)/shard_map/all_to_all | solution.py:27
  71.5 3.3 %collective-permute-start.1 = (bf16[8,32,256]{2,1,0:T(8,128)(2,1)S(1)}, bf16[8,32,256]{2,1,0:T(8,128)(2,1)S(1)}, u32[]{:S(2)}, u32[]{:S(2)}) collective-permute-start(bf16[8,32,256]{2,1,0:T(8,128)(2,1)S(1)} %dynamic-slice_bitcast_fusion), channel_id=1, source_target_pairs={{0,1},{1,0},{2,3},{3,2},{4,5},{5,4},{6,7},{7,6},{8,9},{9,8},{10,11... | collective-permute-start | bytes 393224 | tf_op jit(solution)/shard_map/ppermute | solution.py:31
  74.8 10.2 %copy-start = (f32[2,2,128,512]{3,2,1,0:T(8,128)S(1)}, f32[2,2,128,512]{3,2,1,0:T(8,128)}, u32[]{:S(2)}) copy-start(f32[2,2,128,512]{3,2,1,0:T(8,128)} %memory_ref.7) | copy-start | bytes 3145732
  75.3 0.8 copy-start.1
  76.1 23.4 %all-to-all-start.1 = ((bf16[16,120,128]{2,1,0:T(8,128)(2,1)}), bf16[16,120,128]{2,1,0:T(8,128)(2,1)}, u32[]{:S(2)}, u32[]{:S(2)}) async-start(bf16[16,120,128]{2,1,0:T(8,128)(2,1)} %copy-done.1), calls=%async_computation.1 | async-start | bytes 983040 | tf_op jit(solution)/shard_map/all_to_all | solution.py:27
  85.0 0.7 copy-start.9
  85.0 0.7 copy-start.11
  85.7 0.8 copy-start.2
  86.5 0.7 copy-start.10
  87.9 12.7 %collective-permute-start.2 = (bf16[2,160,512]{2,1,0:T(8,128)(2,1)}, bf16[2,160,512]{2,1,0:T(8,128)(2,1)}, u32[]{:S(2)}, u32[]{:S(2)}) collective-permute-start(bf16[2,160,512]{2,1,0:T(8,128)(2,1)} %get-tuple-element.20), channel_id=1, source_target_pairs={{0,16},{16,0},{1,17},{17,1},{2,18},{18,2},{3,19},{19,3},{4,20},{20... | collective-permute-start | bytes 983048 | tf_op jit(solution)/shard_map/ppermute | solution.py:31
  99.5 1.1 copy-start.3
  102.0 0.6 copy-start.4
  102.6 0.6 copy-start.6
  178.1 15.9 %copy-start.15 = (bf16[2,256,256]{2,1,0:T(8,128)(2,1)S(1)}, bf16[2,256,256]{2,1,0:T(8,128)(2,1)}, u32[]{:S(2)}) copy-start(bf16[2,256,256]{2,1,0:T(8,128)(2,1)} %param.24) | copy-start | bytes 786436
  192.0 3.3 %collective-permute-start.3 = (bf16[18,16,256]{2,1,0:T(8,128)(2,1)S(1)}, bf16[18,16,256]{2,1,0:T(8,128)(2,1)S(1)}, u32[]{:S(2)}, u32[]{:S(2)}) collective-permute-start(bf16[18,16,256]{2,1,0:T(8,128)(2,1)S(1)} %pad_maximum_fusion), channel_id=1, source_target_pairs={{0,1},{1,0},{2,3},{3,2},{4,5},{5,4},{6,7},{7,6},{8,9},{9,8},{10,11... | collective-permute-start | bytes 442376 | tf_op jit(solution)/shard_map/ppermute | solution.py:31
  196.3 4.1 %copy-start.7 = (bf16[96,128]{1,0:T(8,128)(2,1)S(1)}, bf16[96,128]{1,0:T(8,128)(2,1)}, u32[]{:S(2)}) copy-start(bf16[96,128]{1,0:T(8,128)(2,1)} %copy-done.6) | copy-start | bytes 73732
  196.3 22.3 %all-to-all-start.8 = ((bf16[16,32,256]{2,1,0:T(8,128)(2,1)}), bf16[16,32,256]{2,1,0:T(8,128)(2,1)S(1)}, u32[]{:S(2)}, u32[]{:S(2)}) async-start(bf16[16,32,256]{2,1,0:T(8,128)(2,1)} %shard_map.151), calls=%async_computation.8 | async-start | bytes 524288 | tf_op jit(solution)/shard_map/all_to_all | solution.py:27
  200.4 13.9 %copy-start.5 = (bf16[96,128]{1,0:T(8,128)(2,1)S(1)}, bf16[96,128]{1,0:T(8,128)(2,1)}, u32[]{:S(2)}) copy-start(bf16[96,128]{1,0:T(8,128)(2,1)} %copy-done.4) | copy-start | bytes 73732
  200.4 13.9 %collective-permute-start.4 = (bf16[2,96,128]{2,1,0:T(8,128)(2,1)S(1)}, bf16[2,96,128]{2,1,0:T(8,128)(2,1)S(1)}, u32[]{:S(2)}, u32[]{:S(2)}) collective-permute-start(bf16[2,96,128]{2,1,0:T(8,128)(2,1)S(1)} %pad_maximum_fusion.1), channel_id=1, source_target_pairs={{0,16},{16,0},{1,17},{17,1},{2,18},{18,2},{3,19},{19,3},{4,20},{20... | collective-permute-start | bytes 147464 | tf_op jit(solution)/shard_map/ppermute | solution.py:31

commit v8 on v7

--- a/solution.py
+++ b/solution.py
@@ -250,7 +250,7 @@
 
 
 def quad_sum_body(got_ref, out_ref):
-    write_copies(out_ref, add_up(got_ref).astype(BF16))
+    out_ref[...] = add_up(got_ref).astype(BF16)
 
 
 def next_stream_body(got_ref, x_ref, x_next_ref, out_ref):
@@ -307,7 +307,7 @@
     output_projection,
     memory,
 ):
-    quads, quad = lax.axis_size("far"), lax.axis_size(QUAD)
+    quad = lax.axis_size(QUAD)
     tall, wide = lax.axis_size(HEAD), lax.axis_size("c")
     k = lax.axis_index("k")
     frames, features = stream.shape
@@ -389,8 +389,8 @@
             )
             shape = (frames * 2 * tall // quad, features)
             got = exchange(sent.reshape(quad, *shape), QUAD)
-            sent = kernel(quad_sum_body, ((quads, *shape), BF16), got)
-            sent = kernel(next_stream_body, ((quad, *shape), BF16), exchange(sent, "far"), x, x_next)
+            got = lax.all_gather(kernel(quad_sum_body, (shape, BF16), got), "far")
+            sent = kernel(next_stream_body, ((quad, *shape), BF16), got, x, x_next)
             x = exchange(sent, QUAD).reshape(tall, 2, frames, features)
         else:
             theirs_got = other(jnp.concatenate([got, here[0].reshape(2, BLOCK_LEN, features)], 0), "k")

time: 220 us -> 223 us (1.014)
  starting transfers between devices: 69.5 us -> 72.8 us
    all_to_all x6 -> x5, blocking collectives: 86.5 us -> 65.3 us  [exchange(): return lax.all_to_all(array, axes, 0, 0, tiled=True)]
    all_gather x0 -> x1, blocking collectives: none -> 20.5 us  [local(): got = lax.all_gather(kernel(quad_sum_body, (shape, BF16), got), 'far')]
    all_to_all x3, starting transfers between devices: 56.7 us -> 59.6 us  [exchange(): return lax.all_to_all(array, axes, 0, 0, tiled=True)]
where the time goes in v8:
time: 223 us; the launch traced here: 222 us
  blocking collectives  85.9 us (39%)
  starting transfers between devices  72.8 us (33%)
  waiting for transfers between devices  42.3 us (19%)
  Pallas kernels  9.67 us (4%)
  local copies, waits for them, and re-layouts  7.11 us (3%)
  other arithmetic  2.77 us (1%)
    all_to_all x5, blocking collectives, exchange(): return lax.all_to_all(array, axes, 0, 0, tiled=True)  65.3 us
    all_to_all x3, starting transfers between devices, exchange(): return lax.all_to_all(array, axes, 0, 0, tiled=True)  59.6 us
    all_to_all x3, waiting for transfers between devices, exchange(): return lax.all_to_all(array, axes, 0, 0, tiled=True)  29.1 us
    all_gather x1, blocking collectives, local(): got = lax.all_gather(kernel(quad_sum_body, (shape, BF16), got), 'far')  20.5 us
    ppermute x5, waiting for transfers between devices, other(): return lax.ppermute(array, axis, [(0, 1), (1, 0)])  13.2 us
    ppermute x5, starting transfers between devices, other(): return lax.ppermute(array, axis, [(0, 1), (1, 0)])  13.2 us
    pallas_call x14, Pallas kernels, kernel(): pl.pallas_call(body, out_shape=shapes if several else shapes[0], in_specs...  9.67 us
    unnamed x38, local copies, waits for them, and re-layouts  6.31 us
  transfers between devices with their start and end apart: 8, of which 6 were waited for; matrix products, arithmetic and copies ran while one was open for 0% of the time, Pallas kernels for 2%

profile of v8, /device:TPU:80, one launch (start us, length us, event | category | flops | bytes accessed | tf_op | source)
XLA Modules:
  0.0 221.6 jit_solution(1017476762117199370)
XLA Ops:
  0.7 0.8 fusion.20
  1.4 0.9 fusion.14
  2.5 1.0 fusion.16
  3.7 0.8 copy-done.16
  6.5 2.0 collective-permute-start
  9.2 43.7 %all-to-all-start = ((bf16[16,32,256]{2,1,0:T(8,128)(2,1)}), bf16[16,32,256]{2,1,0:T(8,128)(2,1)S(1)}, u32[]{:S(2)}, u32[]{:S(2)}) async-start(bf16[16,32,256]{2,1,0:T(8,128)(2,1)} %shard_map.140), calls=%async_computation | async-start | bytes 524288 | tf_op jit(solution)/shard_map/all_to_all | solution.py:27
  52.9 18.6 %all-to-all-done = bf16[16,32,256]{2,1,0:T(8,128)(2,1)S(1)} async-done(((bf16[16,32,256]{2,1,0:T(8,128)(2,1)}), bf16[16,32,256]{2,1,0:T(8,128)(2,1)S(1)}, u32[]{:S(2)}, u32[]{:S(2)}) %all-to-all-start) | async-done | bytes 262176 | tf_op jit(solution)/shard_map/all_to_all | solution.py:27
  71.5 2.0 collective-permute-start.1
  73.5 1.3 collective-permute-done.1.x_next_ref
  75.3 0.8 copy-done.1
  76.1 8.9 %all-to-all-start.1 = ((bf16[16,120,128]{2,1,0:T(8,128)(2,1)}), bf16[16,120,128]{2,1,0:T(8,128)(2,1)}, u32[]{:S(2)}, u32[]{:S(2)}) async-start(bf16[16,120,128]{2,1,0:T(8,128)(2,1)} %copy-done.1), calls=%async_computation.1 | async-start | bytes 983040 | tf_op jit(solution)/shard_map/all_to_all | solution.py:27
  85.7 0.8 copy-done.2
  87.1 0.8 shard_map.143
  87.9 3.6 %collective-permute-start.2 = (bf16[2,160,512]{2,1,0:T(8,128)(2,1)}, bf16[2,160,512]{2,1,0:T(8,128)(2,1)}, u32[]{:S(2)}, u32[]{:S(2)}) collective-permute-start(bf16[2,160,512]{2,1,0:T(8,128)(2,1)} %get-tuple-element.20), channel_id=1, source_target_pairs={{0,16},{16,0},{1,17},{17,1},{2,18},{18,2},{3,19},{19,3},{4,20},{20... | collective-permute-start | bytes 983048 | tf_op jit(solution)/shard_map/ppermute | solution.py:31
  91.6 7.9 %all-to-all-done.1 = bf16[16,120,128]{2,1,0:T(8,128)(2,1)} async-done(((bf16[16,120,128]{2,1,0:T(8,128)(2,1)}), bf16[16,120,128]{2,1,0:T(8,128)(2,1)}, u32[]{:S(2)}, u32[]{:S(2)}) %all-to-all-start.1) | async-done | bytes 491552 | tf_op jit(solution)/shard_map/all_to_all | solution.py:27
  99.5 1.1 shard_map.142.got_ref
  100.6 1.4 shard_map.144
  103.2 15.0 %all_to_all.40.left_ref = bf16[16,16,256]{2,1,0:T(8,128)(2,1)S(1)} all-to-all(bf16[16,16,256]{2,1,0:T(8,128)(2,1)S(1)} %get-tuple-element.24), channel_id=1, replica_groups=mesh['grp'=2,'far'=4,'near'=2,'b'=2,'c'=8,'k'=2] {'b','c'}, dimensions={0} | all-to-all | bytes 262144 | tf_op jit(solution)/shard_map/all_to_all | solution.py:27
  118.5 10.8 %all_to_all.41.got_ref = bf16[4,128,256]{2,1,0:T(8,128)(2,1)S(1)} all-to-all(bf16[4,128,256]{2,1,0:T(8,128)(2,1)S(1)} %bitcast.57), channel_id=1, replica_groups=mesh['grp'=2,'far'=4,'near'=2,'b'=2,'c'=8,'k'=2] {'near','b'}, dimensions={0} | all-to-all | bytes 524288 | tf_op jit(solution)/shard_map/all_to_all | solution.py:27
  129.3 20.5 %all-gather = bf16[512,256]{1,0:T(8,128)(2,1)S(1)} all-gather(bf16[128,256]{1,0:T(8,128)(2,1)S(1)} %shard_map.146), channel_id=2, replica_groups=mesh['grp'=2,'far'=4,'near'=2,'b'=2,'c'=8,'k'=2] {'far'}, dimensions={0}, use_global_device_ids=true | all-gather | bytes 327680 | tf_op jit(solution)/shard_map/all_gather | solution.py:392
  149.9 10.4 %all_to_all.42 = bf16[4,128,256]{2,1,0:T(8,128)(2,1)S(1)} all-to-all(bf16[4,128,256]{2,1,0:T(8,128)(2,1)S(1)} %shard_map.147), channel_id=1, replica_groups=mesh['grp'=2,'far'=4,'near'=2,'b'=2,'c'=8,'k'=2] {'near','b'}, dimensions={0} | all-to-all | bytes 524288 | tf_op jit(solution)/shard_map/all_to_all | solution.py:27
  160.9 13.7 %all_to_all.43 = bf16[16,120,128]{2,1,0:T(8,128)(2,1)S(1)} all-to-all(bf16[16,120,128]{2,1,0:T(8,128)(2,1)S(1)} %get-tuple-element.25), channel_id=1, replica_groups=mesh['grp'=2,'far'=4,'near'=2,'b'=2,'c'=8,'k'=2] {'b','c'}, dimensions={0} | all-to-all | bytes 983040 | tf_op jit(solution)/shard_map/all_to_all | solution.py:27
  174.7 1.4 shard_map.150
  176.1 15.3 %all_to_all.44.left_ref = bf16[16,16,256]{2,1,0:T(8,128)(2,1)S(1)} all-to-all(bf16[16,16,256]{2,1,0:T(8,128)(2,1)S(1)} %get-tuple-element.27), channel_id=1, replica_groups=mesh['grp'=2,'far'=4,'near'=2,'b'=2,'c'=8,'k'=2] {'b','c'}, dimensions={0} | all-to-all | bytes 262144 | tf_op jit(solution)/shard_map/all_to_all | solution.py:27
  191.4 2.0 collective-permute-start.3
  193.4 1.3 collective-permute-done.3
  194.7 0.9 shard_map.151
  195.7 7.1 %all-to-all-start.7 = ((bf16[16,32,256]{2,1,0:T(8,128)(2,1)}), bf16[16,32,256]{2,1,0:T(8,128)(2,1)S(1)}, u32[]{:S(2)}, u32[]{:S(2)}) async-start(bf16[16,32,256]{2,1,0:T(8,128)(2,1)} %shard_map.151), calls=%async_computation.7 | async-start | bytes 524288 | tf_op jit(solution)/shard_map/all_to_all | solution.py:27
  202.8 3.7 %collective-permute-start.4 = (bf16[2,96,128]{2,1,0:T(8,128)(2,1)S(1)}, bf16[2,96,128]{2,1,0:T(8,128)(2,1)S(1)}, u32[]{:S(2)}, u32[]{:S(2)}) collective-permute-start(bf16[2,96,128]{2,1,0:T(8,128)(2,1)S(1)} %pad_maximum_fusion.1), channel_id=1, source_target_pairs={{0,16},{16,0},{1,17},{17,1},{2,18},{18,2},{3,19},{19,3},{4,20},{20... | collective-permute-start | bytes 147464 | tf_op jit(solution)/shard_map/ppermute | solution.py:31
  206.4 10.6 %collective-permute-done.4.theirs_ref = bf16[2,96,128]{2,1,0:T(8,128)(2,1)S(1)} collective-permute-done((bf16[2,96,128]{2,1,0:T(8,128)(2,1)S(1)}, bf16[2,96,128]{2,1,0:T(8,128)(2,1)S(1)}, u32[]{:S(2)}, u32[]{:S(2)}) %collective-permute-start.4) | collective-permute-done | bytes 49184 | tf_op jit(solution)/shard_map/ppermute | solution.py:31
  217.0 1.3 shard_map.153
  218.3 2.6 %all-to-all-done.7.got_ref = bf16[16,32,256]{2,1,0:T(8,128)(2,1)S(1)} async-done(((bf16[16,32,256]{2,1,0:T(8,128)(2,1)}), bf16[16,32,256]{2,1,0:T(8,128)(2,1)S(1)}, u32[]{:S(2)}, u32[]{:S(2)}) %all-to-all-start.7) | async-done | bytes 262176 | tf_op jit(solution)/shard_map/all_to_all | solution.py:27
  (60 shorter events, 7.7 us)
Async XLA Ops:
  0.6 1.7 copy-start.17
  0.6 2.8 %copy-start.12 = (bf16[2,256,256]{2,1,0:T(8,128)(2,1)S(1)}, bf16[2,256,256]{2,1,0:T(8,128)(2,1)}, u32[]{:S(2)}) copy-start(bf16[2,256,256]{2,1,0:T(8,128)(2,1)} %param.19) | copy-start | bytes 786436
  2.4 1.2 copy-start.13
  3.6 0.9 copy-start.16
  4.5 0.9 copy-start.18
  5.5 1.0 copy-start.14
  6.5 2.0 copy-start.8
  6.5 65.0 %collective-permute-start = (bf16[256,2048]{1,0:T(8,128)(2,1)S(1)}, bf16[256,2048]{1,0:T(8,128)(2,1)S(1)}, u32[]{:S(2)}, u32[]{:S(2)}) collective-permute-start(bf16[256,2048]{1,0:T(8,128)(2,1)S(1)} %bitcast_dynamic-update-slice_fusion.mine_ref), channel_id=1, source_target_pairs={{0,1},{1,0},{2,3},{3,2},{4,5},{5,4},{6,7},{7,6},{8,9},{9,8},{10,11... | collective-permute-start | bytes 3145736 | tf_op jit(solution)/shard_map/ppermute | solution.py:31
  9.2 62.3 %all-to-all-start = ((bf16[16,32,256]{2,1,0:T(8,128)(2,1)}), bf16[16,32,256]{2,1,0:T(8,128)(2,1)S(1)}, u32[]{:S(2)}, u32[]{:S(2)}) async-start(bf16[16,32,256]{2,1,0:T(8,128)(2,1)} %shard_map.140), calls=%async_computation | async-start | bytes 524288 | tf_op jit(solution)/shard_map/all_to_all | solution.py:27
  71.5 3.3 %collective-permute-start.1 = (bf16[8,32,256]{2,1,0:T(8,128)(2,1)S(1)}, bf16[8,32,256]{2,1,0:T(8,128)(2,1)S(1)}, u32[]{:S(2)}, u32[]{:S(2)}) collective-permute-start(bf16[8,32,256]{2,1,0:T(8,128)(2,1)S(1)} %dynamic-slice_bitcast_fusion), channel_id=1, source_target_pairs={{0,1},{1,0},{2,3},{3,2},{4,5},{5,4},{6,7},{7,6},{8,9},{9,8},{10,11... | collective-permute-start | bytes 393224 | tf_op jit(solution)/shard_map/ppermute | solution.py:31
  74.8 10.2 %copy-start = (f32[2,2,128,512]{3,2,1,0:T(8,128)S(1)}, f32[2,2,128,512]{3,2,1,0:T(8,128)}, u32[]{:S(2)}) copy-start(f32[2,2,128,512]{3,2,1,0:T(8,128)} %memory_ref.7) | copy-start | bytes 3145732
  75.3 0.8 copy-start.1
  76.1 23.4 %all-to-all-start.1 = ((bf16[16,120,128]{2,1,0:T(8,128)(2,1)}), bf16[16,120,128]{2,1,0:T(8,128)(2,1)}, u32[]{:S(2)}, u32[]{:S(2)}) async-start(bf16[16,120,128]{2,1,0:T(8,128)(2,1)} %copy-done.1), calls=%async_computation.1 | async-start | bytes 983040 | tf_op jit(solution)/shard_map/all_to_all | solution.py:27
  85.0 0.7 copy-start.9
  85.0 0.7 copy-start.11
  85.7 0.8 copy-start.2
  86.5 0.7 copy-start.10
  87.9 12.7 %collective-permute-start.2 = (bf16[2,160,512]{2,1,0:T(8,128)(2,1)}, bf16[2,160,512]{2,1,0:T(8,128)(2,1)}, u32[]{:S(2)}, u32[]{:S(2)}) collective-permute-start(bf16[2,160,512]{2,1,0:T(8,128)(2,1)} %get-tuple-element.20), channel_id=1, source_target_pairs={{0,16},{16,0},{1,17},{17,1},{2,18},{18,2},{3,19},{19,3},{4,20},{20... | collective-permute-start | bytes 983048 | tf_op jit(solution)/shard_map/ppermute | solution.py:31
  99.5 1.1 copy-start.3
  102.0 0.6 copy-start.4
  102.6 0.6 copy-start.6
  176.1 17.3 %copy-start.15 = (bf16[2,256,256]{2,1,0:T(8,128)(2,1)S(1)}, bf16[2,256,256]{2,1,0:T(8,128)(2,1)}, u32[]{:S(2)}) copy-start(bf16[2,256,256]{2,1,0:T(8,128)(2,1)} %param.24) | copy-start | bytes 786436
  191.4 3.3 %collective-permute-start.3 = (bf16[18,16,256]{2,1,0:T(8,128)(2,1)S(1)}, bf16[18,16,256]{2,1,0:T(8,128)(2,1)S(1)}, u32[]{:S(2)}, u32[]{:S(2)}) collective-permute-start(bf16[18,16,256]{2,1,0:T(8,128)(2,1)S(1)} %pad_maximum_fusion), channel_id=1, source_target_pairs={{0,1},{1,0},{2,3},{3,2},{4,5},{5,4},{6,7},{7,6},{8,9},{9,8},{10,11... | collective-permute-start | bytes 442376 | tf_op jit(solution)/shard_map/ppermute | solution.py:31
  195.7 7.1 %copy-start.7 = (bf16[96,128]{1,0:T(8,128)(2,1)S(1)}, bf16[96,128]{1,0:T(8,128)(2,1)}, u32[]{:S(2)}) copy-start(bf16[96,128]{1,0:T(8,128)(2,1)} %copy-done.6) | copy-start | bytes 73732
  195.7 25.3 %all-to-all-start.7 = ((bf16[16,32,256]{2,1,0:T(8,128)(2,1)}), bf16[16,32,256]{2,1,0:T(8,128)(2,1)S(1)}, u32[]{:S(2)}, u32[]{:S(2)}) async-start(bf16[16,32,256]{2,1,0:T(8,128)(2,1)} %shard_map.151), calls=%async_computation.7 | async-start | bytes 524288 | tf_op jit(solution)/shard_map/all_to_all | solution.py:27
  202.8 14.3 %copy-start.5 = (bf16[96,128]{1,0:T(8,128)(2,1)S(1)}, bf16[96,128]{1,0:T(8,128)(2,1)}, u32[]{:S(2)}) copy-start(bf16[96,128]{1,0:T(8,128)(2,1)} %copy-done.4) | copy-start | bytes 73732
  202.8 14.3 %collective-permute-start.4 = (bf16[2,96,128]{2,1,0:T(8,128)(2,1)S(1)}, bf16[2,96,128]{2,1,0:T(8,128)(2,1)S(1)}, u32[]{:S(2)}, u32[]{:S(2)}) collective-permute-start(bf16[2,96,128]{2,1,0:T(8,128)(2,1)S(1)} %pad_maximum_fusion.1), channel_id=1, source_target_pairs={{0,16},{16,0},{1,17},{17,1},{2,18},{18,2},{3,19},{19,3},{4,20},{20... | collective-permute-start | bytes 147464 | tf_op jit(solution)/shard_map/ppermute | solution.py:31

commit v9 on v8

--- a/solution.py
+++ b/solution.py
@@ -220,7 +220,7 @@
             ref[spot * BLOCK_LEN : (spot + 1) * BLOCK_LEN] = part.astype(BF16)
 
 
-def output_body(at, left_refs, right_refs, out_ref):
+def output_body(at, turns, left_refs, right_refs, out_ref):
     k = lax.axis_index("k")
     wide = out_ref.shape[0] // 2
     for half, left_ref, right_ref in ((k, left_refs[0], right_refs[0]), (1 - k, left_refs[1], right_refs[1])):
@@ -229,17 +229,20 @@
         partial = dot(left, right_ref[:, at : at + width]).astype(BF16)
         for spot in range(2 * wide):
             j, c = divmod(spot, wide)
-            out_ref[2 * c + half, j * BLOCK_LEN : (j + 1) * BLOCK_LEN, :] = partial[
+            place = 2 * c + half
+            if turns is not None:
+                place = (2 * (c % 2) + half) * turns + c // 2
+            out_ref[place, j * BLOCK_LEN : (j + 1) * BLOCK_LEN, :] = partial[
                 spot * BLOCK_LEN : (spot + 1) * BLOCK_LEN
             ]
 
 
 def output_same_frames_body(at, left_ref, mine_ref, theirs_ref, out_ref):
-    output_body(at, (left_ref, left_ref), (mine_ref, theirs_ref), out_ref)
-
-
-def output_same_features_body(left_ref, left_next_ref, right_ref, out_ref):
-    output_body(0, (left_ref, left_next_ref), (right_ref, right_ref), out_ref)
+    output_body(at, None, (left_ref, left_ref), (mine_ref, theirs_ref), out_ref)
+
+
+def output_same_features_body(turns, left_ref, left_next_ref, right_ref, out_ref):
+    output_body(0, turns, (left_ref, left_next_ref), (right_ref, right_ref), out_ref)
 
 
 def add_up(ref):
@@ -395,18 +398,21 @@
         else:
             theirs_got = other(jnp.concatenate([got, here[0].reshape(2, BLOCK_LEN, features)], 0), "k")
             sent = kernel(
-                output_same_features_body,
+                functools.partial(output_same_features_body, lax.axis_size("far")),
                 ((2 * tall, frames, features), BF16),
                 got,
                 theirs_got[: 2 * wide],
                 output_projection[n],
             )
+            shape = (frames * 2 * tall // quad, features)
+            got = exchange(sent.reshape(quad, *shape), QUAD)
+            sent = kernel(quad_sum_body, (shape, BF16), got).reshape(-1, frames, features)
             notes, sent = lax.optimization_barrier((notes, sent))
             theirs_note = other(jnp.stack(notes), "b")
             current = kernel(
                 last_stream_body,
                 (stream.shape, BF16),
-                exchange(sent, ALONG_TP),
+                exchange(sent, "far"),
                 x,
                 theirs_got[2 * wide :].reshape(frames, features),
             )

time: 223 us -> 229 us (1.027)
  blocking collectives: 85.9 us -> 97.7 us
  waiting for transfers between devices: 42.3 us -> 38.7 us
    all_to_all x5 -> x6, blocking collectives: 65.3 us -> 77.2 us  [exchange(): return lax.all_to_all(array, axes, 0, 0, tiled=True)]
    ppermute x5, waiting for transfers between devices: 13.2 us -> 6.47 us  [other(): return lax.ppermute(array, axis, [(0, 1), (1, 0)])]
    all_to_all x3, waiting for transfers between devices: 29.1 us -> 32.2 us  [exchange(): return lax.all_to_all(array, axes, 0, 0, tiled=True)]
    pallas_call x14 -> x15, Pallas kernels: 9.67 us -> 9.61 us  [kernel(): pl.pallas_call(body, out_shape=shapes if several else shapes[0], in_specs...]
where the time goes in v9:
time: 229 us; the launch traced here: 228 us
  blocking collectives  97.7 us (43%)
  starting transfers between devices  71 us (31%)
  waiting for transfers between devices  38.7 us (17%)
  Pallas kernels  9.61 us (4%)
  local copies, waits for them, and re-layouts  7.1 us (3%)
  other arithmetic  2.77 us (1%)
    all_to_all x6, blocking collectives, exchange(): return lax.all_to_all(array, axes, 0, 0, tiled=True)  77.2 us
    all_to_all x3, starting transfers between devices, exchange(): return lax.all_to_all(array, axes, 0, 0, tiled=True)  59.3 us
    all_to_all x3, waiting for transfers between devices, exchange(): return lax.all_to_all(array, axes, 0, 0, tiled=True)  32.2 us
    all_gather x1, blocking collectives, local(): got = lax.all_gather(kernel(quad_sum_body, (shape, BF16), got), 'far')  20.5 us
    ppermute x5, starting transfers between devices, other(): return lax.ppermute(array, axis, [(0, 1), (1, 0)])  11.6 us
    pallas_call x15, Pallas kernels, kernel(): pl.pallas_call(body, out_shape=shapes if several else shapes[0], in_specs...  9.61 us
    ppermute x5, waiting for transfers between devices, other(): return lax.ppermute(array, axis, [(0, 1), (1, 0)])  6.47 us
    unnamed x38, local copies, waits for them, and re-layouts  6.29 us
  transfers between devices with their start and end apart: 8, of which 6 were waited for; matrix products, arithmetic and copies ran while one was open for 0% of the time, Pallas kernels for 2%

profile of v9, /device:TPU:80, one launch (start us, length us, event | category | flops | bytes accessed | tf_op | source)
XLA Modules:
  0.0 227.9 jit_solution(10447468420159305076)
XLA Ops:
  0.7 0.8 fusion.20
  1.4 0.9 fusion.14
  2.5 1.0 fusion.16
  3.7 0.8 copy-done.16
  6.5 2.0 collective-permute-start
  9.2 43.7 %all-to-all-start = ((bf16[16,32,256]{2,1,0:T(8,128)(2,1)}), bf16[16,32,256]{2,1,0:T(8,128)(2,1)S(1)}, u32[]{:S(2)}, u32[]{:S(2)}) async-start(bf16[16,32,256]{2,1,0:T(8,128)(2,1)} %shard_map.140), calls=%async_computation | async-start | bytes 524288 | tf_op jit(solution)/shard_map/all_to_all | solution.py:27
  52.9 18.6 %all-to-all-done = bf16[16,32,256]{2,1,0:T(8,128)(2,1)S(1)} async-done(((bf16[16,32,256]{2,1,0:T(8,128)(2,1)}), bf16[16,32,256]{2,1,0:T(8,128)(2,1)S(1)}, u32[]{:S(2)}, u32[]{:S(2)}) %all-to-all-start) | async-done | bytes 262176 | tf_op jit(solution)/shard_map/all_to_all | solution.py:27
  71.5 2.0 collective-permute-start.1
  73.5 1.3 collective-permute-done.1.x_next_ref
  75.3 0.8 copy-done.1
  76.1 8.9 %all-to-all-start.1 = ((bf16[16,120,128]{2,1,0:T(8,128)(2,1)}), bf16[16,120,128]{2,1,0:T(8,128)(2,1)}, u32[]{:S(2)}, u32[]{:S(2)}) async-start(bf16[16,120,128]{2,1,0:T(8,128)(2,1)} %copy-done.1), calls=%async_computation.1 | async-start | bytes 983040 | tf_op jit(solution)/shard_map/all_to_all | solution.py:27
  85.7 0.8 copy-done.2
  87.1 0.8 shard_map.143
  87.9 3.6 %collective-permute-start.2 = (bf16[2,160,512]{2,1,0:T(8,128)(2,1)}, bf16[2,160,512]{2,1,0:T(8,128)(2,1)}, u32[]{:S(2)}, u32[]{:S(2)}) collective-permute-start(bf16[2,160,512]{2,1,0:T(8,128)(2,1)} %get-tuple-element.20), channel_id=1, source_target_pairs={{0,16},{16,0},{1,17},{17,1},{2,18},{18,2},{3,19},{19,3},{4,20},{20... | collective-permute-start | bytes 983048 | tf_op jit(solution)/shard_map/ppermute | solution.py:31
  91.6 7.9 %all-to-all-done.1 = bf16[16,120,128]{2,1,0:T(8,128)(2,1)} async-done(((bf16[16,120,128]{2,1,0:T(8,128)(2,1)}), bf16[16,120,128]{2,1,0:T(8,128)(2,1)}, u32[]{:S(2)}, u32[]{:S(2)}) %all-to-all-start.1) | async-done | bytes 491552 | tf_op jit(solution)/shard_map/all_to_all | solution.py:27
  99.5 1.1 shard_map.142.got_ref
  100.6 1.4 shard_map.144
  103.2 15.0 %all_to_all.45.left_ref = bf16[16,16,256]{2,1,0:T(8,128)(2,1)S(1)} all-to-all(bf16[16,16,256]{2,1,0:T(8,128)(2,1)S(1)} %get-tuple-element.24), channel_id=1, replica_groups=mesh['grp'=2,'far'=4,'near'=2,'b'=2,'c'=8,'k'=2] {'b','c'}, dimensions={0} | all-to-all | bytes 262144 | tf_op jit(solution)/shard_map/all_to_all | solution.py:27
  118.5 10.8 %all_to_all.46.got_ref = bf16[4,128,256]{2,1,0:T(8,128)(2,1)S(1)} all-to-all(bf16[4,128,256]{2,1,0:T(8,128)(2,1)S(1)} %bitcast.59), channel_id=1, replica_groups=mesh['grp'=2,'far'=4,'near'=2,'b'=2,'c'=8,'k'=2] {'near','b'}, dimensions={0} | all-to-all | bytes 524288 | tf_op jit(solution)/shard_map/all_to_all | solution.py:27
  129.3 20.5 %all-gather = bf16[512,256]{1,0:T(8,128)(2,1)S(1)} all-gather(bf16[128,256]{1,0:T(8,128)(2,1)S(1)} %shard_map.146), channel_id=2, replica_groups=mesh['grp'=2,'far'=4,'near'=2,'b'=2,'c'=8,'k'=2] {'far'}, dimensions={0}, use_global_device_ids=true | all-gather | bytes 327680 | tf_op jit(solution)/shard_map/all_gather | solution.py:395
  149.9 10.4 %all_to_all.47 = bf16[4,128,256]{2,1,0:T(8,128)(2,1)S(1)} all-to-all(bf16[4,128,256]{2,1,0:T(8,128)(2,1)S(1)} %shard_map.147), channel_id=1, replica_groups=mesh['grp'=2,'far'=4,'near'=2,'b'=2,'c'=8,'k'=2] {'near','b'}, dimensions={0} | all-to-all | bytes 524288 | tf_op jit(solution)/shard_map/all_to_all | solution.py:27
  160.8 13.7 %all_to_all.48 = bf16[16,120,128]{2,1,0:T(8,128)(2,1)S(1)} all-to-all(bf16[16,120,128]{2,1,0:T(8,128)(2,1)S(1)} %get-tuple-element.25), channel_id=1, replica_groups=mesh['grp'=2,'far'=4,'near'=2,'b'=2,'c'=8,'k'=2] {'b','c'}, dimensions={0} | all-to-all | bytes 983040 | tf_op jit(solution)/shard_map/all_to_all | solution.py:27
  174.6 1.4 shard_map.150
  176.1 15.3 %all_to_all.49.left_ref = bf16[16,16,256]{2,1,0:T(8,128)(2,1)S(1)} all-to-all(bf16[16,16,256]{2,1,0:T(8,128)(2,1)S(1)} %get-tuple-element.27), channel_id=1, replica_groups=mesh['grp'=2,'far'=4,'near'=2,'b'=2,'c'=8,'k'=2] {'b','c'}, dimensions={0} | all-to-all | bytes 262144 | tf_op jit(solution)/shard_map/all_to_all | solution.py:27
  191.4 2.0 collective-permute-start.3
  193.4 1.3 collective-permute-done.3
  194.9 11.9 %all_to_all.50.got_ref = bf16[4,128,256]{2,1,0:T(8,128)(2,1)S(1)} all-to-all(bf16[4,128,256]{2,1,0:T(8,128)(2,1)S(1)} %bitcast.60), channel_id=1, replica_groups=mesh['grp'=2,'far'=4,'near'=2,'b'=2,'c'=8,'k'=2] {'near','b'}, dimensions={0} | all-to-all | bytes 524288 | tf_op jit(solution)/shard_map/all_to_all | solution.py:27
  207.5 6.7 %all-to-all-start.8 = ((bf16[4,32,256]{2,1,0:T(8,128)(2,1)}), bf16[4,32,256]{2,1,0:T(8,128)(2,1)S(1)}, u32[]{:S(2)}, u32[]{:S(2)}) async-start(bf16[4,32,256]{2,1,0:T(8,128)(2,1)} %bitcast.25), calls=%async_computation.8 | async-start | bytes 131072 | tf_op jit(solution)/shard_map/all_to_all | solution.py:27
  214.3 2.2 collective-permute-start.4
  216.4 3.8 %collective-permute-done.4.theirs_ref = bf16[2,96,128]{2,1,0:T(8,128)(2,1)S(1)} collective-permute-done((bf16[2,96,128]{2,1,0:T(8,128)(2,1)S(1)}, bf16[2,96,128]{2,1,0:T(8,128)(2,1)S(1)}, u32[]{:S(2)}, u32[]{:S(2)}) %collective-permute-start.4) | collective-permute-done | bytes 49184 | tf_op jit(solution)/shard_map/ppermute | solution.py:31
  220.3 1.3 shard_map.154
  221.6 5.7 %all-to-all-done.8.got_ref = bf16[4,32,256]{2,1,0:T(8,128)(2,1)S(1)} async-done(((bf16[4,32,256]{2,1,0:T(8,128)(2,1)}), bf16[4,32,256]{2,1,0:T(8,128)(2,1)S(1)}, u32[]{:S(2)}, u32[]{:S(2)}) %all-to-all-start.8) | async-done | bytes 65568 | tf_op jit(solution)/shard_map/all_to_all | solution.py:27
  (62 shorter events, 8.6 us)
Async XLA Ops:
  0.6 1.7 copy-start.17
  0.6 2.8 %copy-start.12 = (bf16[2,256,256]{2,1,0:T(8,128)(2,1)S(1)}, bf16[2,256,256]{2,1,0:T(8,128)(2,1)}, u32[]{:S(2)}) copy-start(bf16[2,256,256]{2,1,0:T(8,128)(2,1)} %param.19) | copy-start | bytes 786436
  2.4 1.2 copy-start.13
  3.6 0.9 copy-start.16
  4.5 0.9 copy-start.18
  5.5 1.0 copy-start.14
  6.5 2.0 copy-start.8
  6.5 65.0 %collective-permute-start = (bf16[256,2048]{1,0:T(8,128)(2,1)S(1)}, bf16[256,2048]{1,0:T(8,128)(2,1)S(1)}, u32[]{:S(2)}, u32[]{:S(2)}) collective-permute-start(bf16[256,2048]{1,0:T(8,128)(2,1)S(1)} %bitcast_dynamic-update-slice_fusion.mine_ref), channel_id=1, source_target_pairs={{0,1},{1,0},{2,3},{3,2},{4,5},{5,4},{6,7},{7,6},{8,9},{9,8},{10,11... | collective-permute-start | bytes 3145736 | tf_op jit(solution)/shard_map/ppermute | solution.py:31
  9.2 62.3 %all-to-all-start = ((bf16[16,32,256]{2,1,0:T(8,128)(2,1)}), bf16[16,32,256]{2,1,0:T(8,128)(2,1)S(1)}, u32[]{:S(2)}, u32[]{:S(2)}) async-start(bf16[16,32,256]{2,1,0:T(8,128)(2,1)} %shard_map.140), calls=%async_computation | async-start | bytes 524288 | tf_op jit(solution)/shard_map/all_to_all | solution.py:27
  71.5 3.3 %collective-permute-start.1 = (bf16[8,32,256]{2,1,0:T(8,128)(2,1)S(1)}, bf16[8,32,256]{2,1,0:T(8,128)(2,1)S(1)}, u32[]{:S(2)}, u32[]{:S(2)}) collective-permute-start(bf16[8,32,256]{2,1,0:T(8,128)(2,1)S(1)} %dynamic-slice_bitcast_fusion), channel_id=1, source_target_pairs={{0,1},{1,0},{2,3},{3,2},{4,5},{5,4},{6,7},{7,6},{8,9},{9,8},{10,11... | collective-permute-start | bytes 393224 | tf_op jit(solution)/shard_map/ppermute | solution.py:31
  74.8 10.2 %copy-start = (f32[2,2,128,512]{3,2,1,0:T(8,128)S(1)}, f32[2,2,128,512]{3,2,1,0:T(8,128)}, u32[]{:S(2)}) copy-start(f32[2,2,128,512]{3,2,1,0:T(8,128)} %memory_ref.7) | copy-start | bytes 3145732
  75.3 0.8 copy-start.1
  76.1 23.4 %all-to-all-start.1 = ((bf16[16,120,128]{2,1,0:T(8,128)(2,1)}), bf16[16,120,128]{2,1,0:T(8,128)(2,1)}, u32[]{:S(2)}, u32[]{:S(2)}) async-start(bf16[16,120,128]{2,1,0:T(8,128)(2,1)} %copy-done.1), calls=%async_computation.1 | async-start | bytes 983040 | tf_op jit(solution)/shard_map/all_to_all | solution.py:27
  85.0 0.7 copy-start.9
  85.0 0.7 copy-start.11
  85.7 0.8 copy-start.2
  86.5 0.7 copy-start.10
  87.9 12.7 %collective-permute-start.2 = (bf16[2,160,512]{2,1,0:T(8,128)(2,1)}, bf16[2,160,512]{2,1,0:T(8,128)(2,1)}, u32[]{:S(2)}, u32[]{:S(2)}) collective-permute-start(bf16[2,160,512]{2,1,0:T(8,128)(2,1)} %get-tuple-element.20), channel_id=1, source_target_pairs={{0,16},{16,0},{1,17},{17,1},{2,18},{18,2},{3,19},{19,3},{4,20},{20... | collective-permute-start | bytes 983048 | tf_op jit(solution)/shard_map/ppermute | solution.py:31
  99.5 1.1 copy-start.3
  102.0 0.6 copy-start.4
  102.6 0.6 copy-start.6
  176.0 17.3 %copy-start.15 = (bf16[2,256,256]{2,1,0:T(8,128)(2,1)S(1)}, bf16[2,256,256]{2,1,0:T(8,128)(2,1)}, u32[]{:S(2)}) copy-start(bf16[2,256,256]{2,1,0:T(8,128)(2,1)} %param.24) | copy-start | bytes 786436
  191.4 3.3 %collective-permute-start.3 = (bf16[18,16,256]{2,1,0:T(8,128)(2,1)S(1)}, bf16[18,16,256]{2,1,0:T(8,128)(2,1)S(1)}, u32[]{:S(2)}, u32[]{:S(2)}) collective-permute-start(bf16[18,16,256]{2,1,0:T(8,128)(2,1)S(1)} %pad_maximum_fusion), channel_id=1, source_target_pairs={{0,1},{1,0},{2,3},{3,2},{4,5},{5,4},{6,7},{7,6},{8,9},{9,8},{10,11... | collective-permute-start | bytes 442376 | tf_op jit(solution)/shard_map/ppermute | solution.py:31
  207.5 6.7 %copy-start.7 = (bf16[96,128]{1,0:T(8,128)(2,1)S(1)}, bf16[96,128]{1,0:T(8,128)(2,1)}, u32[]{:S(2)}) copy-start(bf16[96,128]{1,0:T(8,128)(2,1)} %copy-done.6) | copy-start | bytes 73732
  207.5 19.7 %all-to-all-start.8 = ((bf16[4,32,256]{2,1,0:T(8,128)(2,1)}), bf16[4,32,256]{2,1,0:T(8,128)(2,1)S(1)}, u32[]{:S(2)}, u32[]{:S(2)}) async-start(bf16[4,32,256]{2,1,0:T(8,128)(2,1)} %bitcast.25), calls=%async_computation.8 | async-start | bytes 131072 | tf_op jit(solution)/shard_map/all_to_all | solution.py:27
  214.2 6.0 %copy-start.5 = (bf16[96,128]{1,0:T(8,128)(2,1)S(1)}, bf16[96,128]{1,0:T(8,128)(2,1)}, u32[]{:S(2)}) copy-start(bf16[96,128]{1,0:T(8,128)(2,1)} %copy-done.4) | copy-start | bytes 73732
  214.3 6.0 %collective-permute-start.4 = (bf16[2,96,128]{2,1,0:T(8,128)(2,1)S(1)}, bf16[2,96,128]{2,1,0:T(8,128)(2,1)S(1)}, u32[]{:S(2)}, u32[]{:S(2)}) collective-permute-start(bf16[2,96,128]{2,1,0:T(8,128)(2,1)S(1)} %pad_maximum_fusion.1), channel_id=1, source_target_pairs={{0,16},{16,0},{1,17},{17,1},{2,18},{18,2},{3,19},{19,3},{4,20},{20... | collective-permute-start | bytes 147464 | tf_op jit(solution)/shard_map/ppermute | solution.py:31
